TPU v7x, 512 devices: a whole 4x8x8 slice. The times are simulated.
512 devices in a mesh: sp: 64 (over z, y), tp: 8 (over x, core).
Axes of the slice: x: 4, y: 8, z: 8, core: 2. Of those that a mesh axis runs over, the one named last changes fastest.
Arguments:
- query_one: bfloat16 [8192, 1024], P('sp', 'tp'), may hold values from -85 to 85
- key_one: bfloat16 [8192, 1024], P('sp', 'tp'), may hold values from -6.5 to 6.5
- query_two: bfloat16 [8192, 1024], P('sp', 'tp'), may hold values from -85 to 85
- key_two: bfloat16 [8192, 1024], P('sp', 'tp'), may hold values from -6.5 to 6.5
- values: bfloat16 [8192, 2048], P('sp', 'tp'), may hold values from -6 to 6
- mix_weight: float32 [8], P('tp'), may hold values from 0.3 to 0.8
- head_gain: float32 [256], replicated, may hold values from 0.1 to 1.9
- residual: bfloat16 [8192, 2048], P(('sp', 'tp')), may hold values from -6 to 6
- out_weight: bfloat16 [2048, 2048], P('tp'), may hold values from -0.125 to 0.125
- norm_gain: float32 [2048], replicated, may hold values from 0.1 to 1.9
- lift_weight: bfloat16 [2048, 5632], P('sp', 'tp'), may hold values from -0.125 to 0.125
- gate_weight: bfloat16 [2048, 5632], P('sp', 'tp'), may hold values from -0.125 to 0.125
- conv_taps: float32 [3, 5632], P(None, 'tp'), may hold values from -3 to 3
- down_weight: bfloat16 [5632, 2048], P('tp'), may hold values from -0.078125 to 0.078125
Outputs:
- layer_out: bfloat16 [8192, 2048], P(('sp', 'tp'))
All inputs are finite; a program needn't handle non-finite values.
Results may differ from a plain program's by a relative error of at most 0.015.
Values may be sent and summed in bfloat16 or wider, within the bound.
No kernel may reach another device: no remote copies, remote signals or barrier semaphores. Data moves between devices by JAX's collectives and lax.ppermute only.
A program may use at most 64 MiB of HBM per device.

v0:
```python
import jax
import jax.numpy as jnp
from jax import lax
from jax.sharding import PartitionSpec as P

HD = 128
STRETCH = 64
WIDTH = 3


epsilon = 1e-06
masked_score = -1e30


def sent_together(arrays, axis, dim, along):
    ends, at = ([], 0)
    for a in arrays[:-1]:
        at += a.shape[along]
        ends.append(at)
    both = jnp.concatenate(arrays, axis=along)
    return tuple(jnp.split(lax.all_gather(both, axis, axis=dim, tiled=True), ends, axis=along))


def in_blocks(shard, dim, peers):
    before, after = (shard.shape[:dim], shard.shape[dim + 1 :])
    return jnp.moveaxis(shard.reshape(*before, peers, -1, *after), dim, 0)


def sent_and_summed(shard, axis, dim):
    parts = in_blocks(shard, dim, lax.axis_size(axis))
    arrived = lax.all_to_all(parts, axis, split_axis=0, concat_axis=0, tiled=True)
    return arrived.astype(jnp.float32).sum(axis=0)


def joined_along(parts, dim):
    parts = jnp.moveaxis(parts, 0, dim)
    lengths = parts.shape
    return parts.reshape(*lengths[:dim], lengths[dim] * lengths[dim + 1], *lengths[dim + 2 :])


def from_everyone(shard, axis):
    peers = lax.axis_size(axis)
    return lax.all_to_all(
        jnp.broadcast_to(shard[None], (peers, *shard.shape)), axis, 0, 0, tiled=True
    )


def gathered_copies(shard, axis, dim):
    return joined_along(from_everyone(shard, axis), dim)


def passed_along(block, axis, distance):
    devices = range(lax.axis_size(axis))
    route = [(i - distance, i) for i in devices if i - distance in devices]
    return lax.ppermute(block, axis, route)


def update_map(peak, total, acc, queries, keys, vals, visible):
    scores = jnp.einsum("thd,shd->hts", queries, keys, preferred_element_type=jnp.float32) * HD ** (
        -0.5
    )
    scores = jnp.where(visible[None], scores, masked_score)
    new_peak = jnp.maximum(peak, jnp.max(scores, axis=-1))
    weights = jnp.where(visible[None], jnp.exp(scores - new_peak[..., None]), 0.0)
    total = jnp.sum(weights, axis=-1)
    acc = jnp.einsum(
        "hts,she->hte", weights.astype(jnp.bfloat16), vals, preferred_element_type=jnp.float32
    )
    return (new_peak, total, acc)


def on_device(
    query_one,
    key_one,
    query_two,
    key_two,
    values,
    mix_weight,
    head_gain,
    residual,
    out_weight,
    norm_gain,
    lift_weight,
    gate_weight,
    conv_taps,
    down_weight,
):
    tok_local = query_one.shape[0]
    heads_local = mix_weight.shape[0]
    val_width = values.shape[1] // heads_local
    model_width = residual.shape[1]
    offset = lax.axis_index("sp") * tok_local
    q_pos = offset + lax.iota(jnp.int32, tok_local)
    q_one = query_one.reshape(tok_local, heads_local, HD)
    q_two = query_two.reshape(tok_local, heads_local, HD)
    start_peak = jnp.full((heads_local, tok_local), masked_score, jnp.float32)
    start_total = jnp.zeros((heads_local, tok_local), jnp.float32)
    start_acc = jnp.zeros((heads_local, tok_local, val_width), jnp.float32)
    initial = (start_peak, start_total, start_acc, start_peak, start_total, start_acc)
    first_keys, second_keys, piece_vals = sent_together((key_one, key_two, values), "sp", 0, 1)
    count = first_keys.shape[0]
    k_pos = lax.iota(jnp.int32, count)
    visible = k_pos[None, :] // STRETCH <= q_pos[:, None] // STRETCH
    first_keys = first_keys.reshape(count, heads_local, HD)
    second_keys = second_keys.reshape(count, heads_local, HD)
    piece_vals = piece_vals.reshape(count, heads_local, val_width)
    first = update_map(initial[0], initial[1], initial[2], q_one, first_keys, piece_vals, visible)
    second = update_map(initial[3], initial[4], initial[5], q_two, second_keys, piece_vals, visible)
    state = first + second
    mixed = (
        state[2] / state[1][..., None] - mix_weight[:, None, None] * state[5] / state[4][..., None]
    )
    head_out = (
        mixed * lax.rsqrt(jnp.mean(mixed * mixed, axis=-1, keepdims=True) + epsilon) * head_gain
    ).astype(jnp.bfloat16)
    out_heads = out_weight.reshape(heads_local, val_width, model_width)
    piece = head_out
    attended = sent_and_summed(
        jnp.einsum("hte,hed->td", piece, out_heads, preferred_element_type=jnp.float32).astype(
            jnp.bfloat16
        ),
        "tp",
        0,
    )
    stream = residual.astype(jnp.float32) + attended
    normed = (
        stream * lax.rsqrt(jnp.mean(stream * stream, axis=-1, keepdims=True) + epsilon) * norm_gain
    ).astype(jnp.bfloat16)
    whole_rows = gathered_copies(normed, "tp", 0)
    pieces = sent_together((lift_weight, gate_weight), "sp", 0, 1)
    lift_pre = jnp.dot(whole_rows, pieces[0], preferred_element_type=jnp.float32)
    gate_pre = jnp.dot(whole_rows, pieces[1], preferred_element_type=jnp.float32)
    lifted = lift_pre.astype(jnp.bfloat16)
    gated = gate_pre.astype(jnp.bfloat16)
    prior = passed_along(gated[tok_local - (WIDTH - 1) :], "sp", 1)
    extended = jnp.concatenate([prior, gated], axis=0).astype(jnp.float32)
    conv = conv_taps[0] * extended[0:tok_local]
    for index in range(1, WIDTH):
        conv = conv + conv_taps[index] * extended[index : index + tok_local]
    hidden = (jax.nn.silu(conv) * lifted.astype(jnp.float32)).astype(jnp.bfloat16)
    piece = hidden
    mixer = sent_and_summed(
        jnp.dot(piece, down_weight, preferred_element_type=jnp.float32).astype(jnp.bfloat16),
        "tp",
        0,
    )
    return (stream + mixer).astype(jnp.bfloat16)


def solution(mesh):
    return jax.shard_map(
        on_device,
        mesh=mesh,
        in_specs=(
            P("sp", "tp"),
            P("sp", "tp"),
            P("sp", "tp"),
            P("sp", "tp"),
            P("sp", "tp"),
            P("tp"),
            P(),
            P(("sp", "tp"), None),
            P("tp", None),
            P(),
            P("sp", "tp"),
            P("sp", "tp"),
            P(None, "tp"),
            P("tp", None),
        ),
        out_specs=P(("sp", "tp"), None),
        check_vma=False,
    )
```

profile of v0, /device:TPU:64, one launch (start us, length us, event | category | flops | bytes accessed | tf_op | source)
XLA Modules:
  0.0 246.5 jit_solution(9248590549182216705)
XLA Ops:
  6.5 1.7 pad_maximum_fusion
  8.3 1.5 pad_maximum_fusion.1
  10.5 101.7 %all-gather.3.cloned.1.call-done = bf16[8192,512]{1,0:T(8,128)(2,1)} async-done(((bf16[128,512]{1,0:T(8,128)(2,1)}), bf16[8192,512]{1,0:T(8,128)(2,1)}) %all-gather.3.cloned.1.call-update) | async-done | bytes 8388624 | tf_op jit(solution)/shard_map/all_gather | solution.py:21
  112.2 6.1 %fusion.85 = (f32[128]{0:T(128)S(1)}, f32[128,8192]{0,1:T(8,128)S(1)}) fusion(bf16[128,128]{1,0:T(8,128)(2,1)} %param.14, bf16[8192,512]{1,0:T(8,128)(2,1)} %all-gather.3.cloned.1.call-done, s32[128]{0:T(128)S(1)} %and_select_fusion, s32[8192]{0:T(1024)S(1)} %add_select_fusion), kind=kOutput, calls=%fused_computation.89 | convolution fusion | flops 272629632 | bytes 6358016 | tf_op jit(solution)/shard_map/thd,shd->hts/dot_general | solution.py:59
  118.4 1.3 fusion.86
  119.7 3.8 %fusion.10 = (f32[128]{0:T(128)S(1)}, f32[128]{0:T(128)S(1)}) fusion(f32[128,8192]{0,1:T(8,128)S(1)} %get-tuple-element.13, f32[128]{0:T(128)S(1)} %get-tuple-element.16, s32[128]{0:T(128)S(1)} %and_select_fusion, s32[8192]{0:T(1024)S(1)} %add_select_fusion, f32[128,8192]{0,1:T(8,128)S(1)} %get-tuple-element.11, f32[128]{0:T(128)S(1)} %get-tuple-element.17), kind=kLoop, calls=%fused_computation.14 | loop fusion | flops 7339776 | bytes 8423936 | tf_op jit(solution)/shard_map/reduce_sum | solution.py:65
  123.4 2.1 fusion.58
  125.6 2.2 multiply_reduce_fusion.1
  127.8 0.4 convolution_convert_fusion.1
  128.2 14.4 %all_to_all.15 = bf16[8,16,2048]{2,1,0:T(8,128)(2,1)S(1)} all-to-all(bf16[8,16,2048]{2,1,0:T(8,128)(2,1)S(1)} %bitcast.19), channel_id=1, replica_groups=mesh['sp'=64,'tp'=8] {'tp'}, dimensions={0} | all-to-all | bytes 1048576 | tf_op jit(solution)/shard_map/all_to_all | solution.py:31
  142.6 0.1 convert_reduce_fusion.1
  142.6 0.1 multiply_reduce_fusion
  142.8 0.1 multiply_convert_fusion
  142.9 0.8 broadcast_in_dim.16
  143.7 4.1 %all-to-all-start.1 = ((bf16[8,16,2048]{2,1,0:T(8,128)(2,1)}), bf16[8,16,2048]{2,1,0:T(8,128)(2,1)}, u32[]{:S(2)}, u32[]{:S(2)}) async-start(bf16[8,16,2048]{2,1,0:T(8,128)(2,1)} %broadcast_in_dim.16), calls=%async_computation.1 | async-start | bytes 1048576 | tf_op jit(solution)/shard_map/all_to_all | solution.py:43
  147.9 55.3 %all-gather.5.cloned.1.call-done = bf16[2048,1408]{1,0:T(8,128)(2,1)} async-done(((bf16[32,1408]{1,0:T(8,128)(2,1)}), bf16[2048,1408]{1,0:T(8,128)(2,1)}) %all-gather.5.cloned.1.call-update) | async-done | bytes 5767184 | tf_op jit(solution)/shard_map/all_gather | solution.py:21
  203.2 4.8 %fusion.28 = bf16[128,704]{0,1:T(8,128)(2,1)S(1)} fusion(bf16[128,2048]{1,0:T(8,128)(2,1)} %bitcast.4, bf16[2048,1408]{1,0:T(8,128)(2,1)} %all-gather.5.cloned.1.call-done), kind=kOutput, calls=%fused_computation.32 | convolution fusion | flops 369188864 | bytes 3850240 | tf_op jit(solution)/shard_map/dot_general | solution.py:132
  208.0 0.1 slice.28
  208.1 2.9 %collective-permute-start = (bf16[2,704]{0,1:T(8,128)(2,1)S(1)}, bf16[2,704]{0,1:T(8,128)(2,1)S(1)}, u32[]{:S(2)}, u32[]{:S(2)}) collective-permute-start(bf16[2,704]{0,1:T(8,128)(2,1)S(1)} %slice.28), channel_id=1, source_target_pairs={{0,8},{8,16},{16,24},{24,32},{32,40},{40,48},{48,56},{56,64},{64,7... | collective-permute-start | bytes 8456 | tf_op jit(solution)/shard_map/ppermute | solution.py:55
  211.0 6.5 %collective-permute-done = bf16[2,704]{0,1:T(8,128)(2,1)S(1)} collective-permute-done((bf16[2,704]{0,1:T(8,128)(2,1)S(1)}, bf16[2,704]{0,1:T(8,128)(2,1)S(1)}, u32[]{:S(2)}, u32[]{:S(2)}) %collective-permute-start) | collective-permute-done | bytes 2848 | tf_op jit(solution)/shard_map/ppermute | solution.py:55
  217.6 1.0 maximum_convert_fusion
  218.6 5.7 %convolution_convert_fusion = bf16[128,2048]{1,0:T(8,128)(2,1)} fusion(bf16[704,2048]{1,0:T(8,128)(2,1)S(1)} %copy-done, bf16[128,2048]{1,0:T(8,128)(2,1)} %bitcast.4, bf16[2048,1408]{1,0:T(8,128)(2,1)} %all-gather.5.cloned.1.call-done, f32[130,704]{0,1:T(8,128)} %maximum_convert_fusion, f32[704]{0:T(1024)S(1)} %get-tuple-element.8, ...), kind=kOutput, calls=%fused_computation.20 | convolution fusion | flops 739631104 | bytes 8167680 | tf_op jit(solution)/shard_map/dot_general | solution.py:143
  224.3 14.6 %all_to_all.16 = bf16[8,16,2048]{2,1,0:T(8,128)(2,1)S(1)} all-to-all(bf16[8,16,2048]{2,1,0:T(8,128)(2,1)} %bitcast.20), channel_id=1, replica_groups=mesh['sp'=64,'tp'=8] {'tp'}, dimensions={0} | all-to-all | bytes 1048576 | tf_op jit(solution)/shard_map/all_to_all | solution.py:31
  239.0 0.7 add_convert_fusion
  (28 shorter events, 0.3 us)
Async XLA Ops:
  6.5 212.1 %copy-start = (bf16[704,2048]{1,0:T(8,128)(2,1)S(1)}, bf16[704,2048]{1,0:T(8,128)(2,1)}, u32[]{:S(2)}) copy-start(bf16[704,2048]{1,0:T(8,128)(2,1)} %param.27) | copy-start | bytes 8650756
  6.5 105.7 %all-gather.3.cloned.1.call-start = ((), (), s32[]{:S(2)}) async-start(), calls=%async_computation.3 | async-start | bytes 8519680 | tf_op jit(solution)/shard_map/all_gather | solution.py:21
  8.2 195.0 %all-gather.5.cloned.1.call-start = ((), (), s32[]{:S(2)}) async-start(), calls=%async_computation.4 | async-start | bytes 5857280 | tf_op jit(solution)/shard_map/all_gather | solution.py:21
  10.5 107.9 %copy-start.7 = (bf16[128,128]{1,0:T(8,128)(2,1)S(1)}, bf16[128,128]{1,0:T(8,128)(2,1)}, u32[]{:S(2)}) copy-start(bf16[128,128]{1,0:T(8,128)(2,1)} %param.16) | copy-start | bytes 98308
  112.2 6.2 %copy-start.6 = (bf16[8192,512]{1,0:T(8,128)(2,1)S(1)}, bf16[8192,512]{1,0:T(8,128)(2,1)}, u32[]{:S(2)}) copy-start(bf16[8192,512]{1,0:T(8,128)(2,1)} %all-gather.3.cloned.1.call-done) | copy-start | bytes 25165828
  125.5 2.2 copy-start.1
  125.5 2.2 copy-start.5
  125.6 17.1 %copy-start.2 = (bf16[16,2048]{1,0:T(8,128)(2,1)S(1)}, bf16[16,2048]{1,0:T(8,128)(2,1)}, u32[]{:S(2)}) copy-start(bf16[16,2048]{1,0:T(8,128)(2,1)} %param.21) | copy-start | bytes 196612
  125.6 17.2 %copy-start.3 = (f32[2048]{0:T(1024)S(1)}, f32[2048]{0:T(1024)}, u32[]{:S(2)}) copy-start(f32[2048]{0:T(1024)} %param.23) | copy-start | bytes 24580
  128.1 82.8 %copy-start.4 = (f32[3,704]{1,0:T(4,128)S(1)}, f32[3,704]{1,0:T(4,128)}, u32[]{:S(2)}) copy-start(f32[3,704]{1,0:T(4,128)} %param.26) | copy-start | bytes 25348
  143.7 59.5 %all-to-all-start.1 = ((bf16[8,16,2048]{2,1,0:T(8,128)(2,1)}), bf16[8,16,2048]{2,1,0:T(8,128)(2,1)}, u32[]{:S(2)}, u32[]{:S(2)}) async-start(bf16[8,16,2048]{2,1,0:T(8,128)(2,1)} %broadcast_in_dim.16), calls=%async_computation.1 | async-start | bytes 1048576 | tf_op jit(solution)/shard_map/all_to_all | solution.py:43
  208.1 9.5 %collective-permute-start = (bf16[2,704]{0,1:T(8,128)(2,1)S(1)}, bf16[2,704]{0,1:T(8,128)(2,1)S(1)}, u32[]{:S(2)}, u32[]{:S(2)}) collective-permute-start(bf16[2,704]{0,1:T(8,128)(2,1)S(1)} %slice.28), channel_id=1, source_target_pairs={{0,8},{8,16},{16,24},{24,32},{32,40},{40,48},{48,56},{56,64},{64,7... | collective-permute-start | bytes 8456 | tf_op jit(solution)/shard_map/ppermute | solution.py:55
Sparse Core Ops, SparseCore 0:
  10.4 101.8 all-gather.2
  115.3 87.8 all-gather.4
where the time goes:
time: 247 us; the launch traced here: 246 us
  waiting for transfers between devices  164 us (66%)
  blocking collectives  29 us (12%)
  matrix products  22.5 us (9%)
  between operations  14.2 us (6%)
  other arithmetic  9.05 us (4%)
  starting transfers between devices  7.1 us (3%)
    all_gather x2, waiting for transfers between devices, sent_together(): lax.all_gather(both, axis, axis=dim, tiled=True)  157 us
    all_to_all x2, blocking collectives, sent_and_summed(): lax.all_to_all(parts, axis, split_axis=0, concat_axis=0, tiled=True)  29 us
    dot_general x2, matrix products, update_map(): jnp.einsum('thd,shd->hts', queries, keys, preferred_element_type=jnp.floa...  7.4 us
    ppermute x1, waiting for transfers between devices, passed_along(): return lax.ppermute(block, axis, route)  6.53 us
    dot_general x1, matrix products, on_device(): jnp.dot(piece, down_weight, preferred_element_type=jnp.float32)  5.69 us
  transfers between devices with their start and end apart: 4, of which 3 were waited for; matrix products, arithmetic and copies ran while one was open for 8% of the time, Pallas kernels for 0%

commit v1 on v0

v1 whole, which is shorter than its diff:
```python
import jax
import jax.numpy as jnp
import numpy as np
from jax import lax
from jax.experimental import pallas as pl
from jax.experimental.pallas import tpu as pltpu
from jax.sharding import Mesh, PartitionSpec as P

HD = 128
VD = 256
STRETCH = 64
WIDTH = 3
SIDE = 8
BLOCK = 128
PACK = 4 * BLOCK + 16
epsilon = 1e-06
masked_score = -1e30
LOG2E = 1.4426950408889634
EXP2_SCALE = LOG2E * HD**-0.5
f32 = jnp.float32
bf16 = jnp.bfloat16
TP = ("x", "core")
ALL = ("z", "y", "x", "core")
PLACES = np.arange(SIDE * SIDE * 8).reshape(SIDE, SIDE, 4, 2)
ROWS = [[PLACES[i, :, x, c].tolist() for i in range(SIDE) for x in range(4)] for c in range(2)]
COLS = [[PLACES[:, i, x, c].tolist() for i in range(SIDE) for x in range(4)] for c in range(2)]
Q_GROUPS = ROWS[0] + COLS[1]
K_GROUPS = COLS[0] + ROWS[1]


def vmem():
    return pl.BlockSpec(memory_space=pltpu.VMEM)


def pack_kernel(q1, q2, k1, k2, v, qsend, ksend):
    for i in range(SIDE):
        qsend[i, 0:128, :] = q1[...]
        qsend[i, 128:256, :] = q2[...]
        ksend[i, 0:128, :] = k1[...]
        ksend[i, 128:256, :] = k2[...]
        ksend[i, 256:384, :] = v[:, 0:128]
        ksend[i, 384:512, :] = v[:, 128:256]


def attend_kernel(plan, qpool, kpool, out, scores):
    q_base, q_step, k_base, k_step = (plan[i] for i in range(4))
    first_chunk, pairs = plan[4], plan[5]
    row = lax.broadcasted_iota(jnp.int32, (256, 256), 0)
    col = lax.broadcasted_iota(jnp.int32, (256, 256), 1)
    at = lax.broadcasted_iota(jnp.int32, (16, 128), 0)

    def blank(c, carry):
        for h in range(2):
            out[2 * c + h, 0:512, :] = jnp.zeros((512, 128), bf16)
            level = jnp.where((at == 0) | (at == 3), masked_score, 0.0)
            out[2 * c + h, 512:528, :] = level.astype(bf16)
        return carry

    lax.fori_loop(0, first_chunk, blank, 0)

    def chunk(c, carry):
        queries = [
            jnp.concatenate(
                [qpool[2 * c, 128 * m : 128 * m + 128, :], qpool[2 * c + 1, 128 * m : 128 * m + 128, :]],
                axis=0,
            )
            for m in range(2)
        ]
        q_at = 2 * (q_base + q_step * (2 * c + row // 128)) + (row % 128) // STRETCH

        def scored(p, peaks):
            k_at = 2 * (k_base + k_step * (2 * p + col // 128)) + (col % 128) // STRETCH
            seen = k_at <= q_at
            new = []
            for m in range(2):
                k = jnp.concatenate(
                    [kpool[2 * p, 128 * m : 128 * m + 128, :], kpool[2 * p + 1, 128 * m : 128 * m + 128, :]],
                    axis=0,
                )
                s = lax.dot_general(
                    queries[m], k, (((1,), (1,)), ((), ())), preferred_element_type=f32
                )
                s = jnp.where(seen, s, masked_score)
                scores[2 * p + m] = s
                new.append(jnp.maximum(peaks[m], jnp.maximum(s[:, 0:128], s[:, 128:256])))
            return tuple(new)

        low = jnp.full((256, 128), masked_score, f32)
        peaks = lax.fori_loop(0, pairs, scored, (low, low))
        tops = [jnp.max(peak, axis=-1, keepdims=True) for peak in peaks]

        def weighed(p, carry):
            totals, acc = carry
            new, ws = [], []
            for m in range(2):
                w = jnp.exp2((scores[2 * p + m] - tops[m]) * EXP2_SCALE)
                new.append(totals[m] + (w[:, 0:128] + w[:, 128:256]))
                ws.append(w.astype(bf16))
            va = jnp.concatenate([kpool[2 * p, 256:384, :], kpool[2 * p, 384:512, :]], axis=1)
            vb = jnp.concatenate([kpool[2 * p + 1, 256:384, :], kpool[2 * p + 1, 384:512, :]], axis=1)
            vals = jnp.concatenate([va, vb], axis=0)
            acc = acc + jnp.dot(
                jnp.concatenate(ws, axis=0), vals, preferred_element_type=f32
            )
            return tuple(new), acc

        none = jnp.zeros((256, 128), f32)
        totals, acc = lax.fori_loop(
            0, pairs, weighed, ((none, none), jnp.zeros((512, VD), f32))
        )
        levels = []
        for m in range(2):
            total = jnp.sum(totals[m], axis=-1, keepdims=True)
            o = (acc[256 * m : 256 * m + 256] / total).astype(bf16)
            seen = tops[m] > 0.5 * masked_score
            levels.append(jnp.where(seen, tops[m] * EXP2_SCALE + jnp.log2(total), masked_score))
            for h in range(2):
                for e in range(2):
                    out[2 * c + h, 256 * m + 128 * e : 256 * m + 128 * e + 128, :] = o[
                        128 * h : 128 * h + 128, 128 * e : 128 * e + 128
                    ]
        for h in range(2):
            rows = jnp.zeros((16, 128), f32)
            for m in range(2):
                wide = jnp.transpose(
                    jnp.broadcast_to(levels[m][128 * h : 128 * h + 128], (128, 128))
                )[0:16]
                a = wide.astype(bf16).astype(f32)
                b = (wide - a).astype(bf16).astype(f32)
                d = wide - a - b
                for n, piece in enumerate((a, b, d)):
                    rows = jnp.where(at == 3 * m + n, piece, rows)
            out[2 * c + h, 512:528, :] = rows.astype(bf16)
        return carry

    lax.fori_loop(first_chunk, SIDE // 2, chunk, 0)


def join_kernel(mix, parts, gain, weight, out):
    tails = [parts[i, 512:528, :].astype(f32) for i in range(SIDE)]

    def joined(m):
        levels = jnp.concatenate(
            [jnp.sum(tail[3 * m : 3 * m + 3], axis=0, keepdims=True) for tail in tails], axis=0
        )
        top = jnp.max(levels, axis=0, keepdims=True)
        w = jnp.exp2(levels - top)
        w = w / jnp.sum(w, axis=0, keepdims=True)
        w = jnp.transpose(jnp.concatenate([w, jnp.zeros((120, 128), f32)], axis=0))
        acc = [jnp.zeros((128, 128), f32), jnp.zeros((128, 128), f32)]
        for i in range(SIDE):
            wi = w[:, i : i + 1]
            for e in range(2):
                at = 256 * m + 128 * e
                acc[e] = acc[e] + wi * parts[i, at : at + 128, :].astype(f32)
        return jnp.concatenate(acc, axis=1)

    mixed = joined(0) - mix[0] * joined(1)
    r = lax.rsqrt(jnp.mean(mixed * mixed, axis=-1, keepdims=True) + epsilon)
    head = (mixed * r * gain[...]).astype(bf16)
    out[...] = jnp.dot(head, weight[...], preferred_element_type=f32).astype(bf16)


def norm_kernel(parts, residual, gain, stream, normed):
    total = residual[...].astype(f32)
    att = parts[0].astype(f32)
    for i in range(1, 8):
        att = att + parts[i].astype(f32)
    total = total + att
    stream[...] = total
    r = lax.rsqrt(jnp.mean(total * total, axis=-1, keepdims=True) + epsilon)
    n = (total * r * gain[...]).astype(bf16)
    for i in range(8):
        normed[i] = n


def last_kernel(parts, stream, out):
    mixer = parts[0].astype(f32)
    for i in range(1, 8):
        mixer = mixer + parts[i].astype(f32)
    out[...] = (stream[...] + mixer).astype(bf16)


def swapped(a, axis, groups=None):
    return lax.all_to_all(a, axis, 0, 0, axis_index_groups=groups, tiled=True)


def on_device(
    query_one,
    key_one,
    query_two,
    key_two,
    values,
    mix_weight,
    head_gain,
    residual,
    out_weight,
    norm_gain,
    lift_weight,
    gate_weight,
    conv_taps,
    down_weight,
):
    tokens = query_one.shape[0]
    own = residual.shape[0]
    width = residual.shape[1]
    z = lax.axis_index("z")
    y = lax.axis_index("y")
    core = lax.axis_index("core")
    along_y = jnp.stack([z * SIDE, 1 + 0 * z, y, SIDE + 0 * z, 0 * z, z // 2 + 1])
    along_z = jnp.stack([y, SIDE + 0 * z, z * SIDE, 1 + 0 * z, z // 2, SIDE // 2 + 0 * z])
    plan = jnp.where(core == 0, along_y, along_z).astype(jnp.int32)
    qsend, ksend = pl.pallas_call(
        pack_kernel,
        out_shape=[
            jax.ShapeDtypeStruct((SIDE, 256, 128), bf16),
            jax.ShapeDtypeStruct((SIDE, 512, 128), bf16),
        ],
        in_specs=[vmem()] * 5,
        out_specs=[vmem()] * 2,
        name="pack",
    )(query_one, query_two, key_one, key_two, values)
    both = jnp.concatenate([lift_weight, gate_weight], axis=1)
    with jax.named_scope("kpool"):
        kpool = swapped(ksend, ALL, K_GROUPS)
    with jax.named_scope("qpool"):
        qpool = swapped(qsend, ALL, Q_GROUPS)
    weights = lax.all_gather(both, ("z", "y"), axis=0, tiled=True)
    out = pl.pallas_call(
        attend_kernel,
        out_shape=jax.ShapeDtypeStruct((SIDE, PACK, 128), bf16),
        in_specs=[pl.BlockSpec(memory_space=pltpu.SMEM), vmem(), vmem()],
        out_specs=vmem(),
        scratch_shapes=[pltpu.VMEM((8, 256, 256), f32)],
        name="attend",
    )(plan, qpool, kpool)
    back = swapped(out, ALL, Q_GROUPS)
    attended = pl.pallas_call(
        join_kernel,
        out_shape=jax.ShapeDtypeStruct((tokens, width), bf16),
        in_specs=[pl.BlockSpec(memory_space=pltpu.SMEM)] + [vmem()] * 3,
        out_specs=vmem(),
        name="join",
    )(mix_weight, back, head_gain.reshape(1, VD), out_weight)
    parts = swapped(attended.reshape(8, own, width), TP)
    stream, normed = pl.pallas_call(
        norm_kernel,
        out_shape=[
            jax.ShapeDtypeStruct((own, width), f32),
            jax.ShapeDtypeStruct((8, own, width), bf16),
        ],
        in_specs=[vmem()] * 3,
        out_specs=[vmem()] * 2,
        name="norm",
    )(parts, residual, norm_gain.reshape(1, width))
    rows = swapped(normed, TP).reshape(tokens, width)
    units = lift_weight.shape[1]
    lift_pre = jnp.dot(rows, weights[:, :units], preferred_element_type=f32)
    gate_pre = jnp.dot(rows, weights[:, units:], preferred_element_type=f32)
    lifted = lift_pre.astype(bf16)
    gated = gate_pre.astype(bf16)
    route = [(i, i + 1) for i in range(SIDE * SIDE - 1)]
    prior = lax.ppermute(gated[tokens - (WIDTH - 1) :], ("z", "y"), route)
    extended = jnp.concatenate([prior, gated], axis=0).astype(f32)
    conv = conv_taps[0] * extended[0:tokens]
    for index in range(1, WIDTH):
        conv = conv + conv_taps[index] * extended[index : index + tokens]
    hidden = (jax.nn.silu(conv) * lifted.astype(f32)).astype(bf16)
    down = jnp.dot(hidden, down_weight, preferred_element_type=f32).astype(bf16)
    mixer = swapped(down.reshape(8, own, width), TP)
    return pl.pallas_call(
        last_kernel,
        out_shape=jax.ShapeDtypeStruct((own, width), bf16),
        in_specs=[vmem()] * 2,
        out_specs=vmem(),
        name="last",
    )(mixer, stream)


def solution(mesh):
    fine = Mesh(mesh.devices.reshape(SIDE, SIDE, 4, 2), ("z", "y", "x", "core"))
    sp = ("z", "y")
    return jax.shard_map(
        on_device,
        mesh=fine,
        in_specs=(
            P(sp, TP),
            P(sp, TP),
            P(sp, TP),
            P(sp, TP),
            P(sp, TP),
            P(TP),
            P(),
            P(("z", "y", "x", "core"), None),
            P(TP, None),
            P(),
            P(sp, TP),
            P(sp, TP),
            P(None, TP),
            P(TP, None),
        ),
        out_specs=P(("z", "y", "x", "core"), None),
        check_vma=False,
    )
```

time: 247 us -> 183 us (0.74)
  the two profiles are of different devices: /device:TPU:64 before, /device:TPU:8 now
where the time goes in v1:
time: 183 us; the launch traced here: 182 us
  blocking collectives  71.2 us (39%)
  waiting for transfers between devices  50.8 us (28%)
  Pallas kernels  16.5 us (9%)
  starting transfers between devices  15.5 us (8%)
  between operations  14.1 us (8%)
  matrix products  10.2 us (6%)
  other arithmetic  3.26 us (2%)
    all_to_all x4, blocking collectives, swapped(): return lax.all_to_all(a, axis, 0, 0, axis_index_groups=groups, tiled=True)  71.2 us
    all_to_all x2, waiting for transfers between devices, swapped(): return lax.all_to_all(a, axis, 0, 0, axis_index_groups=groups, tiled=True)  44.9 us
    all_to_all x2, starting transfers between devices, swapped(): return lax.all_to_all(a, axis, 0, 0, axis_index_groups=groups, tiled=True)  13.6 us
    pallas_call x1, Pallas kernels, on_device(): pl.pallas_call(attend_kernel, out_shape=jax.ShapeDtypeStruct((SIDE, PACK,...  6.91 us
    ppermute x1, waiting for transfers between devices, on_device(): prior = lax.ppermute(gated[tokens - (WIDTH - 1):], ('z', 'y'), route)  5.84 us
    dot_general x1, matrix products, on_device(): down = jnp.dot(hidden, down_weight, preferred_element_type=f32).astype(bf16)  5.6 us
    dot_general x1, matrix products, on_device(): gate_pre = jnp.dot(rows, weights[:, units:], preferred_element_type=f32)  4.58 us
  transfers between devices with their start and end apart: 4, of which 3 were waited for; matrix products, arithmetic and copies ran while one was open for 0% of the time, Pallas kernels for 8%

profile of v1, /device:TPU:8, one launch (start us, length us, event | category | flops | bytes accessed | tf_op | source)
XLA Modules:
  0.0 181.8 jit_solution(8561980233635227962)
XLA Ops:
  6.5 1.7 pad_maximum_fusion
  8.2 0.0 all-gather.2.cloned.1.call-update
  8.3 2.3 %pack.1 = (bf16[8,256,128]{2,1,0:T(8,128)(2,1)}, bf16[8,512,128]{2,1,0:T(8,128)(2,1)}) custom-call(bf16[128,128]{1,0:T(8,128)(2,1)} %q1.1, bf16[128,128]{1,0:T(8,128)(2,1)} %q2.1, bf16[128,128]{1,0:T(8,128)(2,1)} %k1.1, bf16[128,128]{1,0:T(8,128)(2,1)} %k2.1, bf16[128,256]{1,0:T(8,128)(2,1)} %v.1), custom_call_target="tpu_custom_call" | custom-call | tf_op jit(solution)/shard_map/pack/pallas_call | solution.py:213
  10.5 21.8 %all_to_all.30.qpool = bf16[8,256,128]{2,1,0:T(8,128)(2,1)} all-to-all(bf16[8,256,128]{2,1,0:T(8,128)(2,1)} %get-tuple-element.9), channel_id=1, replica_groups={{0,8,16,24,32,40,48,56},{2,10,18,26,34,42,50,58},{4,12,20,28,36,44,52,6..., dimensions={0} | all-to-all | bytes 1048576 | tf_op jit(solution)/shard_map/qpool/all_to_all | solution.py:185
  32.3 8.1 %all-to-all-start.1 = ((bf16[8,512,128]{2,1,0:T(8,128)(2,1)}), bf16[8,512,128]{2,1,0:T(8,128)(2,1)}, u32[]{:S(2)}, u32[]{:S(2)}) async-start(bf16[8,512,128]{2,1,0:T(8,128)(2,1)} %get-tuple-element.10), calls=%async_computation.1 | async-start | bytes 2097152 | tf_op jit(solution)/shard_map/kpool/all_to_all | solution.py:185
  40.4 0.1 stack.25
  40.5 0.1 stack.23
  40.6 0.5 broadcast_select_fusion.plan
  41.1 20.0 %all-to-all-done.1.kpool = bf16[8,512,128]{2,1,0:T(8,128)(2,1)} async-done(((bf16[8,512,128]{2,1,0:T(8,128)(2,1)}), bf16[8,512,128]{2,1,0:T(8,128)(2,1)}, u32[]{:S(2)}, u32[]{:S(2)}) %all-to-all-start.1) | async-done | bytes 1048608 | tf_op jit(solution)/shard_map/kpool/all_to_all | solution.py:185
  61.1 6.9 %attend.1 = bf16[8,528,128]{2,1,0:T(8,128)(2,1)} custom-call(s32[6]{0:T(128)} %broadcast_select_fusion.plan, bf16[8,256,128]{2,1,0:T(8,128)(2,1)} %all_to_all.30.qpool, bf16[8,512,128]{2,1,0:T(8,128)(2,1)} %all-to-all-done.1.kpool), custom_call_target="tpu_custom_call" | custom-call | tf_op jit(solution)/shard_map/attend/pallas_call | solution.py:229
  68.0 5.5 %all-to-all-start.2 = ((bf16[8,528,128]{2,1,0:T(8,128)(2,1)}), bf16[8,528,128]{2,1,0:T(8,128)(2,1)}, u32[]{:S(2)}, u32[]{:S(2)}) async-start(bf16[8,528,128]{2,1,0:T(8,128)(2,1)} %attend.1), calls=%async_computation.2 | async-start | bytes 2162688 | tf_op jit(solution)/shard_map/all_to_all | solution.py:185
  74.1 24.9 %all-to-all-done.2.parts = bf16[8,528,128]{2,1,0:T(8,128)(2,1)} async-done(((bf16[8,528,128]{2,1,0:T(8,128)(2,1)}), bf16[8,528,128]{2,1,0:T(8,128)(2,1)}, u32[]{:S(2)}, u32[]{:S(2)}) %all-to-all-start.2) | async-done | bytes 1081376 | tf_op jit(solution)/shard_map/all_to_all | solution.py:185
  99.1 3.4 %join.1 = bf16[128,2048]{1,0:T(8,128)(2,1)} custom-call(f32[1]{0:T(128)S(6)} %copy.15.mix, bf16[8,528,128]{2,1,0:T(8,128)(2,1)} %all-to-all-done.2.parts, f32[1,256]{1,0:T(1,128)} %bitcast.17, bf16[256,2048]{1,0:T(8,128)(2,1)} %weight.1), custom_call_target="tpu_custom_call" | custom-call | tf_op jit(solution)/shard_map/join/pallas_call | solution.py:238
  102.5 21.2 %all_to_all.31.parts = bf16[8,16,2048]{2,1,0:T(8,128)(2,1)} all-to-all(bf16[8,16,2048]{2,1,0:T(8,128)(2,1)} %bitcast.12), channel_id=1, replica_groups=mesh['z'=8,'y'=8,'x'=4,'core'=2] {'x','core'}, dimensions={0} | all-to-all | bytes 1048576 | tf_op jit(solution)/shard_map/all_to_all | solution.py:185
  123.7 2.1 %norm.1 = (f32[16,2048]{1,0:T(8,128)}, bf16[8,16,2048]{2,1,0:T(8,128)(2,1)}) custom-call(bf16[8,16,2048]{2,1,0:T(8,128)(2,1)} %all_to_all.31.parts, bf16[16,2048]{1,0:T(8,128)(2,1)} %residual.1, f32[1,2048]{1,0:T(1,128)} %bitcast.16), custom_call_target="tpu_custom_call" | custom-call | tf_op jit(solution)/shard_map/norm/pallas_call | solution.py:246
  125.8 13.8 %all_to_all.32 = bf16[8,16,2048]{2,1,0:T(8,128)(2,1)S(1)} all-to-all(bf16[8,16,2048]{2,1,0:T(8,128)(2,1)} %get-tuple-element.11), channel_id=1, replica_groups=mesh['z'=8,'y'=8,'x'=4,'core'=2] {'x','core'}, dimensions={0} | all-to-all | bytes 1048576 | tf_op jit(solution)/shard_map/all_to_all | solution.py:185
  139.5 4.6 %fusion.4 = bf16[128,704]{0,1:T(8,128)(2,1)S(1)} fusion(bf16[128,2048]{1,0:T(8,128)(2,1)S(1)} %bitcast.13, bf16[2048,1408]{1,0:T(8,128)(2,1)} %all-gather.2.cloned.1.call-done), kind=kOutput, calls=%fused_computation.5 | convolution fusion | flops 369188864 | bytes 3850240 | tf_op jit(solution)/shard_map/dot_general | solution.py:259
  144.1 0.1 slice.37
  144.2 1.9 %collective-permute-start = (bf16[2,704]{0,1:T(8,128)(2,1)S(1)}, bf16[2,704]{0,1:T(8,128)(2,1)S(1)}, u32[]{:S(2)}, u32[]{:S(2)}) collective-permute-start(bf16[2,704]{0,1:T(8,128)(2,1)S(1)} %slice.37), channel_id=1, source_target_pairs={{0,8},{8,16},{16,24},{24,32},{32,40},{40,48},{48,56},{56,64},{64,7... | collective-permute-start | bytes 8456 | tf_op jit(solution)/shard_map/ppermute | solution.py:263
  146.2 5.8 %collective-permute-done = bf16[2,704]{0,1:T(8,128)(2,1)S(1)} collective-permute-done((bf16[2,704]{0,1:T(8,128)(2,1)S(1)}, bf16[2,704]{0,1:T(8,128)(2,1)S(1)}, u32[]{:S(2)}, u32[]{:S(2)}) %collective-permute-start) | collective-permute-done | bytes 2848 | tf_op jit(solution)/shard_map/ppermute | solution.py:263
  152.1 1.0 maximum_convert_fusion
  153.1 5.6 %convolution_convert_fusion = bf16[128,2048]{1,0:T(8,128)(2,1)} fusion(bf16[704,2048]{1,0:T(8,128)(2,1)S(1)} %copy-done, bf16[128,2048]{1,0:T(8,128)(2,1)S(1)} %bitcast.14, bf16[2048,1408]{1,0:T(8,128)(2,1)} %all-gather.2.cloned.1.call-done, f32[130,704]{0,1:T(8,128)} %maximum_convert_fusion, f32[704]{0:T(1024)S(1)} %get-tuple-element.14, ...), kind=kOutput, calls=%fused_computation.4 | convolution fusion | flops 739631104 | bytes 8167680 | tf_op jit(solution)/shard_map/dot_general | solution.py:269
  158.7 14.5 %all_to_all.33.parts = bf16[8,16,2048]{2,1,0:T(8,128)(2,1)} all-to-all(bf16[8,16,2048]{2,1,0:T(8,128)(2,1)} %bitcast.15), channel_id=1, replica_groups=mesh['z'=8,'y'=8,'x'=4,'core'=2] {'x','core'}, dimensions={0} | all-to-all | bytes 1048576 | tf_op jit(solution)/shard_map/all_to_all | solution.py:185
  173.2 1.8 last.1
  (7 shorter events, 0.0 us)
Async XLA Ops:
  6.5 146.6 %copy-start = (bf16[704,2048]{1,0:T(8,128)(2,1)S(1)}, bf16[704,2048]{1,0:T(8,128)(2,1)}, u32[]{:S(2)}) copy-start(bf16[704,2048]{1,0:T(8,128)(2,1)} %param.27) | copy-start | bytes 8650756
  6.5 133.0 %all-gather.2.cloned.1.call-start = ((), (), s32[]{:S(2)}) async-start(), calls=%async_computation.6 | async-start | bytes 5857280 | tf_op jit(solution)/shard_map/all_gather | solution.py:228
  32.3 28.8 %all-to-all-start.1 = ((bf16[8,512,128]{2,1,0:T(8,128)(2,1)}), bf16[8,512,128]{2,1,0:T(8,128)(2,1)}, u32[]{:S(2)}, u32[]{:S(2)}) async-start(bf16[8,512,128]{2,1,0:T(8,128)(2,1)} %get-tuple-element.10), calls=%async_computation.1 | async-start | bytes 2097152 | tf_op jit(solution)/shard_map/kpool/all_to_all | solution.py:185
  68.0 31.1 %all-to-all-start.2 = ((bf16[8,528,128]{2,1,0:T(8,128)(2,1)}), bf16[8,528,128]{2,1,0:T(8,128)(2,1)}, u32[]{:S(2)}, u32[]{:S(2)}) async-start(bf16[8,528,128]{2,1,0:T(8,128)(2,1)} %attend.1), calls=%async_computation.2 | async-start | bytes 2162688 | tf_op jit(solution)/shard_map/all_to_all | solution.py:185
  123.7 22.5 %copy-start.1 = (f32[3,704]{1,0:T(4,128)S(1)}, f32[3,704]{1,0:T(4,128)}, u32[]{:S(2)}) copy-start(f32[3,704]{1,0:T(4,128)} %param.26) | copy-start | bytes 25348
  144.2 7.8 %collective-permute-start = (bf16[2,704]{0,1:T(8,128)(2,1)S(1)}, bf16[2,704]{0,1:T(8,128)(2,1)S(1)}, u32[]{:S(2)}, u32[]{:S(2)}) collective-permute-start(bf16[2,704]{0,1:T(8,128)(2,1)S(1)} %slice.37), channel_id=1, source_target_pairs={{0,8},{8,16},{16,24},{24,32},{32,40},{40,48},{48,56},{56,64},{64,7... | collective-permute-start | bytes 8456 | tf_op jit(solution)/shard_map/ppermute | solution.py:263
Sparse Core Ops, SparseCore 0:
  10.3 107.4 all-gather.1

commit v2 on v1

--- a/solution.py
+++ b/solution.py
@@ -13,6 +13,9 @@
 SIDE = 8
 BLOCK = 128
 PACK = 4 * BLOCK + 16
+TILES = 5
+MAIN = 128 * TILES
+SENT = 512 + 352
 epsilon = 1e-06
 masked_score = -1e30
 LOG2E = 1.4426950408889634
@@ -32,14 +35,35 @@
     return pl.BlockSpec(memory_space=pltpu.VMEM)
 
 
-def pack_kernel(q1, q2, k1, k2, v, qsend, ksend):
+def pack_kernel(q1, q2, k1, k2, v, lift, gate, qsend, ksend, vv, ll, gg, kk, sems):
+    moves = [
+        pltpu.make_async_copy(src, dst, sems.at[i])
+        for i, (src, dst) in enumerate(
+            (
+                (k1, kk.at[0]),
+                (k2, kk.at[1]),
+                (v, vv),
+                (lift, ll),
+                (gate, gg),
+                (q1, qsend.at[0:128]),
+                (q2, qsend.at[128:256]),
+            )
+        )
+    ]
+    for move in moves:
+        move.start()
+    for move in moves:
+        move.wait()
+    tail = jnp.concatenate([ll[:, MAIN:], gg[:, MAIN:]], axis=1)
     for i in range(SIDE):
-        qsend[i, 0:128, :] = q1[...]
-        qsend[i, 128:256, :] = q2[...]
-        ksend[i, 0:128, :] = k1[...]
-        ksend[i, 128:256, :] = k2[...]
-        ksend[i, 256:384, :] = v[:, 0:128]
-        ksend[i, 384:512, :] = v[:, 128:256]
+        ksend[i, 0:128, :] = kk[0]
+        ksend[i, 128:256, :] = kk[1]
+        ksend[i, 256:384, :] = vv[:, 0:128]
+        ksend[i, 384:512, :] = vv[:, 128:256]
+        for n in range(TILES):
+            ksend[i, 512 + 32 * n : 544 + 32 * n, :] = gg[:, 128 * n : 128 * n + 128]
+            ksend[i, 704 + 32 * n : 736 + 32 * n, :] = ll[:, 128 * n : 128 * n + 128]
+        ksend[i, 672:704, :] = tail
 
 
 def attend_kernel(plan, qpool, kpool, out, scores):
@@ -162,16 +186,84 @@
 
 
 def norm_kernel(parts, residual, gain, stream, normed):
-    total = residual[...].astype(f32)
     att = parts[0].astype(f32)
     for i in range(1, 8):
         att = att + parts[i].astype(f32)
-    total = total + att
+    total = residual[...].astype(f32) + att
     stream[...] = total
     r = lax.rsqrt(jnp.mean(total * total, axis=-1, keepdims=True) + epsilon)
-    n = (total * r * gain[...]).astype(bf16)
-    for i in range(8):
-        normed[i] = n
+    normed[...] = (total * r * gain[...]).astype(bf16)
+
+
+def fetched(core, weights, buffer, sems, first):
+    height = buffer.shape[2]
+    for g in range(SIDE):
+        rows = pl.ds(first, height)
+
+        @pl.when(core == 0)
+        def _():
+            pltpu.make_async_copy(weights.at[:, g, rows, :], buffer.at[g], sems.at[g]).start()
+
+        @pl.when(core != 0)
+        def _():
+            pltpu.make_async_copy(weights.at[g, :, rows, :], buffer.at[g], sems.at[g]).start()
+
+
+def multiplied(rows, weights, buffer, sems, first):
+    height = buffer.shape[2]
+    count = height // 32
+    acc = [None] * ((count + 1) // 2)
+    for g in range(SIDE):
+        pltpu.make_async_copy(
+            weights.at[0, :, pl.ds(first, height), :], buffer.at[g], sems.at[g]
+        ).wait()
+        lhs = rows[:, 256 * g : 256 * g + 256]
+        for n in range(0, count, 2):
+            tiles = [
+                buffer[g, :, 32 * m : 32 * m + 32, :].reshape(256, 128)
+                for m in range(n, min(n + 2, count))
+            ]
+            rhs = jnp.concatenate(tiles, axis=1) if len(tiles) > 1 else tiles[0]
+            d = jnp.dot(lhs, rhs, preferred_element_type=f32)
+            acc[n // 2] = d if acc[n // 2] is None else acc[n // 2] + d
+    return acc
+
+
+def gate_kernel(core, rows, weights, gated, edge, buffer, sems):
+    fetched(core[0], weights, buffer, sems, 0)
+    for n, part in enumerate(multiplied(rows, weights, buffer, sems, 0)):
+        part = part.astype(bf16)
+        gated[:, 256 * n : 256 * n + 256] = part
+        edge[:, 256 * n : 256 * n + 256] = part[112:128]
+
+
+def lift_kernel(core, rows, weights, lifted, buffer, sems):
+    fetched(core[0], weights, buffer, sems, 192)
+    for n, part in enumerate(multiplied(rows, weights, buffer, sems, 192)):
+        lifted[:, 256 * n : 256 * n + part.shape[1]] = part.astype(bf16)
+
+
+def down_kernel(gated, lifted, prior, taps, weight, out):
+    at = lax.broadcasted_iota(jnp.int32, (128, 1), 0)
+
+    def activated(lo, hi):
+        g = gated[:, lo:hi].astype(f32)
+        p = prior[:, lo:hi].astype(f32)
+        one = jnp.where(at == 0, p[15:16], pltpu.roll(g, 1, 0))
+        two = jnp.where(at == 0, p[14:15], jnp.where(at == 1, p[15:16], pltpu.roll(g, 2, 0)))
+        conv = taps[0:1, lo:hi] * two + taps[1:2, lo:hi] * one + taps[2:3, lo:hi] * g
+        return g, conv * jax.nn.sigmoid(conv)
+
+    acc = None
+    for n in range(0, MAIN, 128):
+        _, a = activated(n, n + 128)
+        h = (a * lifted[:, n : n + 128].astype(f32)).astype(bf16)
+        d = jnp.dot(h, weight[n : n + 128, :], preferred_element_type=f32)
+        acc = d if acc is None else acc + d
+    g, a = activated(MAIN, MAIN + 128)
+    h = (pltpu.roll(a, 64, 1) * g).astype(bf16)
+    acc = acc + jnp.dot(h[:, 0:64], weight[MAIN:, :], preferred_element_type=f32)
+    out[...] = acc.astype(bf16)
 
 
 def last_kernel(parts, stream, out):
@@ -183,6 +275,17 @@
 
 def swapped(a, axis, groups=None):
     return lax.all_to_all(a, axis, 0, 0, axis_index_groups=groups, tiled=True)
+
+
+def gathered(a, axis, groups=None):
+    return lax.all_gather(a, axis, axis_index_groups=groups, axis=0, tiled=True)
+
+
+def in_hbm(a):
+    return pltpu.with_memory_space_constraint(a, pltpu.HBM)
+
+
+SMALL = pltpu.CompilerParams(vmem_limit_bytes=20 << 20)
 
 
 def on_device(
@@ -210,28 +313,43 @@
     along_y = jnp.stack([z * SIDE, 1 + 0 * z, y, SIDE + 0 * z, 0 * z, z // 2 + 1])
     along_z = jnp.stack([y, SIDE + 0 * z, z * SIDE, 1 + 0 * z, z // 2, SIDE // 2 + 0 * z])
     plan = jnp.where(core == 0, along_y, along_z).astype(jnp.int32)
+    smem = pl.BlockSpec(memory_space=pltpu.SMEM)
+    hbm = pl.BlockSpec(memory_space=pltpu.HBM)
+    own_core = core.reshape(1).astype(jnp.int32)
     qsend, ksend = pl.pallas_call(
         pack_kernel,
         out_shape=[
-            jax.ShapeDtypeStruct((SIDE, 256, 128), bf16),
-            jax.ShapeDtypeStruct((SIDE, 512, 128), bf16),
-        ],
-        in_specs=[vmem()] * 5,
+            jax.ShapeDtypeStruct((256, 128), bf16),
+            jax.ShapeDtypeStruct((SIDE, SENT, 128), bf16),
+        ],
+        in_specs=[hbm] * 7,
         out_specs=[vmem()] * 2,
+        scratch_shapes=[
+            pltpu.VMEM((128, 256), bf16),
+            pltpu.VMEM((32, 704), bf16),
+            pltpu.VMEM((32, 704), bf16),
+            pltpu.VMEM((2, 128, 128), bf16),
+            pltpu.SemaphoreType.DMA((7,)),
+        ],
+        compiler_params=SMALL,
         name="pack",
-    )(query_one, query_two, key_one, key_two, values)
-    both = jnp.concatenate([lift_weight, gate_weight], axis=1)
-    with jax.named_scope("kpool"):
-        kpool = swapped(ksend, ALL, K_GROUPS)
-    with jax.named_scope("qpool"):
-        qpool = swapped(qsend, ALL, Q_GROUPS)
-    weights = lax.all_gather(both, ("z", "y"), axis=0, tiled=True)
+    )(*(in_hbm(a) for a in (query_one, query_two, key_one, key_two, values, lift_weight, gate_weight)))
+    kpool = swapped(ksend, ALL, K_GROUPS)
+    qpool = gathered(qsend, ALL, Q_GROUPS).reshape(SIDE, 256, 128)
+    part = kpool[:, 512:, :].reshape(SIDE * 352, 128)
+    weights = in_hbm(gathered(part, ALL, Q_GROUPS).reshape(SIDE, SIDE, 352, 128))
     out = pl.pallas_call(
         attend_kernel,
+        grid=(1,),
         out_shape=jax.ShapeDtypeStruct((SIDE, PACK, 128), bf16),
-        in_specs=[pl.BlockSpec(memory_space=pltpu.SMEM), vmem(), vmem()],
+        in_specs=[
+            pl.BlockSpec(memory_space=pltpu.SMEM),
+            vmem(),
+            pl.BlockSpec((SIDE, 512, 128), lambda i: (0, 0, 0)),
+        ],
         out_specs=vmem(),
         scratch_shapes=[pltpu.VMEM((8, 256, 256), f32)],
+        compiler_params=SMALL,
         name="attend",
     )(plan, qpool, kpool)
     back = swapped(out, ALL, Q_GROUPS)
@@ -240,6 +358,7 @@
         out_shape=jax.ShapeDtypeStruct((tokens, width), bf16),
         in_specs=[pl.BlockSpec(memory_space=pltpu.SMEM)] + [vmem()] * 3,
         out_specs=vmem(),
+        compiler_params=SMALL,
         name="join",
     )(mix_weight, back, head_gain.reshape(1, VD), out_weight)
     parts = swapped(attended.reshape(8, own, width), TP)
@@ -247,32 +366,63 @@
         norm_kernel,
         out_shape=[
             jax.ShapeDtypeStruct((own, width), f32),
-            jax.ShapeDtypeStruct((8, own, width), bf16),
+            jax.ShapeDtypeStruct((own, width), bf16),
         ],
         in_specs=[vmem()] * 3,
         out_specs=[vmem()] * 2,
+        compiler_params=SMALL,
         name="norm",
     )(parts, residual, norm_gain.reshape(1, width))
-    rows = swapped(normed, TP).reshape(tokens, width)
-    units = lift_weight.shape[1]
-    lift_pre = jnp.dot(rows, weights[:, :units], preferred_element_type=f32)
-    gate_pre = jnp.dot(rows, weights[:, units:], preferred_element_type=f32)
-    lifted = lift_pre.astype(bf16)
-    gated = gate_pre.astype(bf16)
+    rows = gathered(normed, TP)
+    gated, edge = pl.pallas_call(
+        gate_kernel,
+        out_shape=[
+            jax.ShapeDtypeStruct((tokens, MAIN + 128), bf16),
+            jax.ShapeDtypeStruct((16, MAIN + 128), bf16),
+        ],
+        in_specs=[smem, vmem(), hbm],
+        out_specs=[vmem()] * 2,
+        scratch_shapes=[
+            pltpu.VMEM((SIDE, SIDE, 192, 128), bf16),
+            pltpu.SemaphoreType.DMA((SIDE,)),
+        ],
+        compiler_params=SMALL,
+        name="gate",
+    )(own_core, rows, weights)
     route = [(i, i + 1) for i in range(SIDE * SIDE - 1)]
-    prior = lax.ppermute(gated[tokens - (WIDTH - 1) :], ("z", "y"), route)
-    extended = jnp.concatenate([prior, gated], axis=0).astype(f32)
-    conv = conv_taps[0] * extended[0:tokens]
-    for index in range(1, WIDTH):
-        conv = conv + conv_taps[index] * extended[index : index + tokens]
-    hidden = (jax.nn.silu(conv) * lifted.astype(f32)).astype(bf16)
-    down = jnp.dot(hidden, down_weight, preferred_element_type=f32).astype(bf16)
+    prior = lax.ppermute(edge, ("z", "y"), route)
+    lifted = pl.pallas_call(
+        lift_kernel,
+        out_shape=jax.ShapeDtypeStruct((tokens, MAIN), bf16),
+        in_specs=[smem, vmem(), hbm],
+        out_specs=vmem(),
+        scratch_shapes=[
+            pltpu.VMEM((SIDE, SIDE, 160, 128), bf16),
+            pltpu.SemaphoreType.DMA((SIDE,)),
+        ],
+        compiler_params=SMALL,
+        cost_estimate=pl.CostEstimate(
+            flops=2 * 128 * 2048 * 640, bytes_accessed=3 << 20, transcendentals=0
+        ),
+        name="lift",
+    )(own_core, rows, weights)
+    gap = jnp.zeros((WIDTH, 64), f32)
+    taps = jnp.concatenate([conv_taps[:, :MAIN], gap, conv_taps[:, MAIN:]], axis=1)
+    down = pl.pallas_call(
+        down_kernel,
+        out_shape=jax.ShapeDtypeStruct((tokens, width), bf16),
+        in_specs=[vmem()] * 5,
+        out_specs=vmem(),
+        compiler_params=SMALL,
+        name="down",
+    )(gated, lifted, prior, taps, down_weight)
     mixer = swapped(down.reshape(8, own, width), TP)
     return pl.pallas_call(
         last_kernel,
         out_shape=jax.ShapeDtypeStruct((own, width), bf16),
         in_specs=[vmem()] * 2,
         out_specs=vmem(),
+        compiler_params=SMALL,
         name="last",
     )(mixer, stream)
 
@@ -280,6 +430,7 @@
 def solution(mesh):
     fine = Mesh(mesh.devices.reshape(SIDE, SIDE, 4, 2), ("z", "y", "x", "core"))
     sp = ("z", "y")
+
     return jax.shard_map(
         on_device,
         mesh=fine,

time: 183 us -> 164 us (0.90)
  the two profiles are of different devices: /device:TPU:8 before, /device:TPU:128 now
where the time goes in v2:
time: 164 us
  blocking collectives  86.3 us (53%)
  waiting for transfers between devices  31.4 us (19%)
  Pallas kernels  18.1 us (11%)
  between operations  14.2 us (9%)
  starting transfers between devices  12.7 us (8%)
    all_to_all x2, blocking collectives, swapped(): return lax.all_to_all(a, axis, 0, 0, axis_index_groups=groups, tiled=True)  45.7 us
    all_gather x2, blocking collectives, gathered(): return lax.all_gather(a, axis, axis_index_groups=groups, axis=0, tiled=True)  40.6 us
    all_to_all x2, waiting for transfers between devices, swapped(): return lax.all_to_all(a, axis, 0, 0, axis_index_groups=groups, tiled=True)  28.8 us
    all_to_all x2, starting transfers between devices, swapped(): return lax.all_to_all(a, axis, 0, 0, axis_index_groups=groups, tiled=True)  9.95 us
    pallas_call x1, Pallas kernels, on_device(): pl.pallas_call(attend_kernel, grid=(1,), out_shape=jax.ShapeDtypeStruct((...  8.27 us
  transfers between devices with their start and end apart: 4, of which 3 were waited for; matrix products, arithmetic and copies ran while one was open for 0% of the time, Pallas kernels for 8%

profile of v2, /device:TPU:128, one launch (start us, length us, event | category | flops | bytes accessed | tf_op | source)
XLA Modules:
  0.0 163.9 jit_solution(14111381455615091800)
XLA Ops:
  6.5 1.2 pack.1
  7.7 32.8 %all_to_all.20.kpool = bf16[8,864,128]{2,1,0:T(8,128)(2,1)S(1)} all-to-all(bf16[8,864,128]{2,1,0:T(8,128)(2,1)S(1)} %get-tuple-element.12), channel_id=1, replica_groups={{0,64,128,192,256,320,384,448},{2,66,130,194,258,322,386,450},{4,68,132..., dimensions={0} | all-to-all | bytes 3538944 | tf_op jit(solution)/shard_map/all_to_all | solution.py:277
  40.5 0.9 slice.12
  41.4 0.0 all-gather.2.cloned.1.call-update
  41.5 0.1 stack.25
  41.6 0.1 stack.23
  41.6 27.5 %all_gather.9 = bf16[2048,128]{1,0:T(8,128)(2,1)S(1)} all-gather(bf16[256,128]{1,0:T(8,128)(2,1)S(1)} %get-tuple-element.11), channel_id=1, replica_groups={{0,8,16,24,32,40,48,56},{2,10,18,26,34,42,50,58},{4,12,20,28,36,44,52,6..., dimensions={0}, use_global_device_ids=true | all-gather | bytes 589824 | tf_op jit(solution)/shard_map/all_gather | solution.py:281
  69.2 8.3 %attend.1 = bf16[8,528,128]{2,1,0:T(8,128)(2,1)} custom-call(s32[6]{0:T(128)S(1)} %broadcast_select_fusion.plan, bf16[8,256,128]{2,1,0:T(8,128)(2,1)S(1)} %bitcast.13, bf16[8,864,128]{2,1,0:T(8,128)(2,1)S(1)} %all_to_all.20.kpool), custom_call_target="tpu_custom_call" | custom-call | tf_op jit(solution)/shard_map/attend/pallas_call | solution.py:341
  77.4 5.6 %all-to-all-start.1 = ((bf16[8,528,128]{2,1,0:T(8,128)(2,1)}), bf16[8,528,128]{2,1,0:T(8,128)(2,1)S(1)}, u32[]{:S(2)}, u32[]{:S(2)}) async-start(bf16[8,528,128]{2,1,0:T(8,128)(2,1)} %attend.1), calls=%async_computation.1 | async-start | bytes 2162688 | tf_op jit(solution)/shard_map/all_to_all | solution.py:277
  83.7 18.6 %all-to-all-done.1.parts = bf16[8,528,128]{2,1,0:T(8,128)(2,1)S(1)} async-done(((bf16[8,528,128]{2,1,0:T(8,128)(2,1)}), bf16[8,528,128]{2,1,0:T(8,128)(2,1)S(1)}, u32[]{:S(2)}, u32[]{:S(2)}) %all-to-all-start.1) | async-done | bytes 1081376 | tf_op jit(solution)/shard_map/all_to_all | solution.py:277
  102.3 0.0 copy-start.2
  102.3 1.8 %join.1 = bf16[128,2048]{1,0:T(8,128)(2,1)} custom-call(f32[1]{0:T(128)S(6)} %copy.15.mix, bf16[8,528,128]{2,1,0:T(8,128)(2,1)S(1)} %all-to-all-done.1.parts, f32[1,256]{1,0:T(1,128)S(1)} %bitcast.15, bf16[256,2048]{1,0:T(8,128)(2,1)S(1)} %copy-done.1), custom_call_target="tpu_custom_call" | custom-call | tf_op jit(solution)/shard_map/join/pallas_call | solution.py:356
  104.1 4.4 %all-to-all-start.2 = ((bf16[8,16,2048]{2,1,0:T(8,128)(2,1)}), bf16[8,16,2048]{2,1,0:T(8,128)(2,1)S(1)}, u32[]{:S(2)}, u32[]{:S(2)}) async-start(bf16[8,16,2048]{2,1,0:T(8,128)(2,1)} %bitcast.7), calls=%async_computation.2 | async-start | bytes 1048576 | tf_op jit(solution)/shard_map/all_to_all | solution.py:277
  108.5 0.1 pad_maximum_fusion.taps
  108.6 10.2 %all-to-all-done.2.parts = bf16[8,16,2048]{2,1,0:T(8,128)(2,1)S(1)} async-done(((bf16[8,16,2048]{2,1,0:T(8,128)(2,1)}), bf16[8,16,2048]{2,1,0:T(8,128)(2,1)S(1)}, u32[]{:S(2)}, u32[]{:S(2)}) %all-to-all-start.2) | async-done | bytes 524320 | tf_op jit(solution)/shard_map/all_to_all | solution.py:277
  118.8 0.2 norm.1
  119.0 13.1 %all_gather.10.rows = bf16[128,2048]{1,0:T(8,128)(2,1)S(1)} all-gather(bf16[16,2048]{1,0:T(8,128)(2,1)S(1)} %get-tuple-element.13), channel_id=1, replica_groups=mesh['z'=8,'y'=8,'x'=4,'core'=2] {'x','core'}, dimensions={0}, use_global_device_ids=true | all-gather | bytes 589824 | tf_op jit(solution)/shard_map/all_gather | solution.py:281
  132.1 2.3 %gate.3 = (bf16[128,768]{1,0:T(8,128)(2,1)S(1)}, bf16[16,768]{1,0:T(8,128)(2,1)S(1)}) custom-call(s32[1]{0:T(128)} %bitcast.core, bf16[128,2048]{1,0:T(8,128)(2,1)S(1)} %all_gather.10.rows, bf16[8,8,352,128]{3,2,1,0:T(8,128)(2,1)} %bitcast.16), custom_call_target="tpu_custom_call" | custom-call | tf_op jit(solution)/shard_map/gate/pallas_call | solution.py:377
  134.4 2.8 %collective-permute-start = (bf16[16,768]{1,0:T(8,128)(2,1)S(1)}, bf16[16,768]{1,0:T(8,128)(2,1)S(1)}, u32[]{:S(2)}, u32[]{:S(2)}) collective-permute-start(bf16[16,768]{1,0:T(8,128)(2,1)S(1)} %get-tuple-element.15), channel_id=1, source_target_pairs={{0,8},{8,16},{16,24},{24,32},{32,40},{40,48},{48,56},{56,64},{64,7... | collective-permute-start | bytes 73736 | tf_op jit(solution)/shard_map/ppermute | solution.py:393
  137.2 2.8 %lift.3.lifted = bf16[128,640]{1,0:T(8,128)(2,1)S(1)} custom-call(s32[1]{0:T(128)} %bitcast.core, bf16[128,2048]{1,0:T(8,128)(2,1)S(1)} %all_gather.10.rows, bf16[8,8,352,128]{3,2,1,0:T(8,128)(2,1)} %bitcast.17), custom_call_target="tpu_custom_call" | custom-call | flops 335544320 | bytes 3145728 | tf_op jit(solution)/shard_map/lift/pallas_call | solution.py:394
  140.0 2.5 %collective-permute-done.prior = bf16[16,768]{1,0:T(8,128)(2,1)S(1)} collective-permute-done((bf16[16,768]{1,0:T(8,128)(2,1)S(1)}, bf16[16,768]{1,0:T(8,128)(2,1)S(1)}, u32[]{:S(2)}, u32[]{:S(2)}) %collective-permute-start) | collective-permute-done | bytes 24608 | tf_op jit(solution)/shard_map/ppermute | solution.py:393
  142.5 1.0 down.1
  143.5 12.9 %all_to_all.21.parts = bf16[8,16,2048]{2,1,0:T(8,128)(2,1)S(1)} all-to-all(bf16[8,16,2048]{2,1,0:T(8,128)(2,1)S(1)} %bitcast.12), channel_id=1, replica_groups=mesh['z'=8,'y'=8,'x'=4,'core'=2] {'x','core'}, dimensions={0} | all-to-all | bytes 1048576 | tf_op jit(solution)/shard_map/all_to_all | solution.py:277
  156.4 0.7 last.1
  (18 shorter events, 0.0 us)
Async XLA Ops:
  6.5 125.6 %all-gather.2.cloned.1.call-start = ((), (), s32[]{:S(2)}) async-start(), calls=%async_computation.4 | async-start | bytes 6488064 | tf_op jit(solution)/shard_map/all_gather | solution.py:281
  77.4 24.9 %copy-start.1 = (bf16[256,2048]{1,0:T(8,128)(2,1)S(1)}, bf16[256,2048]{1,0:T(8,128)(2,1)}, u32[]{:S(2)}) copy-start(bf16[256,2048]{1,0:T(8,128)(2,1)} %weight.2) | copy-start | bytes 3145732
  77.4 24.9 %copy-start.4 = (f32[256]{0:T(256)S(1)}, f32[256]{0:T(256)}, u32[]{:S(2)}) copy-start(f32[256]{0:T(256)} %param.20) | copy-start | bytes 3076
  77.4 24.9 %all-to-all-start.1 = ((bf16[8,528,128]{2,1,0:T(8,128)(2,1)}), bf16[8,528,128]{2,1,0:T(8,128)(2,1)S(1)}, u32[]{:S(2)}, u32[]{:S(2)}) async-start(bf16[8,528,128]{2,1,0:T(8,128)(2,1)} %attend.1), calls=%async_computation.1 | async-start | bytes 2162688 | tf_op jit(solution)/shard_map/all_to_all | solution.py:277
  102.3 6.2 %slice-start = ((f32[3,704]{1,0:T(4,128)}), f32[3,640]{1,0:T(4,128)S(1)}, s32[]{:S(2)}) async-start(f32[3,704]{1,0:T(4,128)} %param.26), calls=%async_computation.5 | async-start | bytes 20480 | tf_op jit(solution)/shard_map/slice | solution.py:410
  102.3 6.2 %slice-start.1 = ((f32[3,704]{1,0:T(4,128)}), f32[3,64]{1,0:T(4,128)S(1)}, s32[]{:S(2)}) async-start(f32[3,704]{1,0:T(4,128)} %param.26), calls=%async_computation.6 | async-start | bytes 4096 | tf_op jit(solution)/shard_map/slice | solution.py:410
  102.3 16.5 %copy-start.2 = (bf16[16,2048]{1,0:T(8,128)(2,1)S(1)}, bf16[16,2048]{1,0:T(8,128)(2,1)}, u32[]{:S(2)}) copy-start(bf16[16,2048]{1,0:T(8,128)(2,1)} %residual.1) | copy-start | bytes 196612
  102.3 16.5 %copy-start.3 = (f32[2048]{0:T(1024)S(1)}, f32[2048]{0:T(1024)}, u32[]{:S(2)}) copy-start(f32[2048]{0:T(1024)} %param.23) | copy-start | bytes 24580
  104.1 14.7 %all-to-all-start.2 = ((bf16[8,16,2048]{2,1,0:T(8,128)(2,1)}), bf16[8,16,2048]{2,1,0:T(8,128)(2,1)S(1)}, u32[]{:S(2)}, u32[]{:S(2)}) async-start(bf16[8,16,2048]{2,1,0:T(8,128)(2,1)} %bitcast.7), calls=%async_computation.2 | async-start | bytes 1048576 | tf_op jit(solution)/shard_map/all_to_all | solution.py:277
  134.4 8.1 %copy-start = (bf16[704,2048]{1,0:T(8,128)(2,1)S(1)}, bf16[704,2048]{1,0:T(8,128)(2,1)}, u32[]{:S(2)}) copy-start(bf16[704,2048]{1,0:T(8,128)(2,1)} %weight.3) | copy-start | bytes 8650756
  134.4 8.1 %collective-permute-start = (bf16[16,768]{1,0:T(8,128)(2,1)S(1)}, bf16[16,768]{1,0:T(8,128)(2,1)S(1)}, u32[]{:S(2)}, u32[]{:S(2)}) collective-permute-start(bf16[16,768]{1,0:T(8,128)(2,1)S(1)} %get-tuple-element.15), channel_id=1, source_target_pairs={{0,8},{8,16},{16,24},{24,32},{32,40},{40,48},{48,56},{56,64},{64,7... | collective-permute-start | bytes 73736 | tf_op jit(solution)/shard_map/ppermute | solution.py:393
Sparse Core Ops, SparseCore 0:
  41.6 48.0 all-gather.1

commit v3 on v2

--- a/solution.py
+++ b/solution.py
@@ -16,6 +16,7 @@
 TILES = 5
 MAIN = 128 * TILES
 SENT = 512 + 352
+SHIFTS = (0, 1, -1, 2, -2, 3, -3, 4)
 epsilon = 1e-06
 masked_score = -1e30
 LOG2E = 1.4426950408889634
@@ -29,6 +30,16 @@
 COLS = [[PLACES[:, i, x, c].tolist() for i in range(SIDE) for x in range(4)] for c in range(2)]
 Q_GROUPS = ROWS[0] + COLS[1]
 K_GROUPS = COLS[0] + ROWS[1]
+
+
+def steps(by):
+    moved = np.stack(
+        [np.roll(PLACES, -by, axis=1)[..., 0], np.roll(PLACES, -by, axis=0)[..., 1]], axis=-1
+    )
+    return list(zip(PLACES.reshape(-1).tolist(), moved.reshape(-1).tolist()))
+
+
+UP, DOWN = steps(1), steps(-1)
 
 
 def vmem():
@@ -192,31 +203,36 @@
     total = residual[...].astype(f32) + att
     stream[...] = total
     r = lax.rsqrt(jnp.mean(total * total, axis=-1, keepdims=True) + epsilon)
-    normed[...] = (total * r * gain[...]).astype(bf16)
-
-
-def fetched(core, weights, buffer, sems, first):
+    n = (total * r * gain[...]).astype(bf16)
+    for i in range(8):
+        normed[i] = n
+
+
+def fetched(place, pieces, buffer, sems, first):
     height = buffer.shape[2]
-    for g in range(SIDE):
-        rows = pl.ds(first, height)
+    core, me = place[0], place[1]
+    rows = pl.ds(first, height)
+    for n, (piece, shift) in enumerate(zip(pieces, SHIFTS)):
+        at = lax.rem(me + SIDE - shift, SIDE)
 
         @pl.when(core == 0)
         def _():
-            pltpu.make_async_copy(weights.at[:, g, rows, :], buffer.at[g], sems.at[g]).start()
+            pltpu.make_async_copy(piece.at[:, rows, :], buffer.at[:, at], sems.at[n]).start()
 
         @pl.when(core != 0)
         def _():
-            pltpu.make_async_copy(weights.at[g, :, rows, :], buffer.at[g], sems.at[g]).start()
-
-
-def multiplied(rows, weights, buffer, sems, first):
+            pltpu.make_async_copy(piece.at[:, rows, :], buffer.at[at], sems.at[n]).start()
+
+
+def multiplied(rows, pieces, buffer, sems, first):
     height = buffer.shape[2]
     count = height // 32
     acc = [None] * ((count + 1) // 2)
+    for n in range(SIDE):
+        pltpu.make_async_copy(
+            pieces[0].at[:, pl.ds(first, height), :], buffer.at[n], sems.at[n]
+        ).wait()
     for g in range(SIDE):
-        pltpu.make_async_copy(
-            weights.at[0, :, pl.ds(first, height), :], buffer.at[g], sems.at[g]
-        ).wait()
         lhs = rows[:, 256 * g : 256 * g + 256]
         for n in range(0, count, 2):
             tiles = [
@@ -229,17 +245,19 @@
     return acc
 
 
-def gate_kernel(core, rows, weights, gated, edge, buffer, sems):
-    fetched(core[0], weights, buffer, sems, 0)
-    for n, part in enumerate(multiplied(rows, weights, buffer, sems, 0)):
+def gate_kernel(place, rows, *refs):
+    pieces, (gated, edge, buffer, sems) = refs[:SIDE], refs[SIDE:]
+    fetched(place, pieces, buffer, sems, 0)
+    for n, part in enumerate(multiplied(rows, pieces, buffer, sems, 0)):
         part = part.astype(bf16)
         gated[:, 256 * n : 256 * n + 256] = part
         edge[:, 256 * n : 256 * n + 256] = part[112:128]
 
 
-def lift_kernel(core, rows, weights, lifted, buffer, sems):
-    fetched(core[0], weights, buffer, sems, 192)
-    for n, part in enumerate(multiplied(rows, weights, buffer, sems, 192)):
+def lift_kernel(place, rows, *refs):
+    pieces, (lifted, buffer, sems) = refs[:SIDE], refs[SIDE:]
+    fetched(place, pieces, buffer, sems, 192)
+    for n, part in enumerate(multiplied(rows, pieces, buffer, sems, 192)):
         lifted[:, 256 * n : 256 * n + part.shape[1]] = part.astype(bf16)
 
 
@@ -315,7 +333,7 @@
     plan = jnp.where(core == 0, along_y, along_z).astype(jnp.int32)
     smem = pl.BlockSpec(memory_space=pltpu.SMEM)
     hbm = pl.BlockSpec(memory_space=pltpu.HBM)
-    own_core = core.reshape(1).astype(jnp.int32)
+    place = jnp.stack([core, jnp.where(core == 0, y, z)]).astype(jnp.int32)
     qsend, ksend = pl.pallas_call(
         pack_kernel,
         out_shape=[
@@ -336,12 +354,10 @@
     )(*(in_hbm(a) for a in (query_one, query_two, key_one, key_two, values, lift_weight, gate_weight)))
     kpool = swapped(ksend, ALL, K_GROUPS)
     qpool = gathered(qsend, ALL, Q_GROUPS).reshape(SIDE, 256, 128)
-    part = kpool[:, 512:, :].reshape(SIDE * 352, 128)
-    weights = in_hbm(gathered(part, ALL, Q_GROUPS).reshape(SIDE, SIDE, 352, 128))
     out = pl.pallas_call(
         attend_kernel,
         grid=(1,),
-        out_shape=jax.ShapeDtypeStruct((SIDE, PACK, 128), bf16),
+        out_shape=pltpu.HBM((SIDE, PACK, 128), bf16),
         in_specs=[
             pl.BlockSpec(memory_space=pltpu.SMEM),
             vmem(),
@@ -352,7 +368,11 @@
         compiler_params=SMALL,
         name="attend",
     )(plan, qpool, kpool)
+    kpool, out = lax.optimization_barrier((kpool, out))
     back = swapped(out, ALL, Q_GROUPS)
+    piece = kpool[:, 512:, :].reshape(SIDE * 352, 128)
+    above, below = lax.ppermute(piece, ALL, UP), lax.ppermute(piece, ALL, DOWN)
+    above_two, below_two = lax.ppermute(above, ALL, UP), lax.ppermute(below, ALL, DOWN)
     attended = pl.pallas_call(
         join_kernel,
         out_shape=jax.ShapeDtypeStruct((tokens, width), bf16),
@@ -361,26 +381,33 @@
         compiler_params=SMALL,
         name="join",
     )(mix_weight, back, head_gain.reshape(1, VD), out_weight)
+    attended, above_two, below_two = lax.optimization_barrier((attended, above_two, below_two))
     parts = swapped(attended.reshape(8, own, width), TP)
+    above_three = lax.ppermute(above_two, ALL, UP)
+    below_three = lax.ppermute(below_two, ALL, DOWN)
     stream, normed = pl.pallas_call(
         norm_kernel,
         out_shape=[
             jax.ShapeDtypeStruct((own, width), f32),
-            jax.ShapeDtypeStruct((own, width), bf16),
+            jax.ShapeDtypeStruct((8, own, width), bf16),
         ],
         in_specs=[vmem()] * 3,
         out_specs=[vmem()] * 2,
         compiler_params=SMALL,
         name="norm",
     )(parts, residual, norm_gain.reshape(1, width))
-    rows = gathered(normed, TP)
+    normed, above_three = lax.optimization_barrier((normed, above_three))
+    rows = swapped(normed, TP).reshape(tokens, width)
+    above_four = lax.ppermute(above_three, ALL, UP)
+    pieces = [piece, above, below, above_two, below_two, above_three, below_three, above_four]
+    pieces = [p.reshape(SIDE, 352, 128) for p in pieces]
     gated, edge = pl.pallas_call(
         gate_kernel,
         out_shape=[
             jax.ShapeDtypeStruct((tokens, MAIN + 128), bf16),
             jax.ShapeDtypeStruct((16, MAIN + 128), bf16),
         ],
-        in_specs=[smem, vmem(), hbm],
+        in_specs=[smem, vmem()] + [pl.BlockSpec(memory_space=pl.ANY)] * SIDE,
         out_specs=[vmem()] * 2,
         scratch_shapes=[
             pltpu.VMEM((SIDE, SIDE, 192, 128), bf16),
@@ -388,13 +415,13 @@
         ],
         compiler_params=SMALL,
         name="gate",
-    )(own_core, rows, weights)
+    )(place, rows, *pieces)
     route = [(i, i + 1) for i in range(SIDE * SIDE - 1)]
     prior = lax.ppermute(edge, ("z", "y"), route)
     lifted = pl.pallas_call(
         lift_kernel,
         out_shape=jax.ShapeDtypeStruct((tokens, MAIN), bf16),
-        in_specs=[smem, vmem(), hbm],
+        in_specs=[smem, vmem()] + [pl.BlockSpec(memory_space=pl.ANY)] * SIDE,
         out_specs=vmem(),
         scratch_shapes=[
             pltpu.VMEM((SIDE, SIDE, 160, 128), bf16),
@@ -405,7 +432,7 @@
             flops=2 * 128 * 2048 * 640, bytes_accessed=3 << 20, transcendentals=0
         ),
         name="lift",
-    )(own_core, rows, weights)
+    )(place, rows, *pieces)
     gap = jnp.zeros((WIDTH, 64), f32)
     taps = jnp.concatenate([conv_taps[:, :MAIN], gap, conv_taps[:, MAIN:]], axis=1)
     down = pl.pallas_call(

time: 164 us -> 165 us (level)
  the two profiles are of different devices: /device:TPU:128 before, /device:TPU:384 now
where the time goes in v3:
time: 165 us; the launch traced here: 164 us
  starting transfers between devices  50.7 us (31%)
  blocking collectives  49.2 us (30%)
  waiting for transfers between devices  35.6 us (22%)
  Pallas kernels  26.4 us (16%)
    all_gather x1, blocking collectives, gathered(): return lax.all_gather(a, axis, axis_index_groups=groups, axis=0, tiled=True)  36.4 us
    all_to_all x4, starting transfers between devices, swapped(): return lax.all_to_all(a, axis, 0, 0, axis_index_groups=groups, tiled=True)  19.4 us
    ppermute x1, waiting for transfers between devices, on_device(): lax.ppermute(piece, ALL, UP)  17.2 us
    all_to_all x4, waiting for transfers between devices, swapped(): return lax.all_to_all(a, axis, 0, 0, axis_index_groups=groups, tiled=True)  14.7 us
    all_to_all x1, blocking collectives, swapped(): return lax.all_to_all(a, axis, 0, 0, axis_index_groups=groups, tiled=True)  12.8 us
    pallas_call x1, Pallas kernels, on_device(): pl.pallas_call(attend_kernel, grid=(1,), out_shape=pltpu.HBM((SIDE, PACK,...  12.7 us
    ppermute x1, starting transfers between devices, on_device(): below_three = lax.ppermute(below_two, ALL, DOWN)  5.69 us
    ppermute x1, starting transfers between devices, on_device(): prior = lax.ppermute(edge, ('z', 'y'), route)  5.4 us
  transfers between devices with their start and end apart: 12, of which 5 were waited for; matrix products, arithmetic and copies ran while one was open for 0% of the time, Pallas kernels for 4%

profile of v3, /device:TPU:384, one launch (start us, length us, event | category | flops | bytes accessed | tf_op | source)
XLA Modules:
  0.0 164.4 jit_solution(6533813824084500074)
XLA Ops:
  0.0 2.4 %pack.1 = (bf16[256,128]{1,0:T(8,128)(2,1)S(1)}, bf16[8,864,128]{2,1,0:T(8,128)(2,1)}) custom-call(bf16[128,128]{1,0:T(8,128)(2,1)} %q1.1, bf16[128,128]{1,0:T(8,128)(2,1)} %q2.1, bf16[128,128]{1,0:T(8,128)(2,1)} %k1.1, bf16[128,128]{1,0:T(8,128)(2,1)} %k2.1, bf16[128,256]{1,0:T(8,128)(2,1)} %v.1, bf16[32,704]{1,0:T(8,128)(2,1)} %lift.2, bf16[32,704]{1,0:T(8,128)(2,1)} %gate.2), custom_call_target="tpu_custom_call" | custom-call | tf_op jit(solution)/shard_map/pack/pallas_call | solution.py:337
  2.4 5.4 %all-to-all-start = ((bf16[8,864,128]{2,1,0:T(8,128)(2,1)}), bf16[8,864,128]{2,1,0:T(8,128)(2,1)S(1)}, u32[]{:S(2)}, u32[]{:S(2)}) async-start(bf16[8,864,128]{2,1,0:T(8,128)(2,1)} %get-tuple-element.18), calls=%async_computation | async-start | bytes 3538944 | tf_op jit(solution)/shard_map/all_to_all | solution.py:295
  8.1 36.4 %all_gather.3 = bf16[2048,128]{1,0:T(8,128)(2,1)S(1)} all-gather(bf16[256,128]{1,0:T(8,128)(2,1)S(1)} %get-tuple-element.19), channel_id=1, replica_groups={{0,8,16,24,32,40,48,56},{2,10,18,26,34,42,50,58},{4,12,20,28,36,44,52,6..., dimensions={0}, use_global_device_ids=true | all-gather | bytes 589824 | tf_op jit(solution)/shard_map/all_gather | solution.py:299
  44.5 12.7 %attend.1 = bf16[8,528,128]{2,1,0:T(8,128)(2,1)} custom-call(s32[6]{0:T(128)S(1)} %broadcast_select_fusion.plan, bf16[8,256,128]{2,1,0:T(8,128)(2,1)S(1)} %bitcast.28, bf16[8,864,128]{2,1,0:T(8,128)(2,1)S(1)} %all-to-all-done.kpool), custom_call_target="tpu_custom_call" | custom-call | tf_op jit(solution)/shard_map/attend/pallas_call | solution.py:357
  57.2 6.2 %all-to-all-start.1 = ((bf16[8,528,128]{2,1,0:T(8,128)(2,1)}), bf16[8,528,128]{2,1,0:T(8,128)(2,1)}, u32[]{:S(2)}, u32[]{:S(2)}) async-start(bf16[8,528,128]{2,1,0:T(8,128)(2,1)} %attend.1), calls=%async_computation.1 | async-start | bytes 2162688 | tf_op jit(solution)/shard_map/all_to_all | solution.py:295
  63.4 3.9 %collective-permute-start = (bf16[2816,128]{1,0:T(8,128)(2,1)S(1)}, bf16[2816,128]{1,0:T(8,128)(2,1)S(1)}, u32[]{:S(2)}, u32[]{:S(2)}) collective-permute-start(bf16[2816,128]{1,0:T(8,128)(2,1)S(1)} %bitcast.20), channel_id=1, source_target_pairs={{0,8},{1,65},{2,10},{3,67},{4,12},{5,69},{6,14},{7,71},{8,16},{9,7... | collective-permute-start | bytes 2162696 | tf_op jit(solution)/shard_map/ppermute | solution.py:374
  67.3 3.1 %collective-permute-start.2 = (bf16[2816,128]{1,0:T(8,128)(2,1)S(1)}, bf16[2816,128]{1,0:T(8,128)(2,1)S(1)}, u32[]{:S(2)}, u32[]{:S(2)}) collective-permute-start(bf16[2816,128]{1,0:T(8,128)(2,1)S(1)} %bitcast.21), channel_id=1, source_target_pairs={{0,56},{1,449},{2,58},{3,451},{4,60},{5,453},{6,62},{7,455},{8,0},... | collective-permute-start | bytes 2162696 | tf_op jit(solution)/shard_map/ppermute | solution.py:374
  70.5 17.2 %collective-permute-done = bf16[2816,128]{1,0:T(8,128)(2,1)S(1)} collective-permute-done((bf16[2816,128]{1,0:T(8,128)(2,1)S(1)}, bf16[2816,128]{1,0:T(8,128)(2,1)S(1)}, u32[]{:S(2)}, u32[]{:S(2)}) %collective-permute-start) | collective-permute-done | bytes 720928 | tf_op jit(solution)/shard_map/ppermute | solution.py:374
  87.6 1.9 %collective-permute-start.1 = (bf16[2816,128]{1,0:T(8,128)(2,1)S(1)}, bf16[2816,128]{1,0:T(8,128)(2,1)}, u32[]{:S(2)}, u32[]{:S(2)}) collective-permute-start(bf16[2816,128]{1,0:T(8,128)(2,1)S(1)} %collective-permute-done), channel_id=1, source_target_pairs={{0,8},{1,65},{2,10},{3,67},{4,12},{5,69},{6,14},{7,71},{8,16},{9,7... | collective-permute-start | bytes 2162696 | tf_op jit(solution)/shard_map/ppermute | solution.py:375
  89.6 5.1 %collective-permute-start.3 = (bf16[2816,128]{1,0:T(8,128)(2,1)S(1)}, bf16[2816,128]{1,0:T(8,128)(2,1)}, u32[]{:S(2)}, u32[]{:S(2)}) collective-permute-start(bf16[2816,128]{1,0:T(8,128)(2,1)S(1)} %collective-permute-done.2), channel_id=1, source_target_pairs={{0,56},{1,449},{2,58},{3,451},{4,60},{5,453},{6,62},{7,455},{8,0},... | collective-permute-start | bytes 2162696 | tf_op jit(solution)/shard_map/ppermute | solution.py:375
  96.6 3.1 %join.1 = bf16[128,2048]{1,0:T(8,128)(2,1)} custom-call(f32[1]{0:T(128)S(6)} %copy.15.mix, bf16[8,528,128]{2,1,0:T(8,128)(2,1)} %all-to-all-done.1.parts, f32[1,256]{1,0:T(1,128)S(1)} %bitcast.31, bf16[256,2048]{1,0:T(8,128)(2,1)S(1)} %copy-done.1), custom_call_target="tpu_custom_call" | custom-call | tf_op jit(solution)/shard_map/join/pallas_call | solution.py:376
  99.7 2.4 %collective-permute-done.1 = bf16[2816,128]{1,0:T(8,128)(2,1)} collective-permute-done((bf16[2816,128]{1,0:T(8,128)(2,1)S(1)}, bf16[2816,128]{1,0:T(8,128)(2,1)}, u32[]{:S(2)}, u32[]{:S(2)}) %collective-permute-start.1) | collective-permute-done | bytes 720928 | tf_op jit(solution)/shard_map/ppermute | solution.py:375
  102.1 1.4 collective-permute-done.3
  103.5 1.9 %collective-permute-start.4 = (bf16[2816,128]{1,0:T(8,128)(2,1)}, bf16[2816,128]{1,0:T(8,128)(2,1)}, u32[]{:S(2)}, u32[]{:S(2)}) collective-permute-start(bf16[2816,128]{1,0:T(8,128)(2,1)} %collective-permute-done.1), channel_id=1, source_target_pairs={{0,8},{1,65},{2,10},{3,67},{4,12},{5,69},{6,14},{7,71},{8,16},{9,7... | collective-permute-start | bytes 2162696 | tf_op jit(solution)/shard_map/ppermute | solution.py:386
  105.4 4.3 %all-to-all-start.2 = ((bf16[8,16,2048]{2,1,0:T(8,128)(2,1)}), bf16[8,16,2048]{2,1,0:T(8,128)(2,1)S(1)}, u32[]{:S(2)}, u32[]{:S(2)}) async-start(bf16[8,16,2048]{2,1,0:T(8,128)(2,1)} %bitcast.9), calls=%async_computation.2 | async-start | bytes 1048576 | tf_op jit(solution)/shard_map/all_to_all | solution.py:295
  109.7 5.7 %collective-permute-start.5 = (bf16[2816,128]{1,0:T(8,128)(2,1)}, bf16[2816,128]{1,0:T(8,128)(2,1)}, u32[]{:S(2)}, u32[]{:S(2)}) collective-permute-start(bf16[2816,128]{1,0:T(8,128)(2,1)} %collective-permute-done.3), channel_id=1, source_target_pairs={{0,56},{1,449},{2,58},{3,451},{4,60},{5,453},{6,62},{7,455},{8,0},... | collective-permute-start | bytes 2162696 | tf_op jit(solution)/shard_map/ppermute | solution.py:387
  115.4 4.6 %all-to-all-done.2.parts = bf16[8,16,2048]{2,1,0:T(8,128)(2,1)S(1)} async-done(((bf16[8,16,2048]{2,1,0:T(8,128)(2,1)}), bf16[8,16,2048]{2,1,0:T(8,128)(2,1)S(1)}, u32[]{:S(2)}, u32[]{:S(2)}) %all-to-all-start.2) | async-done | bytes 524320 | tf_op jit(solution)/shard_map/all_to_all | solution.py:295
  121.0 4.2 %collective-permute-start.6 = (bf16[2816,128]{1,0:T(8,128)(2,1)}, bf16[2816,128]{1,0:T(8,128)(2,1)}, u32[]{:S(2)}, u32[]{:S(2)}) collective-permute-start(bf16[2816,128]{1,0:T(8,128)(2,1)} %collective-permute-done.4), channel_id=1, source_target_pairs={{0,8},{1,65},{2,10},{3,67},{4,12},{5,69},{6,14},{7,71},{8,16},{9,7... | collective-permute-start | bytes 2162696 | tf_op jit(solution)/shard_map/ppermute | solution.py:401
  125.2 3.5 %all-to-all-start.3 = ((bf16[8,16,2048]{2,1,0:T(8,128)(2,1)}), bf16[8,16,2048]{2,1,0:T(8,128)(2,1)S(1)}, u32[]{:S(2)}, u32[]{:S(2)}) async-start(bf16[8,16,2048]{2,1,0:T(8,128)(2,1)} %get-tuple-element.25), calls=%async_computation.3 | async-start | bytes 1048576 | tf_op jit(solution)/shard_map/all_to_all | solution.py:295
  128.9 10.0 %all-to-all-done.3 = bf16[8,16,2048]{2,1,0:T(8,128)(2,1)S(1)} async-done(((bf16[8,16,2048]{2,1,0:T(8,128)(2,1)}), bf16[8,16,2048]{2,1,0:T(8,128)(2,1)S(1)}, u32[]{:S(2)}, u32[]{:S(2)}) %all-to-all-start.3) | async-done | bytes 524320 | tf_op jit(solution)/shard_map/all_to_all | solution.py:295
  139.0 2.8 %gate.3 = (bf16[128,768]{1,0:T(8,128)(2,1)S(1)}, bf16[16,768]{1,0:T(8,128)(2,1)S(1)}) custom-call(s32[2]{0:T(128)S(1)} %pad_add_fusion.place, bf16[128,2048]{1,0:T(8,128)(2,1)S(1)} %bitcast.22, bf16[8,352,128]{2,1,0:T(8,128)(2,1)S(1)} %slice.9.refs_0_, bf16[8,352,128]{2,1,0:T(8,128)(2,1)S(1)} %bitcast.24, bf16[8,352,128]{2,1,0:T(8,128)(2,1)S(1)} %bitcast.26, ...), custom_call_target="tpu_custom_call" | custom-call | tf_op jit(solution)/shard_map/gate/pallas_call | solution.py:404
  141.8 5.4 %collective-permute-start.7 = (bf16[16,768]{1,0:T(8,128)(2,1)S(1)}, bf16[16,768]{1,0:T(8,128)(2,1)S(1)}, u32[]{:S(2)}, u32[]{:S(2)}) collective-permute-start(bf16[16,768]{1,0:T(8,128)(2,1)S(1)} %get-tuple-element.29), channel_id=1, source_target_pairs={{0,8},{8,16},{16,24},{24,32},{32,40},{40,48},{48,56},{56,64},{64,7... | collective-permute-start | bytes 73736 | tf_op jit(solution)/shard_map/ppermute | solution.py:420
  147.2 2.7 %lift.3.lifted = bf16[128,640]{1,0:T(8,128)(2,1)S(1)} custom-call(s32[2]{0:T(128)S(1)} %pad_add_fusion.place, bf16[128,2048]{1,0:T(8,128)(2,1)S(1)} %bitcast.23, bf16[8,352,128]{2,1,0:T(8,128)(2,1)S(1)} %slice.9.refs_0_, bf16[8,352,128]{2,1,0:T(8,128)(2,1)S(1)} %bitcast.25, bf16[8,352,128]{2,1,0:T(8,128)(2,1)S(1)} %bitcast.27, ...), custom_call_target="tpu_custom_call" | custom-call | flops 335544320 | bytes 3145728 | tf_op jit(solution)/shard_map/lift/pallas_call | solution.py:421
  150.9 12.8 %all_to_all.25.parts = bf16[8,16,2048]{2,1,0:T(8,128)(2,1)S(1)} all-to-all(bf16[8,16,2048]{2,1,0:T(8,128)(2,1)S(1)} %bitcast.29), channel_id=1, replica_groups=mesh['z'=8,'y'=8,'x'=4,'core'=2] {'x','core'}, dimensions={0} | all-to-all | bytes 1048576 | tf_op jit(solution)/shard_map/all_to_all | solution.py:295
  (32 shorter events, 4.3 us)
Async XLA Ops:
  2.4 42.0 %all-to-all-start = ((bf16[8,864,128]{2,1,0:T(8,128)(2,1)}), bf16[8,864,128]{2,1,0:T(8,128)(2,1)S(1)}, u32[]{:S(2)}, u32[]{:S(2)}) async-start(bf16[8,864,128]{2,1,0:T(8,128)(2,1)} %get-tuple-element.18), calls=%async_computation | async-start | bytes 3538944 | tf_op jit(solution)/shard_map/all_to_all | solution.py:295
  57.2 38.2 %copy-start.4 = (f32[256]{0:T(256)S(1)}, f32[256]{0:T(256)}, u32[]{:S(2)}) copy-start(f32[256]{0:T(256)} %param.20) | copy-start | bytes 3076
  57.2 38.2 %all-to-all-start.1 = ((bf16[8,528,128]{2,1,0:T(8,128)(2,1)}), bf16[8,528,128]{2,1,0:T(8,128)(2,1)}, u32[]{:S(2)}, u32[]{:S(2)}) async-start(bf16[8,528,128]{2,1,0:T(8,128)(2,1)} %attend.1), calls=%async_computation.1 | async-start | bytes 2162688 | tf_op jit(solution)/shard_map/all_to_all | solution.py:295
  63.4 24.2 %collective-permute-start = (bf16[2816,128]{1,0:T(8,128)(2,1)S(1)}, bf16[2816,128]{1,0:T(8,128)(2,1)S(1)}, u32[]{:S(2)}, u32[]{:S(2)}) collective-permute-start(bf16[2816,128]{1,0:T(8,128)(2,1)S(1)} %bitcast.20), channel_id=1, source_target_pairs={{0,8},{1,65},{2,10},{3,67},{4,12},{5,69},{6,14},{7,71},{8,16},{9,7... | collective-permute-start | bytes 2162696 | tf_op jit(solution)/shard_map/ppermute | solution.py:374
  67.3 22.2 %collective-permute-start.2 = (bf16[2816,128]{1,0:T(8,128)(2,1)S(1)}, bf16[2816,128]{1,0:T(8,128)(2,1)S(1)}, u32[]{:S(2)}, u32[]{:S(2)}) collective-permute-start(bf16[2816,128]{1,0:T(8,128)(2,1)S(1)} %bitcast.21), channel_id=1, source_target_pairs={{0,56},{1,449},{2,58},{3,451},{4,60},{5,453},{6,62},{7,455},{8,0},... | collective-permute-start | bytes 2162696 | tf_op jit(solution)/shard_map/ppermute | solution.py:374
  87.6 14.5 %collective-permute-start.1 = (bf16[2816,128]{1,0:T(8,128)(2,1)S(1)}, bf16[2816,128]{1,0:T(8,128)(2,1)}, u32[]{:S(2)}, u32[]{:S(2)}) collective-permute-start(bf16[2816,128]{1,0:T(8,128)(2,1)S(1)} %collective-permute-done), channel_id=1, source_target_pairs={{0,8},{1,65},{2,10},{3,67},{4,12},{5,69},{6,14},{7,71},{8,16},{9,7... | collective-permute-start | bytes 2162696 | tf_op jit(solution)/shard_map/ppermute | solution.py:375
  89.6 13.9 %collective-permute-start.3 = (bf16[2816,128]{1,0:T(8,128)(2,1)S(1)}, bf16[2816,128]{1,0:T(8,128)(2,1)}, u32[]{:S(2)}, u32[]{:S(2)}) collective-permute-start(bf16[2816,128]{1,0:T(8,128)(2,1)S(1)} %collective-permute-done.2), channel_id=1, source_target_pairs={{0,56},{1,449},{2,58},{3,451},{4,60},{5,453},{6,62},{7,455},{8,0},... | collective-permute-start | bytes 2162696 | tf_op jit(solution)/shard_map/ppermute | solution.py:375
  95.4 1.2 copy-start.1
  96.6 23.4 %copy-start.2 = (bf16[16,2048]{1,0:T(8,128)(2,1)S(1)}, bf16[16,2048]{1,0:T(8,128)(2,1)}, u32[]{:S(2)}) copy-start(bf16[16,2048]{1,0:T(8,128)(2,1)} %residual.1) | copy-start | bytes 196612
  96.6 23.4 %copy-start.3 = (f32[2048]{0:T(1024)S(1)}, f32[2048]{0:T(1024)}, u32[]{:S(2)}) copy-start(f32[2048]{0:T(1024)} %param.23) | copy-start | bytes 24580
  99.7 29.2 %slice-start = ((f32[3,704]{1,0:T(4,128)}), f32[3,640]{1,0:T(4,128)S(1)}, s32[]{:S(2)}) async-start(f32[3,704]{1,0:T(4,128)} %param.26), calls=%async_computation.5 | async-start | bytes 20480 | tf_op jit(solution)/shard_map/slice | solution.py:437
  99.7 29.2 %slice-start.1 = ((f32[3,704]{1,0:T(4,128)}), f32[3,64]{1,0:T(4,128)S(1)}, s32[]{:S(2)}) async-start(f32[3,704]{1,0:T(4,128)} %param.26), calls=%async_computation.6 | async-start | bytes 4096 | tf_op jit(solution)/shard_map/slice | solution.py:437
  103.5 17.5 %collective-permute-start.4 = (bf16[2816,128]{1,0:T(8,128)(2,1)}, bf16[2816,128]{1,0:T(8,128)(2,1)}, u32[]{:S(2)}, u32[]{:S(2)}) collective-permute-start(bf16[2816,128]{1,0:T(8,128)(2,1)} %collective-permute-done.1), channel_id=1, source_target_pairs={{0,8},{1,65},{2,10},{3,67},{4,12},{5,69},{6,14},{7,71},{8,16},{9,7... | collective-permute-start | bytes 2162696 | tf_op jit(solution)/shard_map/ppermute | solution.py:386
  105.4 14.6 %all-to-all-start.2 = ((bf16[8,16,2048]{2,1,0:T(8,128)(2,1)}), bf16[8,16,2048]{2,1,0:T(8,128)(2,1)S(1)}, u32[]{:S(2)}, u32[]{:S(2)}) async-start(bf16[8,16,2048]{2,1,0:T(8,128)(2,1)} %bitcast.9), calls=%async_computation.2 | async-start | bytes 1048576 | tf_op jit(solution)/shard_map/all_to_all | solution.py:295
  109.7 19.2 %collective-permute-start.5 = (bf16[2816,128]{1,0:T(8,128)(2,1)}, bf16[2816,128]{1,0:T(8,128)(2,1)}, u32[]{:S(2)}, u32[]{:S(2)}) collective-permute-start(bf16[2816,128]{1,0:T(8,128)(2,1)} %collective-permute-done.3), channel_id=1, source_target_pairs={{0,56},{1,449},{2,58},{3,451},{4,60},{5,453},{6,62},{7,455},{8,0},... | collective-permute-start | bytes 2162696 | tf_op jit(solution)/shard_map/ppermute | solution.py:387
  121.0 17.9 %collective-permute-start.6 = (bf16[2816,128]{1,0:T(8,128)(2,1)}, bf16[2816,128]{1,0:T(8,128)(2,1)}, u32[]{:S(2)}, u32[]{:S(2)}) collective-permute-start(bf16[2816,128]{1,0:T(8,128)(2,1)} %collective-permute-done.4), channel_id=1, source_target_pairs={{0,8},{1,65},{2,10},{3,67},{4,12},{5,69},{6,14},{7,71},{8,16},{9,7... | collective-permute-start | bytes 2162696 | tf_op jit(solution)/shard_map/ppermute | solution.py:401
  125.2 13.8 %all-to-all-start.3 = ((bf16[8,16,2048]{2,1,0:T(8,128)(2,1)}), bf16[8,16,2048]{2,1,0:T(8,128)(2,1)S(1)}, u32[]{:S(2)}, u32[]{:S(2)}) async-start(bf16[8,16,2048]{2,1,0:T(8,128)(2,1)} %get-tuple-element.25), calls=%async_computation.3 | async-start | bytes 1048576 | tf_op jit(solution)/shard_map/all_to_all | solution.py:295
  141.8 8.1 %copy-start = (bf16[704,2048]{1,0:T(8,128)(2,1)S(1)}, bf16[704,2048]{1,0:T(8,128)(2,1)}, u32[]{:S(2)}) copy-start(bf16[704,2048]{1,0:T(8,128)(2,1)} %weight.3) | copy-start | bytes 8650756
  141.8 8.1 %collective-permute-start.7 = (bf16[16,768]{1,0:T(8,128)(2,1)S(1)}, bf16[16,768]{1,0:T(8,128)(2,1)S(1)}, u32[]{:S(2)}, u32[]{:S(2)}) collective-permute-start(bf16[16,768]{1,0:T(8,128)(2,1)S(1)} %get-tuple-element.29), channel_id=1, source_target_pairs={{0,8},{8,16},{16,24},{24,32},{32,40},{40,48},{48,56},{56,64},{64,7... | collective-permute-start | bytes 73736 | tf_op jit(solution)/shard_map/ppermute | solution.py:420

commit v4 on v2

--- a/solution.py
+++ b/solution.py
@@ -16,6 +16,7 @@
 TILES = 5
 MAIN = 128 * TILES
 SENT = 512 + 352
+SHIFTS = (0, 1, -1, 2)
 epsilon = 1e-06
 masked_score = -1e30
 LOG2E = 1.4426950408889634
@@ -35,13 +36,13 @@
     return pl.BlockSpec(memory_space=pltpu.VMEM)
 
 
-def pack_kernel(q1, q2, k1, k2, v, lift, gate, qsend, ksend, vv, ll, gg, kk, sems):
+def pack_kernel(q1, q2, k1, k2, v, lift, gate, qsend, ksend, vv, ll, gg, rows, sems, sent):
     moves = [
         pltpu.make_async_copy(src, dst, sems.at[i])
         for i, (src, dst) in enumerate(
             (
-                (k1, kk.at[0]),
-                (k2, kk.at[1]),
+                (k1, rows.at[0:128]),
+                (k2, rows.at[128:256]),
                 (v, vv),
                 (lift, ll),
                 (gate, gg),
@@ -54,16 +55,17 @@
         move.start()
     for move in moves:
         move.wait()
-    tail = jnp.concatenate([ll[:, MAIN:], gg[:, MAIN:]], axis=1)
-    for i in range(SIDE):
-        ksend[i, 0:128, :] = kk[0]
-        ksend[i, 128:256, :] = kk[1]
-        ksend[i, 256:384, :] = vv[:, 0:128]
-        ksend[i, 384:512, :] = vv[:, 128:256]
-        for n in range(TILES):
-            ksend[i, 512 + 32 * n : 544 + 32 * n, :] = gg[:, 128 * n : 128 * n + 128]
-            ksend[i, 704 + 32 * n : 736 + 32 * n, :] = ll[:, 128 * n : 128 * n + 128]
-        ksend[i, 672:704, :] = tail
+    rows[256:384, :] = vv[:, 0:128]
+    rows[384:512, :] = vv[:, 128:256]
+    for n in range(TILES):
+        rows[512 + 32 * n : 544 + 32 * n, :] = gg[:, 128 * n : 128 * n + 128]
+        rows[704 + 32 * n : 736 + 32 * n, :] = ll[:, 128 * n : 128 * n + 128]
+    rows[672:704, :] = jnp.concatenate([ll[:, MAIN:], gg[:, MAIN:]], axis=1)
+    copies = [pltpu.make_async_copy(rows, ksend.at[i], sent.at[i]) for i in range(SIDE)]
+    for copy in copies:
+        copy.start()
+    for copy in copies:
+        copy.wait()
 
 
 def attend_kernel(plan, qpool, kpool, out, scores):
@@ -160,7 +162,7 @@
     lax.fori_loop(first_chunk, SIDE // 2, chunk, 0)
 
 
-def join_kernel(mix, parts, gain, weight, out):
+def join_kernel(mix, parts, gain, out):
     tails = [parts[i, 512:528, :].astype(f32) for i in range(SIDE)]
 
     def joined(m):
@@ -182,17 +184,28 @@
     mixed = joined(0) - mix[0] * joined(1)
     r = lax.rsqrt(jnp.mean(mixed * mixed, axis=-1, keepdims=True) + epsilon)
     head = (mixed * r * gain[...]).astype(bf16)
-    out[...] = jnp.dot(head, weight[...], preferred_element_type=f32).astype(bf16)
-
-
-def norm_kernel(parts, residual, gain, stream, normed):
-    att = parts[0].astype(f32)
-    for i in range(1, 8):
-        att = att + parts[i].astype(f32)
-    total = residual[...].astype(f32) + att
-    stream[...] = total
-    r = lax.rsqrt(jnp.mean(total * total, axis=-1, keepdims=True) + epsilon)
-    normed[...] = (total * r * gain[...]).astype(bf16)
+    for i in range(4):
+        out[i] = head
+
+
+def project_kernel(place, heads, *refs):
+    weights, (half, sent, buffer, sems) = refs[:4], refs[4:]
+    x = place[1]
+    moves = [
+        pltpu.make_async_copy(weight, buffer.at[i], sems.at[i]) for i, weight in enumerate(weights)
+    ]
+    for move in moves:
+        move.start()
+    for i, shift in enumerate(SHIFTS):
+        moves[i].wait()
+        head = heads[lax.rem(x + 4 - shift, 4)]
+        for n in range(0, 2048, 256):
+            d = jnp.dot(head, buffer[i, :, n : n + 256], preferred_element_type=f32)
+            if i > 0:
+                d = d + half[:, n : n + 256]
+            half[:, n : n + 256] = d
+            if i == 3:
+                sent[:, n : n + 256] = d.astype(bf16)
 
 
 def fetched(core, weights, buffer, sems, first):
@@ -229,8 +242,16 @@
     return acc
 
 
-def gate_kernel(core, rows, weights, gated, edge, buffer, sems):
-    fetched(core[0], weights, buffer, sems, 0)
+def gate_kernel(place, half, other, residual, gain, weights, gated, edge, rows, stream, buffer, sems):
+    fetched(place[0], weights, buffer, sems, 0)
+    for n in range(0, 128, 32):
+        total = residual[n : n + 32].astype(f32) + (
+            half[n : n + 32] + other[n : n + 32].astype(f32)
+        )
+        r = lax.rsqrt(jnp.mean(total * total, axis=-1, keepdims=True) + epsilon)
+        rows[n : n + 32] = (total * r * gain[...]).astype(bf16)
+    own = pl.ds(pl.multiple_of(place[2] * 16, 16), 16)
+    stream[...] = residual[own].astype(f32) + (half[own] + other[own].astype(f32))
     for n, part in enumerate(multiplied(rows, weights, buffer, sems, 0)):
         part = part.astype(bf16)
         gated[:, 256 * n : 256 * n + 256] = part
@@ -315,7 +336,10 @@
     plan = jnp.where(core == 0, along_y, along_z).astype(jnp.int32)
     smem = pl.BlockSpec(memory_space=pltpu.SMEM)
     hbm = pl.BlockSpec(memory_space=pltpu.HBM)
-    own_core = core.reshape(1).astype(jnp.int32)
+    x = lax.axis_index("x")
+    place = jnp.stack([core, x, 2 * x + core]).astype(jnp.int32)
+    above = lax.ppermute(out_weight, "x", [(i, (i + 1) % 4) for i in range(4)])
+    below = lax.ppermute(out_weight, "x", [(i, (i + 3) % 4) for i in range(4)])
     qsend, ksend = pl.pallas_call(
         pack_kernel,
         out_shape=[
@@ -323,13 +347,14 @@
             jax.ShapeDtypeStruct((SIDE, SENT, 128), bf16),
         ],
         in_specs=[hbm] * 7,
-        out_specs=[vmem()] * 2,
+        out_specs=[vmem(), hbm],
         scratch_shapes=[
             pltpu.VMEM((128, 256), bf16),
             pltpu.VMEM((32, 704), bf16),
             pltpu.VMEM((32, 704), bf16),
-            pltpu.VMEM((2, 128, 128), bf16),
+            pltpu.VMEM((SENT, 128), bf16),
             pltpu.SemaphoreType.DMA((7,)),
+            pltpu.SemaphoreType.DMA((SIDE,)),
         ],
         compiler_params=SMALL,
         name="pack",
@@ -353,42 +378,47 @@
         name="attend",
     )(plan, qpool, kpool)
     back = swapped(out, ALL, Q_GROUPS)
-    attended = pl.pallas_call(
+    before = gathered(residual, TP)
+    across = lax.ppermute(above, "x", [(i, (i + 1) % 4) for i in range(4)])
+    heads = pl.pallas_call(
         join_kernel,
-        out_shape=jax.ShapeDtypeStruct((tokens, width), bf16),
-        in_specs=[pl.BlockSpec(memory_space=pltpu.SMEM)] + [vmem()] * 3,
+        out_shape=jax.ShapeDtypeStruct((4, tokens, VD), bf16),
+        in_specs=[pl.BlockSpec(memory_space=pltpu.SMEM)] + [vmem()] * 2,
         out_specs=vmem(),
         compiler_params=SMALL,
         name="join",
-    )(mix_weight, back, head_gain.reshape(1, VD), out_weight)
-    parts = swapped(attended.reshape(8, own, width), TP)
-    stream, normed = pl.pallas_call(
-        norm_kernel,
+    )(mix_weight, back, head_gain.reshape(1, VD))
+    heads = swapped(heads, "x")
+    half, sent = pl.pallas_call(
+        project_kernel,
         out_shape=[
-            jax.ShapeDtypeStruct((own, width), f32),
-            jax.ShapeDtypeStruct((own, width), bf16),
-        ],
-        in_specs=[vmem()] * 3,
+            jax.ShapeDtypeStruct((tokens, width), f32),
+            jax.ShapeDtypeStruct((tokens, width), bf16),
+        ],
+        in_specs=[smem, vmem()] + [pl.BlockSpec(memory_space=pl.ANY)] * 4,
         out_specs=[vmem()] * 2,
-        compiler_params=SMALL,
-        name="norm",
-    )(parts, residual, norm_gain.reshape(1, width))
-    rows = gathered(normed, TP)
-    gated, edge = pl.pallas_call(
+        scratch_shapes=[pltpu.VMEM((4, VD, 2048), bf16), pltpu.SemaphoreType.DMA((4,))],
+        compiler_params=SMALL,
+        name="project",
+    )(place, heads, out_weight, above, below, across)
+    other = lax.ppermute(sent, "core", [(0, 1), (1, 0)])
+    gated, edge, rows, stream = pl.pallas_call(
         gate_kernel,
         out_shape=[
             jax.ShapeDtypeStruct((tokens, MAIN + 128), bf16),
             jax.ShapeDtypeStruct((16, MAIN + 128), bf16),
-        ],
-        in_specs=[smem, vmem(), hbm],
-        out_specs=[vmem()] * 2,
+            jax.ShapeDtypeStruct((tokens, width), bf16),
+            jax.ShapeDtypeStruct((own, width), f32),
+        ],
+        in_specs=[smem] + [vmem()] * 4 + [hbm],
+        out_specs=[vmem()] * 4,
         scratch_shapes=[
             pltpu.VMEM((SIDE, SIDE, 192, 128), bf16),
             pltpu.SemaphoreType.DMA((SIDE,)),
         ],
         compiler_params=SMALL,
         name="gate",
-    )(own_core, rows, weights)
+    )(place, half, other, before, norm_gain.reshape(1, width), weights)
     route = [(i, i + 1) for i in range(SIDE * SIDE - 1)]
     prior = lax.ppermute(edge, ("z", "y"), route)
     lifted = pl.pallas_call(
@@ -405,7 +435,7 @@
             flops=2 * 128 * 2048 * 640, bytes_accessed=3 << 20, transcendentals=0
         ),
         name="lift",
-    )(own_core, rows, weights)
+    )(place, rows, weights)
     gap = jnp.zeros((WIDTH, 64), f32)
     taps = jnp.concatenate([conv_taps[:, :MAIN], gap, conv_taps[:, MAIN:]], axis=1)
     down = pl.pallas_call(

time: 164 us -> 176 us (1.073)
  the two profiles are of different devices: /device:TPU:128 before, /device:TPU:64 now
where the time goes in v4:
time: 176 us; the launch traced here: 175 us
  blocking collectives  88.5 us (50%)
  waiting for transfers between devices  25.9 us (15%)
  starting transfers between devices  22.9 us (13%)
  Pallas kernels  21.7 us (12%)
  between operations  14.2 us (8%)
    all_to_all x2, blocking collectives, swapped(): return lax.all_to_all(a, axis, 0, 0, axis_index_groups=groups, tiled=True)  47.8 us
    all_gather x2, blocking collectives, gathered(): return lax.all_gather(a, axis, axis_index_groups=groups, axis=0, tiled=True)  40.7 us
    all_to_all x2, waiting for transfers between devices, swapped(): return lax.all_to_all(a, axis, 0, 0, axis_index_groups=groups, tiled=True)  15.2 us
    all_to_all x2, starting transfers between devices, swapped(): return lax.all_to_all(a, axis, 0, 0, axis_index_groups=groups, tiled=True)  9.84 us
    pallas_call x1, Pallas kernels, on_device(): pl.pallas_call(attend_kernel, grid=(1,), out_shape=jax.ShapeDtypeStruct((...  6.04 us
    ppermute x1, waiting for transfers between devices, on_device(): across = lax.ppermute(above, 'x', [(i, (i + 1) % 4) for i in range(4)])  5.75 us
    pallas_call x1, Pallas kernels, on_device(): pl.pallas_call(lift_kernel, out_shape=jax.ShapeDtypeStruct((tokens, MAIN)...  3.59 us
    ppermute x1, starting transfers between devices, on_device(): below = lax.ppermute(out_weight, 'x', [(i, (i + 3) % 4) for i in range(4)])  3.57 us
  transfers between devices with their start and end apart: 8, of which 5 were waited for; matrix products, arithmetic and copies ran while one was open for 0% of the time, Pallas kernels for 8%

profile of v4, /device:TPU:64, one launch (start us, length us, event | category | flops | bytes accessed | tf_op | source)
XLA Modules:
  0.0 175.0 jit_solution(15660870929974939494)
XLA Ops:
  6.5 3.4 %pack.1 = (bf16[256,128]{1,0:T(8,128)(2,1)S(1)}, bf16[8,864,128]{2,1,0:T(8,128)(2,1)S(1)}) custom-call(bf16[128,128]{1,0:T(8,128)(2,1)} %q1.1, bf16[128,128]{1,0:T(8,128)(2,1)} %q2.1, bf16[128,128]{1,0:T(8,128)(2,1)} %k1.1, bf16[128,128]{1,0:T(8,128)(2,1)} %k2.1, bf16[128,256]{1,0:T(8,128)(2,1)} %v.1, bf16[32,704]{1,0:T(8,128)(2,1)} %lift.2, ...), custom_call_target="tpu_custom_call" | custom-call | tf_op jit(solution)/shard_map/pack/pallas_call | solution.py:343
  9.9 34.9 %all_to_all.20.kpool = bf16[8,864,128]{2,1,0:T(8,128)(2,1)S(1)} all-to-all(bf16[8,864,128]{2,1,0:T(8,128)(2,1)S(1)} %get-tuple-element.14), channel_id=1, replica_groups={{0,64,128,192,256,320,384,448},{2,66,130,194,258,322,386,450},{4,68,132..., dimensions={0} | all-to-all | bytes 3538944 | tf_op jit(solution)/shard_map/all_to_all | solution.py:298
  44.9 0.9 slice.12
  46.4 3.4 %collective-permute-start = (bf16[256,2048]{1,0:T(8,128)(2,1)S(1)}, bf16[256,2048]{1,0:T(8,128)(2,1)}, u32[]{:S(2)}, u32[]{:S(2)}) collective-permute-start(bf16[256,2048]{1,0:T(8,128)(2,1)S(1)} %copy-done.1), channel_id=1, source_target_pairs={{0,2},{2,4},{4,6},{6,0},{1,3},{3,5},{5,7},{7,1},{8,10},{10,12},{12... | collective-permute-start | bytes 3145736 | tf_op jit(solution)/shard_map/ppermute | solution.py:341
  49.9 27.6 %all_gather.9 = bf16[2048,128]{1,0:T(8,128)(2,1)S(1)} all-gather(bf16[256,128]{1,0:T(8,128)(2,1)S(1)} %get-tuple-element.13), channel_id=1, replica_groups={{0,8,16,24,32,40,48,56},{2,10,18,26,34,42,50,58},{4,12,20,28,36,44,52,6..., dimensions={0}, use_global_device_ids=true | all-gather | bytes 589824 | tf_op jit(solution)/shard_map/all_gather | solution.py:302
  77.5 6.0 %attend.1 = bf16[8,528,128]{2,1,0:T(8,128)(2,1)} custom-call(s32[6]{0:T(128)S(1)} %broadcast_select_fusion.plan, bf16[8,256,128]{2,1,0:T(8,128)(2,1)S(1)} %bitcast.13, bf16[8,864,128]{2,1,0:T(8,128)(2,1)S(1)} %all_to_all.20.kpool), custom_call_target="tpu_custom_call" | custom-call | tf_op jit(solution)/shard_map/attend/pallas_call | solution.py:366
  83.5 5.9 %all-to-all-start.1 = ((bf16[8,528,128]{2,1,0:T(8,128)(2,1)}), bf16[8,528,128]{2,1,0:T(8,128)(2,1)S(1)}, u32[]{:S(2)}, u32[]{:S(2)}) async-start(bf16[8,528,128]{2,1,0:T(8,128)(2,1)} %attend.1), calls=%async_computation.1 | async-start | bytes 2162688 | tf_op jit(solution)/shard_map/all_to_all | solution.py:298
  89.4 3.6 %collective-permute-start.1 = (bf16[256,2048]{1,0:T(8,128)(2,1)S(1)}, bf16[256,2048]{1,0:T(8,128)(2,1)}, u32[]{:S(2)}, u32[]{:S(2)}) collective-permute-start(bf16[256,2048]{1,0:T(8,128)(2,1)S(1)} %copy-done.1), channel_id=1, source_target_pairs={{0,6},{2,0},{4,2},{6,4},{1,7},{3,1},{5,3},{7,5},{8,14},{10,8},{12,... | collective-permute-start | bytes 3145736 | tf_op jit(solution)/shard_map/ppermute | solution.py:342
  93.0 2.3 %collective-permute-start.2 = (bf16[256,2048]{1,0:T(8,128)(2,1)}, bf16[256,2048]{1,0:T(8,128)(2,1)}, u32[]{:S(2)}, u32[]{:S(2)}) collective-permute-start(bf16[256,2048]{1,0:T(8,128)(2,1)} %collective-permute-done.refs_1_), channel_id=1, source_target_pairs={{0,2},{2,4},{4,6},{6,0},{1,3},{3,5},{5,7},{7,1},{8,10},{10,12},{12... | collective-permute-start | bytes 3145736 | tf_op jit(solution)/shard_map/ppermute | solution.py:382
  95.9 12.8 %all-to-all-done.1.parts = bf16[8,528,128]{2,1,0:T(8,128)(2,1)S(1)} async-done(((bf16[8,528,128]{2,1,0:T(8,128)(2,1)}), bf16[8,528,128]{2,1,0:T(8,128)(2,1)S(1)}, u32[]{:S(2)}, u32[]{:S(2)}) %all-to-all-start.1) | async-done | bytes 1081376 | tf_op jit(solution)/shard_map/all_to_all | solution.py:298
  108.7 1.3 join.1
  110.1 4.0 %all-to-all-start.2 = ((bf16[4,128,256]{2,1,0:T(8,128)(2,1)}), bf16[4,128,256]{2,1,0:T(8,128)(2,1)S(1)}, u32[]{:S(2)}, u32[]{:S(2)}) async-start(bf16[4,128,256]{2,1,0:T(8,128)(2,1)} %join.1), calls=%async_computation.2 | async-start | bytes 524288 | tf_op jit(solution)/shard_map/all_to_all | solution.py:298
  114.1 2.6 %collective-permute-done.1.refs_2_ = bf16[256,2048]{1,0:T(8,128)(2,1)} collective-permute-done((bf16[256,2048]{1,0:T(8,128)(2,1)S(1)}, bf16[256,2048]{1,0:T(8,128)(2,1)}, u32[]{:S(2)}, u32[]{:S(2)}) %collective-permute-start.1) | collective-permute-done | bytes 1048608 | tf_op jit(solution)/shard_map/ppermute | solution.py:342
  116.7 5.8 %collective-permute-done.2.refs_3_ = bf16[256,2048]{1,0:T(8,128)(2,1)} collective-permute-done((bf16[256,2048]{1,0:T(8,128)(2,1)}, bf16[256,2048]{1,0:T(8,128)(2,1)}, u32[]{:S(2)}, u32[]{:S(2)}) %collective-permute-start.2) | collective-permute-done | bytes 1048608 | tf_op jit(solution)/shard_map/ppermute | solution.py:382
  122.5 2.4 %all-to-all-done.2.heads = bf16[4,128,256]{2,1,0:T(8,128)(2,1)S(1)} async-done(((bf16[4,128,256]{2,1,0:T(8,128)(2,1)}), bf16[4,128,256]{2,1,0:T(8,128)(2,1)S(1)}, u32[]{:S(2)}, u32[]{:S(2)}) %all-to-all-start.2) | async-done | bytes 262176 | tf_op jit(solution)/shard_map/all_to_all | solution.py:298
  124.9 2.8 %project.1 = (f32[128,2048]{1,0:T(8,128)S(1)}, bf16[128,2048]{1,0:T(8,128)(2,1)S(1)}) custom-call(s32[3]{0:T(128)S(1)} %pad_add_fusion.place.core, bf16[4,128,256]{2,1,0:T(8,128)(2,1)S(1)} %all-to-all-done.2.heads, bf16[256,2048]{1,0:T(8,128)(2,1)S(1)} %copy-done.1, bf16[256,2048]{1,0:T(8,128)(2,1)} %collective-permute-done.refs_1_, ...), custom_call_target="tpu_custom_call" | custom-call | tf_op jit(solution)/shard_map/project/pallas_call | solution.py:392
  127.7 1.9 %collective-permute-start.3 = (bf16[128,2048]{1,0:T(8,128)(2,1)S(1)}, bf16[128,2048]{1,0:T(8,128)(2,1)S(1)}, u32[]{:S(2)}, u32[]{:S(2)}) collective-permute-start(bf16[128,2048]{1,0:T(8,128)(2,1)S(1)} %get-tuple-element.16), channel_id=1, source_target_pairs={{0,1},{1,0},{2,3},{3,2},{4,5},{5,4},{6,7},{7,6},{8,9},{9,8},{10,11... | collective-permute-start | bytes 1572872 | tf_op jit(solution)/shard_map/ppermute | solution.py:404
  129.8 13.1 %all_gather.10.residual = bf16[128,2048]{1,0:T(8,128)(2,1)S(1)} all-gather(bf16[16,2048]{1,0:T(8,128)(2,1)S(1)} %copy-done.4), channel_id=1, replica_groups=mesh['z'=8,'y'=8,'x'=4,'core'=2] {'x','core'}, dimensions={0}, use_global_device_ids=true | all-gather | bytes 589824 | tf_op jit(solution)/shard_map/all_gather | solution.py:302
  142.9 2.8 %gate.3 = (bf16[128,768]{1,0:T(8,128)(2,1)S(1)}, bf16[16,768]{1,0:T(8,128)(2,1)S(1)}, bf16[128,2048]{1,0:T(8,128)(2,1)S(1)}, f32[16,2048]{1,0:T(8,128)S(1)}) custom-call(s32[3]{0:T(128)S(1)} %pad_add_fusion.place.core, f32[128,2048]{1,0:T(8,128)S(1)} %get-tuple-element.15.half, bf16[128,2048]{1,0:T(8,128)(2,1)S(1)} %collective-permute-done.3.other, ...), custom_call_target="tpu_custom_call" | custom-call | tf_op jit(solution)/shard_map/gate/pallas_call | solution.py:405
  145.7 1.9 %collective-permute-start.4 = (bf16[16,768]{1,0:T(8,128)(2,1)S(1)}, bf16[16,768]{1,0:T(8,128)(2,1)S(1)}, u32[]{:S(2)}, u32[]{:S(2)}) collective-permute-start(bf16[16,768]{1,0:T(8,128)(2,1)S(1)} %get-tuple-element.19), channel_id=1, source_target_pairs={{0,8},{8,16},{16,24},{24,32},{32,40},{40,48},{48,56},{56,64},{64,7... | collective-permute-start | bytes 73736 | tf_op jit(solution)/shard_map/ppermute | solution.py:423
  147.7 3.6 %lift.3.lifted = bf16[128,640]{1,0:T(8,128)(2,1)S(1)} custom-call(s32[3]{0:T(128)S(1)} %pad_add_fusion.place.core, bf16[128,2048]{1,0:T(8,128)(2,1)S(1)} %get-tuple-element.18.rows, bf16[8,8,352,128]{3,2,1,0:T(8,128)(2,1)} %bitcast.18), custom_call_target="tpu_custom_call" | custom-call | flops 335544320 | bytes 3145728 | tf_op jit(solution)/shard_map/lift/pallas_call | solution.py:424
  151.3 2.3 %collective-permute-done.4.prior = bf16[16,768]{1,0:T(8,128)(2,1)S(1)} collective-permute-done((bf16[16,768]{1,0:T(8,128)(2,1)S(1)}, bf16[16,768]{1,0:T(8,128)(2,1)S(1)}, u32[]{:S(2)}, u32[]{:S(2)}) %collective-permute-start.4) | collective-permute-done | bytes 24608 | tf_op jit(solution)/shard_map/ppermute | solution.py:423
  153.6 1.0 down.1
  154.5 12.9 %all_to_all.21.parts = bf16[8,16,2048]{2,1,0:T(8,128)(2,1)S(1)} all-to-all(bf16[8,16,2048]{2,1,0:T(8,128)(2,1)S(1)} %bitcast.14), channel_id=1, replica_groups=mesh['z'=8,'y'=8,'x'=4,'core'=2] {'x','core'}, dimensions={0} | all-to-all | bytes 1048576 | tf_op jit(solution)/shard_map/all_to_all | solution.py:298
  (27 shorter events, 1.6 us)
Async XLA Ops:
  6.5 136.3 %all-gather.2.cloned.1.call-start = ((), (), s32[]{:S(2)}) async-start(), calls=%async_computation.4 | async-start | bytes 6488064 | tf_op jit(solution)/shard_map/all_gather | solution.py:302
  44.9 1.5 copy-start.1
  46.4 46.7 %collective-permute-start = (bf16[256,2048]{1,0:T(8,128)(2,1)S(1)}, bf16[256,2048]{1,0:T(8,128)(2,1)}, u32[]{:S(2)}, u32[]{:S(2)}) collective-permute-start(bf16[256,2048]{1,0:T(8,128)(2,1)S(1)} %copy-done.1), channel_id=1, source_target_pairs={{0,2},{2,4},{4,6},{6,0},{1,3},{3,5},{5,7},{7,1},{8,10},{10,12},{12... | collective-permute-start | bytes 3145736 | tf_op jit(solution)/shard_map/ppermute | solution.py:341
  83.5 25.2 %copy-start.3 = (f32[256]{0:T(256)S(1)}, f32[256]{0:T(256)}, u32[]{:S(2)}) copy-start(f32[256]{0:T(256)} %param.20) | copy-start | bytes 3076
  83.5 25.2 %all-to-all-start.1 = ((bf16[8,528,128]{2,1,0:T(8,128)(2,1)}), bf16[8,528,128]{2,1,0:T(8,128)(2,1)S(1)}, u32[]{:S(2)}, u32[]{:S(2)}) async-start(bf16[8,528,128]{2,1,0:T(8,128)(2,1)} %attend.1), calls=%async_computation.1 | async-start | bytes 2162688 | tf_op jit(solution)/shard_map/all_to_all | solution.py:298
  89.4 27.3 %collective-permute-start.1 = (bf16[256,2048]{1,0:T(8,128)(2,1)S(1)}, bf16[256,2048]{1,0:T(8,128)(2,1)}, u32[]{:S(2)}, u32[]{:S(2)}) collective-permute-start(bf16[256,2048]{1,0:T(8,128)(2,1)S(1)} %copy-done.1), channel_id=1, source_target_pairs={{0,6},{2,0},{4,2},{6,4},{1,7},{3,1},{5,3},{7,5},{8,14},{10,8},{12,... | collective-permute-start | bytes 3145736 | tf_op jit(solution)/shard_map/ppermute | solution.py:342
  93.0 29.5 %collective-permute-start.2 = (bf16[256,2048]{1,0:T(8,128)(2,1)}, bf16[256,2048]{1,0:T(8,128)(2,1)}, u32[]{:S(2)}, u32[]{:S(2)}) collective-permute-start(bf16[256,2048]{1,0:T(8,128)(2,1)} %collective-permute-done.refs_1_), channel_id=1, source_target_pairs={{0,2},{2,4},{4,6},{6,0},{1,3},{3,5},{5,7},{7,1},{8,10},{10,12},{12... | collective-permute-start | bytes 3145736 | tf_op jit(solution)/shard_map/ppermute | solution.py:382
  110.1 14.8 %all-to-all-start.2 = ((bf16[4,128,256]{2,1,0:T(8,128)(2,1)}), bf16[4,128,256]{2,1,0:T(8,128)(2,1)S(1)}, u32[]{:S(2)}, u32[]{:S(2)}) async-start(bf16[4,128,256]{2,1,0:T(8,128)(2,1)} %join.1), calls=%async_computation.2 | async-start | bytes 524288 | tf_op jit(solution)/shard_map/all_to_all | solution.py:298
  114.1 15.6 %slice-start = ((f32[3,704]{1,0:T(4,128)}), f32[3,640]{1,0:T(4,128)S(1)}, s32[]{:S(2)}) async-start(f32[3,704]{1,0:T(4,128)} %param.26), calls=%async_computation.5 | async-start | bytes 20480 | tf_op jit(solution)/shard_map/slice | solution.py:440
  114.1 15.6 %slice-start.1 = ((f32[3,704]{1,0:T(4,128)}), f32[3,64]{1,0:T(4,128)S(1)}, s32[]{:S(2)}) async-start(f32[3,704]{1,0:T(4,128)} %param.26), calls=%async_computation.6 | async-start | bytes 4096 | tf_op jit(solution)/shard_map/slice | solution.py:440
  114.1 15.6 %copy-start.4 = (bf16[16,2048]{1,0:T(8,128)(2,1)S(1)}, bf16[16,2048]{1,0:T(8,128)(2,1)}, u32[]{:S(2)}) copy-start(bf16[16,2048]{1,0:T(8,128)(2,1)} %param.21) | copy-start | bytes 196612
  114.1 28.7 %copy-start.2 = (f32[2048]{0:T(1024)S(1)}, f32[2048]{0:T(1024)}, u32[]{:S(2)}) copy-start(f32[2048]{0:T(1024)} %param.23) | copy-start | bytes 24580
  127.7 15.2 %collective-permute-start.3 = (bf16[128,2048]{1,0:T(8,128)(2,1)S(1)}, bf16[128,2048]{1,0:T(8,128)(2,1)S(1)}, u32[]{:S(2)}, u32[]{:S(2)}) collective-permute-start(bf16[128,2048]{1,0:T(8,128)(2,1)S(1)} %get-tuple-element.16), channel_id=1, source_target_pairs={{0,1},{1,0},{2,3},{3,2},{4,5},{5,4},{6,7},{7,6},{8,9},{9,8},{10,11... | collective-permute-start | bytes 1572872 | tf_op jit(solution)/shard_map/ppermute | solution.py:404
  145.7 7.8 %collective-permute-start.4 = (bf16[16,768]{1,0:T(8,128)(2,1)S(1)}, bf16[16,768]{1,0:T(8,128)(2,1)S(1)}, u32[]{:S(2)}, u32[]{:S(2)}) collective-permute-start(bf16[16,768]{1,0:T(8,128)(2,1)S(1)} %get-tuple-element.19), channel_id=1, source_target_pairs={{0,8},{8,16},{16,24},{24,32},{32,40},{40,48},{48,56},{56,64},{64,7... | collective-permute-start | bytes 73736 | tf_op jit(solution)/shard_map/ppermute | solution.py:423
  147.6 5.9 %copy-start = (bf16[704,2048]{1,0:T(8,128)(2,1)S(1)}, bf16[704,2048]{1,0:T(8,128)(2,1)}, u32[]{:S(2)}) copy-start(bf16[704,2048]{1,0:T(8,128)(2,1)} %weight.1) | copy-start | bytes 8650756
Sparse Core Ops, SparseCore 0:
  46.0 45.3 all-gather.1

commit v5 on v4

--- a/solution.py
+++ b/solution.py
@@ -189,15 +189,19 @@
 
 
 def project_kernel(place, heads, *refs):
-    weights, (half, sent, buffer, sems) = refs[:4], refs[4:]
+    weights, (half, sent, buffer, sems) = refs[:5], refs[5:]
     x = place[1]
+    slots = [buffer.at[0], buffer.at[1], buffer.at[2], buffer.at[3, 0:128], buffer.at[3, 128:256]]
     moves = [
-        pltpu.make_async_copy(weight, buffer.at[i], sems.at[i]) for i, weight in enumerate(weights)
+        pltpu.make_async_copy(weight, slot, sems.at[i])
+        for i, (weight, slot) in enumerate(zip(weights, slots))
     ]
     for move in moves:
         move.start()
     for i, shift in enumerate(SHIFTS):
         moves[i].wait()
+        if i == 3:
+            moves[4].wait()
         head = heads[lax.rem(x + 4 - shift, 4)]
         for n in range(0, 2048, 256):
             d = jnp.dot(head, buffer[i, :, n : n + 256], preferred_element_type=f32)
@@ -379,7 +383,11 @@
     )(plan, qpool, kpool)
     back = swapped(out, ALL, Q_GROUPS)
     before = gathered(residual, TP)
-    across = lax.ppermute(above, "x", [(i, (i + 1) % 4) for i in range(4)])
+    above, below, before = lax.optimization_barrier((above, below, before))
+    across = (
+        lax.ppermute(above[0:128], "x", [(i, (i + 1) % 4) for i in range(4)]),
+        lax.ppermute(below[128:256], "x", [(i, (i + 3) % 4) for i in range(4)]),
+    )
     heads = pl.pallas_call(
         join_kernel,
         out_shape=jax.ShapeDtypeStruct((4, tokens, VD), bf16),
@@ -395,12 +403,12 @@
             jax.ShapeDtypeStruct((tokens, width), f32),
             jax.ShapeDtypeStruct((tokens, width), bf16),
         ],
-        in_specs=[smem, vmem()] + [pl.BlockSpec(memory_space=pl.ANY)] * 4,
+        in_specs=[smem, vmem()] + [pl.BlockSpec(memory_space=pl.ANY)] * 5,
         out_specs=[vmem()] * 2,
-        scratch_shapes=[pltpu.VMEM((4, VD, 2048), bf16), pltpu.SemaphoreType.DMA((4,))],
+        scratch_shapes=[pltpu.VMEM((4, VD, 2048), bf16), pltpu.SemaphoreType.DMA((5,))],
         compiler_params=SMALL,
         name="project",
-    )(place, heads, out_weight, above, below, across)
+    )(place, heads, in_hbm(out_weight), above, below, *across)
     other = lax.ppermute(sent, "core", [(0, 1), (1, 0)])
     gated, edge, rows, stream = pl.pallas_call(
         gate_kernel,

time: 176 us -> 193 us (1.097)
  blocking collectives: 88.5 us -> 111 us
  waiting for transfers between devices: 25.9 us -> 13.1 us
  starting transfers between devices: 22.9 us -> 26.9 us
  local copies, waits for them, and re-layouts: 1.67 us -> 4.97 us
    all_gather x2, blocking collectives: 40.7 us -> 61.2 us  [gathered(): return lax.all_gather(a, axis, axis_index_groups=groups, axis=0, tiled=True)]
    all_to_all x2, waiting for transfers between devices: 15.2 us -> 1.1 us  [swapped(): return lax.all_to_all(a, axis, 0, 0, axis_index_groups=groups, tiled=True)]
    ppermute x1 -> x2, starting transfers between devices: 2.26 us -> 7.03 us  [the longest x1 3.52 us: on_device(): lax.ppermute(above[0:128], 'x', [(i, (i + 1) % 4) for i in range(4)])]
    ppermute x1, waiting for transfers between devices: 2.58 us -> 0.01 us  [on_device(): below = lax.ppermute(out_weight, 'x', [(i, (i + 3) % 4) for i in range(4)])]
    ppermute x1 -> x2, waiting for transfers between devices: 5.75 us -> 7.95 us  [the longest x1 4.6 us: on_device(): lax.ppermute(above[0:128], 'x', [(i, (i + 1) % 4) for i in range(4)])]
    all_to_all x2, blocking collectives: 47.8 us -> 49.9 us  [swapped(): return lax.all_to_all(a, axis, 0, 0, axis_index_groups=groups, tiled=True)]
  transfers between devices with their start and end apart: 8 -> 9, of which waited for: 5 -> 5; matrix products, arithmetic and copies ran while one was open for 0% -> 1% of each run, Pallas kernels for 8% -> 7%
where the time goes in v5:
time: 193 us; the launch traced here: 192 us
  blocking collectives  111 us (58%)
  starting transfers between devices  26.9 us (14%)
  Pallas kernels  21.6 us (11%)
  between operations  14.3 us (7%)
  waiting for transfers between devices  13.1 us (7%)
  local copies, waits for them, and re-layouts  4.97 us (3%)
    all_gather x2, blocking collectives, gathered(): return lax.all_gather(a, axis, axis_index_groups=groups, axis=0, tiled=True)  61.2 us
    all_to_all x2, blocking collectives, swapped(): return lax.all_to_all(a, axis, 0, 0, axis_index_groups=groups, tiled=True)  49.9 us
    all_to_all x2, starting transfers between devices, swapped(): return lax.all_to_all(a, axis, 0, 0, axis_index_groups=groups, tiled=True)  9.01 us
    pallas_call x1, Pallas kernels, on_device(): pl.pallas_call(attend_kernel, grid=(1,), out_shape=jax.ShapeDtypeStruct((...  6.07 us
    ppermute x1, waiting for transfers between devices, on_device(): lax.ppermute(above[0:128], 'x', [(i, (i + 1) % 4) for i in range(4)])  4.6 us
  transfers between devices with their start and end apart: 9, of which 5 were waited for; matrix products, arithmetic and copies ran while one was open for 1% of the time, Pallas kernels for 7%

profile of v5, /device:TPU:64, one launch (start us, length us, event | category | flops | bytes accessed | tf_op | source)
XLA Modules:
  0.0 192.2 jit_solution(10650854172182781856)
XLA Ops:
  6.5 3.4 %pack.1 = (bf16[256,128]{1,0:T(8,128)(2,1)S(1)}, bf16[8,864,128]{2,1,0:T(8,128)(2,1)S(1)}) custom-call(bf16[128,128]{1,0:T(8,128)(2,1)} %q1.1, bf16[128,128]{1,0:T(8,128)(2,1)} %q2.1, bf16[128,128]{1,0:T(8,128)(2,1)} %k1.1, bf16[128,128]{1,0:T(8,128)(2,1)} %k2.1, bf16[128,256]{1,0:T(8,128)(2,1)} %v.1, bf16[32,704]{1,0:T(8,128)(2,1)} %lift.2, ...), custom_call_target="tpu_custom_call" | custom-call | tf_op jit(solution)/shard_map/pack/pallas_call | solution.py:347
  9.9 34.9 %all_to_all.20.kpool = bf16[8,864,128]{2,1,0:T(8,128)(2,1)S(1)} all-to-all(bf16[8,864,128]{2,1,0:T(8,128)(2,1)S(1)} %get-tuple-element.17), channel_id=1, replica_groups={{0,64,128,192,256,320,384,448},{2,66,130,194,258,322,386,450},{4,68,132..., dimensions={0} | all-to-all | bytes 3538944 | tf_op jit(solution)/shard_map/all_to_all | solution.py:302
  46.0 27.6 %all_gather.9 = bf16[2048,128]{1,0:T(8,128)(2,1)S(1)} all-gather(bf16[256,128]{1,0:T(8,128)(2,1)S(1)} %get-tuple-element.16), channel_id=1, replica_groups={{0,8,16,24,32,40,48,56},{2,10,18,26,34,42,50,58},{4,12,20,28,36,44,52,6..., dimensions={0}, use_global_device_ids=true | all-gather | bytes 589824 | tf_op jit(solution)/shard_map/all_gather | solution.py:306
  73.6 6.1 %attend.1 = bf16[8,528,128]{2,1,0:T(8,128)(2,1)} custom-call(s32[6]{0:T(128)S(1)} %broadcast_select_fusion.plan, bf16[8,256,128]{2,1,0:T(8,128)(2,1)S(1)} %bitcast.14, bf16[8,864,128]{2,1,0:T(8,128)(2,1)S(1)} %all_to_all.20.kpool), custom_call_target="tpu_custom_call" | custom-call | tf_op jit(solution)/shard_map/attend/pallas_call | solution.py:370
  79.7 5.6 %all-to-all-start.1 = ((bf16[8,528,128]{2,1,0:T(8,128)(2,1)}), bf16[8,528,128]{2,1,0:T(8,128)(2,1)S(1)}, u32[]{:S(2)}, u32[]{:S(2)}) async-start(bf16[8,528,128]{2,1,0:T(8,128)(2,1)} %attend.1), calls=%async_computation.1 | async-start | bytes 2162688 | tf_op jit(solution)/shard_map/all_to_all | solution.py:302
  85.3 3.4 %collective-permute-start = (bf16[256,2048]{1,0:T(8,128)(2,1)}, bf16[256,2048]{1,0:T(8,128)(2,1)S(1)}, u32[]{:S(2)}, u32[]{:S(2)}) collective-permute-start(bf16[256,2048]{1,0:T(8,128)(2,1)} %refs_0_.1), channel_id=1, source_target_pairs={{0,2},{2,4},{4,6},{6,0},{1,3},{3,5},{5,7},{7,1},{8,10},{10,12},{12... | collective-permute-start | bytes 3145736 | tf_op jit(solution)/shard_map/ppermute | solution.py:345
  88.7 3.7 %collective-permute-start.1 = (bf16[256,2048]{1,0:T(8,128)(2,1)}, bf16[256,2048]{1,0:T(8,128)(2,1)S(1)}, u32[]{:S(2)}, u32[]{:S(2)}) collective-permute-start(bf16[256,2048]{1,0:T(8,128)(2,1)} %refs_0_.1), channel_id=1, source_target_pairs={{0,6},{2,0},{4,2},{6,4},{1,7},{3,1},{5,3},{7,5},{8,14},{10,8},{12,... | collective-permute-start | bytes 3145736 | tf_op jit(solution)/shard_map/ppermute | solution.py:346
  92.4 33.6 %all_gather.10.residual = bf16[128,2048]{1,0:T(8,128)(2,1)} all-gather(bf16[16,2048]{1,0:T(8,128)(2,1)S(1)} %copy-done.6), channel_id=1, replica_groups=mesh['z'=8,'y'=8,'x'=4,'core'=2] {'x','core'}, dimensions={0}, use_global_device_ids=true | all-gather | bytes 589824 | tf_op jit(solution)/shard_map/all_gather | solution.py:306
  126.8 3.5 %collective-permute-start.2 = (bf16[128,2048]{1,0:T(8,128)(2,1)}, bf16[128,2048]{1,0:T(8,128)(2,1)}, u32[]{:S(2)}, u32[]{:S(2)}) collective-permute-start(bf16[128,2048]{1,0:T(8,128)(2,1)} %slice.15), channel_id=1, source_target_pairs={{0,2},{2,4},{4,6},{6,0},{1,3},{3,5},{5,7},{7,1},{8,10},{10,12},{12... | collective-permute-start | bytes 1572872 | tf_op jit(solution)/shard_map/ppermute | solution.py:388
  131.2 3.5 %collective-permute-start.3 = (bf16[128,2048]{1,0:T(8,128)(2,1)}, bf16[128,2048]{1,0:T(8,128)(2,1)}, u32[]{:S(2)}, u32[]{:S(2)}) collective-permute-start(bf16[128,2048]{1,0:T(8,128)(2,1)} %slice.16), channel_id=1, source_target_pairs={{0,6},{2,0},{4,2},{6,4},{1,7},{3,1},{5,3},{7,5},{8,14},{10,8},{12,... | collective-permute-start | bytes 1572872 | tf_op jit(solution)/shard_map/ppermute | solution.py:389
  135.4 1.3 join.1
  136.7 3.4 %all-to-all-start.2 = ((bf16[4,128,256]{2,1,0:T(8,128)(2,1)}), bf16[4,128,256]{2,1,0:T(8,128)(2,1)S(1)}, u32[]{:S(2)}, u32[]{:S(2)}) async-start(bf16[4,128,256]{2,1,0:T(8,128)(2,1)} %join.1), calls=%async_computation.2 | async-start | bytes 524288 | tf_op jit(solution)/shard_map/all_to_all | solution.py:302
  140.2 4.6 %collective-permute-done.2.refs_3_ = bf16[128,2048]{1,0:T(8,128)(2,1)} collective-permute-done((bf16[128,2048]{1,0:T(8,128)(2,1)}, bf16[128,2048]{1,0:T(8,128)(2,1)}, u32[]{:S(2)}, u32[]{:S(2)}) %collective-permute-start.2) | collective-permute-done | bytes 524320 | tf_op jit(solution)/shard_map/ppermute | solution.py:388
  144.8 3.4 %collective-permute-done.3.refs_4_ = bf16[128,2048]{1,0:T(8,128)(2,1)} collective-permute-done((bf16[128,2048]{1,0:T(8,128)(2,1)}, bf16[128,2048]{1,0:T(8,128)(2,1)}, u32[]{:S(2)}, u32[]{:S(2)}) %collective-permute-start.3) | collective-permute-done | bytes 524320 | tf_op jit(solution)/shard_map/ppermute | solution.py:389
  148.2 1.1 all-to-all-done.2.heads
  149.3 2.7 %project.1 = (f32[128,2048]{1,0:T(8,128)S(1)}, bf16[128,2048]{1,0:T(8,128)(2,1)S(1)}) custom-call(s32[3]{0:T(128)S(1)} %pad_add_fusion.place.core, bf16[4,128,256]{2,1,0:T(8,128)(2,1)S(1)} %all-to-all-done.2.heads, bf16[256,2048]{1,0:T(8,128)(2,1)} %refs_0_.1, bf16[256,2048]{1,0:T(8,128)(2,1)S(1)} %collective-permute-done.refs_1_, ...), custom_call_target="tpu_custom_call" | custom-call | tf_op jit(solution)/shard_map/project/pallas_call | solution.py:400
  153.0 1.9 collective-permute-start.4
  155.1 1.8 collective-permute-done.4.other
  156.8 1.2 copy-done.3
  158.0 2.9 %gate.3 = (bf16[128,768]{1,0:T(8,128)(2,1)S(1)}, bf16[16,768]{1,0:T(8,128)(2,1)S(1)}, bf16[128,2048]{1,0:T(8,128)(2,1)S(1)}, f32[16,2048]{1,0:T(8,128)S(1)}) custom-call(s32[3]{0:T(128)S(1)} %pad_add_fusion.place.core, f32[128,2048]{1,0:T(8,128)S(1)} %copy-done.3, bf16[128,2048]{1,0:T(8,128)(2,1)S(1)} %collective-permute-done.4.other, ...), custom_call_target="tpu_custom_call" | custom-call | tf_op jit(solution)/shard_map/gate/pallas_call | solution.py:413
  160.9 1.9 collective-permute-start.5
  162.8 3.6 %lift.3.lifted = bf16[128,640]{1,0:T(8,128)(2,1)S(1)} custom-call(s32[3]{0:T(128)S(1)} %pad_add_fusion.place.core, bf16[128,2048]{1,0:T(8,128)(2,1)S(1)} %get-tuple-element.24.rows, bf16[8,8,352,128]{3,2,1,0:T(8,128)(2,1)} %bitcast.18), custom_call_target="tpu_custom_call" | custom-call | flops 335544320 | bytes 3145728 | tf_op jit(solution)/shard_map/lift/pallas_call | solution.py:432
  166.4 2.3 %collective-permute-done.5.prior = bf16[16,768]{1,0:T(8,128)(2,1)S(1)} collective-permute-done((bf16[16,768]{1,0:T(8,128)(2,1)S(1)}, bf16[16,768]{1,0:T(8,128)(2,1)S(1)}, u32[]{:S(2)}, u32[]{:S(2)}) %collective-permute-start.5) | collective-permute-done | bytes 24608 | tf_op jit(solution)/shard_map/ppermute | solution.py:431
  169.7 15.0 %all_to_all.21.parts = bf16[8,16,2048]{2,1,0:T(8,128)(2,1)S(1)} all-to-all(bf16[8,16,2048]{2,1,0:T(8,128)(2,1)S(1)} %bitcast.13), channel_id=1, replica_groups=mesh['z'=8,'y'=8,'x'=4,'core'=2] {'x','core'}, dimensions={0} | all-to-all | bytes 1048576 | tf_op jit(solution)/shard_map/all_to_all | solution.py:302
  (35 shorter events, 5.6 us)
Async XLA Ops:
  6.5 150.3 %all-gather.2.cloned.1.call-start = ((), (), s32[]{:S(2)}) async-start(), calls=%async_computation.4 | async-start | bytes 6488064 | tf_op jit(solution)/shard_map/all_gather | solution.py:306
  79.7 12.7 %copy-start.6 = (bf16[16,2048]{1,0:T(8,128)(2,1)S(1)}, bf16[16,2048]{1,0:T(8,128)(2,1)}, u32[]{:S(2)}) copy-start(bf16[16,2048]{1,0:T(8,128)(2,1)} %param.21) | copy-start | bytes 196612
  79.7 55.7 %all-to-all-start.1 = ((bf16[8,528,128]{2,1,0:T(8,128)(2,1)}), bf16[8,528,128]{2,1,0:T(8,128)(2,1)S(1)}, u32[]{:S(2)}, u32[]{:S(2)}) async-start(bf16[8,528,128]{2,1,0:T(8,128)(2,1)} %attend.1), calls=%async_computation.1 | async-start | bytes 2162688 | tf_op jit(solution)/shard_map/all_to_all | solution.py:302
  85.3 50.1 %copy-start.5 = (f32[256]{0:T(256)S(1)}, f32[256]{0:T(256)}, u32[]{:S(2)}) copy-start(f32[256]{0:T(256)} %param.20) | copy-start | bytes 3076
  85.3 40.7 %collective-permute-start = (bf16[256,2048]{1,0:T(8,128)(2,1)}, bf16[256,2048]{1,0:T(8,128)(2,1)S(1)}, u32[]{:S(2)}, u32[]{:S(2)}) collective-permute-start(bf16[256,2048]{1,0:T(8,128)(2,1)} %refs_0_.1), channel_id=1, source_target_pairs={{0,2},{2,4},{4,6},{6,0},{1,3},{3,5},{5,7},{7,1},{8,10},{10,12},{12... | collective-permute-start | bytes 3145736 | tf_op jit(solution)/shard_map/ppermute | solution.py:345
  88.7 37.3 %collective-permute-start.1 = (bf16[256,2048]{1,0:T(8,128)(2,1)}, bf16[256,2048]{1,0:T(8,128)(2,1)S(1)}, u32[]{:S(2)}, u32[]{:S(2)}) collective-permute-start(bf16[256,2048]{1,0:T(8,128)(2,1)} %refs_0_.1), channel_id=1, source_target_pairs={{0,6},{2,0},{4,2},{6,4},{1,7},{3,1},{5,3},{7,5},{8,14},{10,8},{12,... | collective-permute-start | bytes 3145736 | tf_op jit(solution)/shard_map/ppermute | solution.py:346
  126.8 18.0 %collective-permute-start.2 = (bf16[128,2048]{1,0:T(8,128)(2,1)}, bf16[128,2048]{1,0:T(8,128)(2,1)}, u32[]{:S(2)}, u32[]{:S(2)}) collective-permute-start(bf16[128,2048]{1,0:T(8,128)(2,1)} %slice.15), channel_id=1, source_target_pairs={{0,2},{2,4},{4,6},{6,0},{1,3},{3,5},{5,7},{7,1},{8,10},{10,12},{12... | collective-permute-start | bytes 1572872 | tf_op jit(solution)/shard_map/ppermute | solution.py:388
  131.2 17.0 %collective-permute-start.3 = (bf16[128,2048]{1,0:T(8,128)(2,1)}, bf16[128,2048]{1,0:T(8,128)(2,1)}, u32[]{:S(2)}, u32[]{:S(2)}) collective-permute-start(bf16[128,2048]{1,0:T(8,128)(2,1)} %slice.16), channel_id=1, source_target_pairs={{0,6},{2,0},{4,2},{6,4},{1,7},{3,1},{5,3},{7,5},{8,14},{10,8},{12,... | collective-permute-start | bytes 1572872 | tf_op jit(solution)/shard_map/ppermute | solution.py:389
  136.7 12.6 %all-to-all-start.2 = ((bf16[4,128,256]{2,1,0:T(8,128)(2,1)}), bf16[4,128,256]{2,1,0:T(8,128)(2,1)S(1)}, u32[]{:S(2)}, u32[]{:S(2)}) async-start(bf16[4,128,256]{2,1,0:T(8,128)(2,1)} %join.1), calls=%async_computation.2 | async-start | bytes 524288 | tf_op jit(solution)/shard_map/all_to_all | solution.py:302
  140.2 14.7 %slice-start = ((f32[3,704]{1,0:T(4,128)}), f32[3,640]{1,0:T(4,128)S(1)}, s32[]{:S(2)}) async-start(f32[3,704]{1,0:T(4,128)} %param.26), calls=%async_computation.5 | async-start | bytes 20480 | tf_op jit(solution)/shard_map/slice | solution.py:448
  140.2 14.7 %slice-start.1 = ((f32[3,704]{1,0:T(4,128)}), f32[3,64]{1,0:T(4,128)S(1)}, s32[]{:S(2)}) async-start(f32[3,704]{1,0:T(4,128)} %param.26), calls=%async_computation.6 | async-start | bytes 4096 | tf_op jit(solution)/shard_map/slice | solution.py:448
  140.2 16.6 %copy-start.1 = (bf16[128,2048]{1,0:T(8,128)(2,1)S(1)}, bf16[128,2048]{1,0:T(8,128)(2,1)}, u32[]{:S(2)}) copy-start(bf16[128,2048]{1,0:T(8,128)(2,1)} %all_gather.10.residual) | copy-start | bytes 1572868
  140.2 16.6 %copy-start.4 = (f32[2048]{0:T(1024)S(1)}, f32[2048]{0:T(1024)}, u32[]{:S(2)}) copy-start(f32[2048]{0:T(1024)} %param.23) | copy-start | bytes 24580
  152.0 1.0 copy-start.2
  153.0 3.8 %collective-permute-start.4 = (bf16[128,2048]{1,0:T(8,128)(2,1)S(1)}, bf16[128,2048]{1,0:T(8,128)(2,1)S(1)}, u32[]{:S(2)}, u32[]{:S(2)}) collective-permute-start(bf16[128,2048]{1,0:T(8,128)(2,1)S(1)} %get-tuple-element.21), channel_id=1, source_target_pairs={{0,1},{1,0},{2,3},{3,2},{4,5},{5,4},{6,7},{7,6},{8,9},{9,8},{10,11... | collective-permute-start | bytes 1572872 | tf_op jit(solution)/shard_map/ppermute | solution.py:412
  156.8 1.2 copy-start.3
  160.9 7.8 %collective-permute-start.5 = (bf16[16,768]{1,0:T(8,128)(2,1)S(1)}, bf16[16,768]{1,0:T(8,128)(2,1)S(1)}, u32[]{:S(2)}, u32[]{:S(2)}) collective-permute-start(bf16[16,768]{1,0:T(8,128)(2,1)S(1)} %get-tuple-element.25), channel_id=1, source_target_pairs={{0,8},{8,16},{16,24},{24,32},{32,40},{40,48},{48,56},{56,64},{64,7... | collective-permute-start | bytes 73736 | tf_op jit(solution)/shard_map/ppermute | solution.py:431
  162.8 5.9 %copy-start = (bf16[704,2048]{1,0:T(8,128)(2,1)S(1)}, bf16[704,2048]{1,0:T(8,128)(2,1)}, u32[]{:S(2)}) copy-start(bf16[704,2048]{1,0:T(8,128)(2,1)} %weight.1) | copy-start | bytes 8650756
Sparse Core Ops, SparseCore 0:
  45.9 46.7 all-gather.1

commit v6 on v5

--- a/solution.py
+++ b/solution.py
@@ -162,7 +162,7 @@
     lax.fori_loop(first_chunk, SIDE // 2, chunk, 0)
 
 
-def join_kernel(mix, parts, gain, out):
+def join_kernel(mix, parts, gain, residual, out):
     tails = [parts[i, 512:528, :].astype(f32) for i in range(SIDE)]
 
     def joined(m):
@@ -185,7 +185,17 @@
     r = lax.rsqrt(jnp.mean(mixed * mixed, axis=-1, keepdims=True) + epsilon)
     head = (mixed * r * gain[...]).astype(bf16)
     for i in range(4):
-        out[i] = head
+        out[i, 0:128] = head
+        for j in range(8):
+            out[i, 128 + 16 * j : 144 + 16 * j, :] = residual[:, 256 * j : 256 * j + 256]
+
+
+def own_rows(place, i):
+    return pl.ds(pl.multiple_of(32 * i + 16 * place[0], 16), 16)
+
+
+def other_rows(place, i):
+    return pl.ds(pl.multiple_of(32 * i + 16 - 16 * place[0], 16), 16)
 
 
 def project_kernel(place, heads, *refs):
@@ -202,14 +212,18 @@
         moves[i].wait()
         if i == 3:
             moves[4].wait()
-        head = heads[lax.rem(x + 4 - shift, 4)]
+        head = heads[lax.rem(x + 4 - shift, 4), 0:128]
         for n in range(0, 2048, 256):
             d = jnp.dot(head, buffer[i, :, n : n + 256], preferred_element_type=f32)
             if i > 0:
                 d = d + half[:, n : n + 256]
             half[:, n : n + 256] = d
-            if i == 3:
-                sent[:, n : n + 256] = d.astype(bf16)
+    for i in range(4):
+        rows = own_rows(place, i)
+        for j in range(8):
+            r = heads[i, 128 + 16 * j : 144 + 16 * j, :].astype(f32)
+            half[rows, 256 * j : 256 * j + 256] = half[rows, 256 * j : 256 * j + 256] + r
+    sent[...] = half[...].astype(bf16)
 
 
 def fetched(core, weights, buffer, sems, first):
@@ -246,16 +260,14 @@
     return acc
 
 
-def gate_kernel(place, half, other, residual, gain, weights, gated, edge, rows, stream, buffer, sems):
+def gate_kernel(place, half, other, gain, weights, gated, edge, rows, stream, buffer, sems):
     fetched(place[0], weights, buffer, sems, 0)
     for n in range(0, 128, 32):
-        total = residual[n : n + 32].astype(f32) + (
-            half[n : n + 32] + other[n : n + 32].astype(f32)
-        )
+        total = half[n : n + 32] + other[n : n + 32].astype(f32)
         r = lax.rsqrt(jnp.mean(total * total, axis=-1, keepdims=True) + epsilon)
         rows[n : n + 32] = (total * r * gain[...]).astype(bf16)
     own = pl.ds(pl.multiple_of(place[2] * 16, 16), 16)
-    stream[...] = residual[own].astype(f32) + (half[own] + other[own].astype(f32))
+    stream[...] = half[own] + other[own].astype(f32)
     for n, part in enumerate(multiplied(rows, weights, buffer, sems, 0)):
         part = part.astype(bf16)
         gated[:, 256 * n : 256 * n + 256] = part
@@ -268,7 +280,7 @@
         lifted[:, 256 * n : 256 * n + part.shape[1]] = part.astype(bf16)
 
 
-def down_kernel(gated, lifted, prior, taps, weight, out):
+def down_kernel(place, gated, lifted, prior, taps, weight, keep, give, whole):
     at = lax.broadcasted_iota(jnp.int32, (128, 1), 0)
 
     def activated(lo, hi):
@@ -287,13 +299,21 @@
         acc = d if acc is None else acc + d
     g, a = activated(MAIN, MAIN + 128)
     h = (pltpu.roll(a, 64, 1) * g).astype(bf16)
-    acc = acc + jnp.dot(h[:, 0:64], weight[MAIN:, :], preferred_element_type=f32)
-    out[...] = acc.astype(bf16)
+    whole[...] = acc + jnp.dot(h[:, 0:64], weight[MAIN:, :], preferred_element_type=f32)
+    for i in range(4):
+        keep[16 * i : 16 * i + 16] = whole[own_rows(place, i)]
+        give[16 * i : 16 * i + 16] = whole[other_rows(place, i)].astype(bf16)
+
+
+def pair_kernel(keep, other, out):
+    for i in range(4):
+        rows = slice(16 * i, 16 * i + 16)
+        out[i] = (keep[rows] + other[rows].astype(f32)).astype(bf16)
 
 
 def last_kernel(parts, stream, out):
     mixer = parts[0].astype(f32)
-    for i in range(1, 8):
+    for i in range(1, 4):
         mixer = mixer + parts[i].astype(f32)
     out[...] = (stream[...] + mixer).astype(bf16)
 
@@ -342,8 +362,6 @@
     hbm = pl.BlockSpec(memory_space=pltpu.HBM)
     x = lax.axis_index("x")
     place = jnp.stack([core, x, 2 * x + core]).astype(jnp.int32)
-    above = lax.ppermute(out_weight, "x", [(i, (i + 1) % 4) for i in range(4)])
-    below = lax.ppermute(out_weight, "x", [(i, (i + 3) % 4) for i in range(4)])
     qsend, ksend = pl.pallas_call(
         pack_kernel,
         out_shape=[
@@ -366,36 +384,38 @@
     kpool = swapped(ksend, ALL, K_GROUPS)
     qpool = gathered(qsend, ALL, Q_GROUPS).reshape(SIDE, 256, 128)
     part = kpool[:, 512:, :].reshape(SIDE * 352, 128)
+    own_rows_sent, qpool, part = lax.optimization_barrier((out_weight, qpool, part))
     weights = in_hbm(gathered(part, ALL, Q_GROUPS).reshape(SIDE, SIDE, 352, 128))
-    out = pl.pallas_call(
-        attend_kernel,
-        grid=(1,),
-        out_shape=jax.ShapeDtypeStruct((SIDE, PACK, 128), bf16),
-        in_specs=[
-            pl.BlockSpec(memory_space=pltpu.SMEM),
-            vmem(),
-            pl.BlockSpec((SIDE, 512, 128), lambda i: (0, 0, 0)),
-        ],
-        out_specs=vmem(),
-        scratch_shapes=[pltpu.VMEM((8, 256, 256), f32)],
-        compiler_params=SMALL,
-        name="attend",
-    )(plan, qpool, kpool)
+    above = lax.ppermute(own_rows_sent, "x", [(i, (i + 1) % 4) for i in range(4)])
+    below = lax.ppermute(own_rows_sent, "x", [(i, (i + 3) % 4) for i in range(4)])
+    run = pl.pallas_call(
+    attend_kernel,
+    grid=(1,),
+    out_shape=jax.ShapeDtypeStruct((SIDE, PACK, 128), bf16),
+    in_specs=[
+        pl.BlockSpec(memory_space=pltpu.SMEM),
+        vmem(),
+        pl.BlockSpec((SIDE, 512, 128), lambda i: (0, 0, 0)),
+    ],
+    out_specs=vmem(),
+    scratch_shapes=[pltpu.VMEM((8, 256, 256), f32)],
+    compiler_params=SMALL,
+    name="attend",
+    )
+    out = run(plan, qpool, kpool)
     back = swapped(out, ALL, Q_GROUPS)
-    before = gathered(residual, TP)
-    above, below, before = lax.optimization_barrier((above, below, before))
     across = (
         lax.ppermute(above[0:128], "x", [(i, (i + 1) % 4) for i in range(4)]),
         lax.ppermute(below[128:256], "x", [(i, (i + 3) % 4) for i in range(4)]),
     )
     heads = pl.pallas_call(
         join_kernel,
-        out_shape=jax.ShapeDtypeStruct((4, tokens, VD), bf16),
-        in_specs=[pl.BlockSpec(memory_space=pltpu.SMEM)] + [vmem()] * 2,
+        out_shape=jax.ShapeDtypeStruct((4, 2 * tokens, VD), bf16),
+        in_specs=[pl.BlockSpec(memory_space=pltpu.SMEM)] + [vmem()] * 3,
         out_specs=vmem(),
         compiler_params=SMALL,
         name="join",
-    )(mix_weight, back, head_gain.reshape(1, VD))
+    )(mix_weight, back, head_gain.reshape(1, VD), residual)
     heads = swapped(heads, "x")
     half, sent = pl.pallas_call(
         project_kernel,
@@ -408,7 +428,7 @@
         scratch_shapes=[pltpu.VMEM((4, VD, 2048), bf16), pltpu.SemaphoreType.DMA((5,))],
         compiler_params=SMALL,
         name="project",
-    )(place, heads, in_hbm(out_weight), above, below, *across)
+    )(place, heads, in_hbm(out_weight), above, below, *(in_hbm(a) for a in across))
     other = lax.ppermute(sent, "core", [(0, 1), (1, 0)])
     gated, edge, rows, stream = pl.pallas_call(
         gate_kernel,
@@ -418,7 +438,7 @@
             jax.ShapeDtypeStruct((tokens, width), bf16),
             jax.ShapeDtypeStruct((own, width), f32),
         ],
-        in_specs=[smem] + [vmem()] * 4 + [hbm],
+        in_specs=[smem] + [vmem()] * 3 + [hbm],
         out_specs=[vmem()] * 4,
         scratch_shapes=[
             pltpu.VMEM((SIDE, SIDE, 192, 128), bf16),
@@ -426,7 +446,7 @@
         ],
         compiler_params=SMALL,
         name="gate",
-    )(place, half, other, before, norm_gain.reshape(1, width), weights)
+    )(place, half, other, norm_gain.reshape(1, width), weights)
     route = [(i, i + 1) for i in range(SIDE * SIDE - 1)]
     prior = lax.ppermute(edge, ("z", "y"), route)
     lifted = pl.pallas_call(
@@ -446,15 +466,28 @@
     )(place, rows, weights)
     gap = jnp.zeros((WIDTH, 64), f32)
     taps = jnp.concatenate([conv_taps[:, :MAIN], gap, conv_taps[:, MAIN:]], axis=1)
-    down = pl.pallas_call(
+    keep, give = pl.pallas_call(
         down_kernel,
-        out_shape=jax.ShapeDtypeStruct((tokens, width), bf16),
-        in_specs=[vmem()] * 5,
+        out_shape=[
+            jax.ShapeDtypeStruct((tokens // 2, width), f32),
+            jax.ShapeDtypeStruct((tokens // 2, width), bf16),
+        ],
+        in_specs=[smem] + [vmem()] * 5,
+        out_specs=[vmem()] * 2,
+        scratch_shapes=[pltpu.VMEM((128, 2048), f32)],
+        compiler_params=SMALL,
+        name="down",
+    )(place, gated, lifted, prior, taps, down_weight)
+    taken = lax.ppermute(give, "core", [(0, 1), (1, 0)])
+    pair = pl.pallas_call(
+        pair_kernel,
+        out_shape=jax.ShapeDtypeStruct((4, own, width), bf16),
+        in_specs=[vmem()] * 2,
         out_specs=vmem(),
         compiler_params=SMALL,
-        name="down",
-    )(gated, lifted, prior, taps, down_weight)
-    mixer = swapped(down.reshape(8, own, width), TP)
+        name="pair",
+    )(keep, taken)
+    mixer = swapped(pair, "x")
     return pl.pallas_call(
         last_kernel,
         out_shape=jax.ShapeDtypeStruct((own, width), bf16),

time: 193 us -> 164 us (0.85)
  the two profiles are of different devices: /device:TPU:64 before, /device:TPU:24 now
where the time goes in v6:
time: 164 us
  starting transfers between devices  48.2 us (29%)
  blocking collectives  42.1 us (26%)
  waiting for transfers between devices  32.6 us (20%)
  Pallas kernels  20.6 us (13%)
  between operations  14.3 us (9%)
  local copies, waits for them, and re-layouts  5.83 us (4%)
    all_gather x1, blocking collectives, gathered(): return lax.all_gather(a, axis, axis_index_groups=groups, axis=0, tiled=True)  30.4 us
    all_to_all x3, starting transfers between devices, swapped(): return lax.all_to_all(a, axis, 0, 0, axis_index_groups=groups, tiled=True)  21.2 us
    ppermute x1, waiting for transfers between devices, on_device(): lax.ppermute(own_rows_sent, 'x', [(i, (i + 1) % 4) for i in range(4)])  20 us
    all_to_all x1, blocking collectives, swapped(): return lax.all_to_all(a, axis, 0, 0, axis_index_groups=groups, tiled=True)  11.6 us
    ppermute x1, starting transfers between devices, on_device(): prior = lax.ppermute(edge, ('z', 'y'), route)  6.13 us
    pallas_call x1, Pallas kernels, on_device(): out = run(plan, qpool, kpool)  6.05 us
    ppermute x1, starting transfers between devices, on_device(): lax.ppermute(below[128:256], 'x', [(i, (i + 3) % 4) for i in range(4)])  4.82 us
    ppermute x1, starting transfers between devices, on_device(): other = lax.ppermute(sent, 'core', [(0, 1), (1, 0)])  4.78 us
  transfers between devices with their start and end apart: 11, of which 6 were waited for; matrix products, arithmetic and copies ran while one was open for 1% of the time, Pallas kernels for 8%

profile of v6, /device:TPU:24, one launch (start us, length us, event | category | flops | bytes accessed | tf_op | source)
XLA Modules:
  0.0 163.7 jit_solution(2587891915986744615)
XLA Ops:
  6.5 2.3 %pack.1 = (bf16[256,128]{1,0:T(8,128)(2,1)S(1)}, bf16[8,864,128]{2,1,0:T(8,128)(2,1)}) custom-call(bf16[128,128]{1,0:T(8,128)(2,1)} %q1.1, bf16[128,128]{1,0:T(8,128)(2,1)} %q2.1, bf16[128,128]{1,0:T(8,128)(2,1)} %k1.1, bf16[128,128]{1,0:T(8,128)(2,1)} %k2.1, bf16[128,256]{1,0:T(8,128)(2,1)} %v.1, bf16[32,704]{1,0:T(8,128)(2,1)} %lift.2, bf16[32,704]{1,0:T(8,128)(2,1)} %gate.2), custom_call_target="tpu_custom_call" | custom-call | tf_op jit(solution)/shard_map/pack/pallas_call | solution.py:365
  8.9 10.3 %all-to-all-start = ((bf16[8,864,128]{2,1,0:T(8,128)(2,1)}), bf16[8,864,128]{2,1,0:T(8,128)(2,1)S(1)}, u32[]{:S(2)}, u32[]{:S(2)}) async-start(bf16[8,864,128]{2,1,0:T(8,128)(2,1)} %get-tuple-element.19), calls=%async_computation | async-start | bytes 3538944 | tf_op jit(solution)/shard_map/all_to_all | solution.py:322
  19.2 30.4 %all_gather.6 = bf16[2048,128]{1,0:T(8,128)(2,1)S(1)} all-gather(bf16[256,128]{1,0:T(8,128)(2,1)S(1)} %get-tuple-element.18), channel_id=1, replica_groups={{0,8,16,24,32,40,48,56},{2,10,18,26,34,42,50,58},{4,12,20,28,36,44,52,6..., dimensions={0}, use_global_device_ids=true | all-gather | bytes 589824 | tf_op jit(solution)/shard_map/all_gather | solution.py:326
  50.8 6.1 %attend.1 = bf16[8,528,128]{2,1,0:T(8,128)(2,1)} custom-call(s32[6]{0:T(128)S(1)} %broadcast_select_fusion.plan, bf16[8,256,128]{2,1,0:T(8,128)(2,1)S(1)} %bitcast.12, bf16[8,864,128]{2,1,0:T(8,128)(2,1)S(1)} %all-to-all-done.kpool), custom_call_target="tpu_custom_call" | custom-call | tf_op jit(solution)/shard_map/attend/pallas_call | solution.py:405
  56.9 7.4 %all-to-all-start.1 = ((bf16[8,528,128]{2,1,0:T(8,128)(2,1)}), bf16[8,528,128]{2,1,0:T(8,128)(2,1)S(1)}, u32[]{:S(2)}, u32[]{:S(2)}) async-start(bf16[8,528,128]{2,1,0:T(8,128)(2,1)} %attend.1), calls=%async_computation.1 | async-start | bytes 2162688 | tf_op jit(solution)/shard_map/all_to_all | solution.py:322
  64.3 3.4 %collective-permute-start = (bf16[256,2048]{1,0:T(8,128)(2,1)}, bf16[256,2048]{1,0:T(8,128)(2,1)S(1)}, u32[]{:S(2)}, u32[]{:S(2)}) collective-permute-start(bf16[256,2048]{1,0:T(8,128)(2,1)} %refs_0_.1), channel_id=1, source_target_pairs={{0,2},{2,4},{4,6},{6,0},{1,3},{3,5},{5,7},{7,1},{8,10},{10,12},{12... | collective-permute-start | bytes 3145736 | tf_op jit(solution)/shard_map/ppermute | solution.py:389
  67.7 3.6 %collective-permute-start.1 = (bf16[256,2048]{1,0:T(8,128)(2,1)}, bf16[256,2048]{1,0:T(8,128)(2,1)S(1)}, u32[]{:S(2)}, u32[]{:S(2)}) collective-permute-start(bf16[256,2048]{1,0:T(8,128)(2,1)} %refs_0_.1), channel_id=1, source_target_pairs={{0,6},{2,0},{4,2},{6,4},{1,7},{3,1},{5,3},{7,5},{8,14},{10,8},{12,... | collective-permute-start | bytes 3145736 | tf_op jit(solution)/shard_map/ppermute | solution.py:390
  71.3 20.0 %collective-permute-done.refs_1_ = bf16[256,2048]{1,0:T(8,128)(2,1)S(1)} collective-permute-done((bf16[256,2048]{1,0:T(8,128)(2,1)}, bf16[256,2048]{1,0:T(8,128)(2,1)S(1)}, u32[]{:S(2)}, u32[]{:S(2)}) %collective-permute-start) | collective-permute-done | bytes 1048608 | tf_op jit(solution)/shard_map/ppermute | solution.py:389
  92.2 2.2 %collective-permute-start.2 = (bf16[128,2048]{1,0:T(8,128)(2,1)}, bf16[128,2048]{1,0:T(8,128)(2,1)}, u32[]{:S(2)}, u32[]{:S(2)}) collective-permute-start(bf16[128,2048]{1,0:T(8,128)(2,1)} %slice.21), channel_id=1, source_target_pairs={{0,2},{2,4},{4,6},{6,0},{1,3},{3,5},{5,7},{7,1},{8,10},{10,12},{12... | collective-permute-start | bytes 1572872 | tf_op jit(solution)/shard_map/ppermute | solution.py:408
  95.2 4.8 %collective-permute-start.3 = (bf16[128,2048]{1,0:T(8,128)(2,1)}, bf16[128,2048]{1,0:T(8,128)(2,1)}, u32[]{:S(2)}, u32[]{:S(2)}) collective-permute-start(bf16[128,2048]{1,0:T(8,128)(2,1)} %slice.22), channel_id=1, source_target_pairs={{0,6},{2,0},{4,2},{6,4},{1,7},{3,1},{5,3},{7,5},{8,14},{10,8},{12,... | collective-permute-start | bytes 1572872 | tf_op jit(solution)/shard_map/ppermute | solution.py:409
  102.2 3.5 %all-to-all-start.2 = ((bf16[4,256,256]{2,1,0:T(8,128)(2,1)}), bf16[4,256,256]{2,1,0:T(8,128)(2,1)S(1)}, u32[]{:S(2)}, u32[]{:S(2)}) async-start(bf16[4,256,256]{2,1,0:T(8,128)(2,1)} %copy-done.1), calls=%async_computation.2 | async-start | bytes 1048576 | tf_op jit(solution)/shard_map/all_to_all | solution.py:322
  105.8 3.0 %collective-permute-done.2.refs_3_ = bf16[128,2048]{1,0:T(8,128)(2,1)} collective-permute-done((bf16[128,2048]{1,0:T(8,128)(2,1)}, bf16[128,2048]{1,0:T(8,128)(2,1)}, u32[]{:S(2)}, u32[]{:S(2)}) %collective-permute-start.2) | collective-permute-done | bytes 524320 | tf_op jit(solution)/shard_map/ppermute | solution.py:408
  108.8 2.6 %collective-permute-done.3.refs_4_ = bf16[128,2048]{1,0:T(8,128)(2,1)} collective-permute-done((bf16[128,2048]{1,0:T(8,128)(2,1)}, bf16[128,2048]{1,0:T(8,128)(2,1)}, u32[]{:S(2)}, u32[]{:S(2)}) %collective-permute-start.3) | collective-permute-done | bytes 524320 | tf_op jit(solution)/shard_map/ppermute | solution.py:409
  111.4 4.1 %all-to-all-done.2.heads = bf16[4,256,256]{2,1,0:T(8,128)(2,1)S(1)} async-done(((bf16[4,256,256]{2,1,0:T(8,128)(2,1)}), bf16[4,256,256]{2,1,0:T(8,128)(2,1)S(1)}, u32[]{:S(2)}, u32[]{:S(2)}) %all-to-all-start.2) | async-done | bytes 524320 | tf_op jit(solution)/shard_map/all_to_all | solution.py:322
  115.5 2.8 %project.1 = (f32[128,2048]{1,0:T(8,128)S(1)}, bf16[128,2048]{1,0:T(8,128)(2,1)S(1)}) custom-call(s32[3]{0:T(128)S(1)} %pad_add_fusion.place.core, bf16[4,256,256]{2,1,0:T(8,128)(2,1)S(1)} %all-to-all-done.2.heads, bf16[256,2048]{1,0:T(8,128)(2,1)} %refs_0_.1, bf16[256,2048]{1,0:T(8,128)(2,1)S(1)} %collective-permute-done.refs_1_, ...), custom_call_target="tpu_custom_call" | custom-call | tf_op jit(solution)/shard_map/project/pallas_call | solution.py:420
  119.4 4.8 %collective-permute-start.4 = (bf16[128,2048]{1,0:T(8,128)(2,1)S(1)}, bf16[128,2048]{1,0:T(8,128)(2,1)S(1)}, u32[]{:S(2)}, u32[]{:S(2)}) collective-permute-start(bf16[128,2048]{1,0:T(8,128)(2,1)S(1)} %get-tuple-element.23), channel_id=1, source_target_pairs={{0,1},{1,0},{2,3},{3,2},{4,5},{5,4},{6,7},{7,6},{8,9},{9,8},{10,11... | collective-permute-start | bytes 1572872 | tf_op jit(solution)/shard_map/ppermute | solution.py:432
  124.3 1.4 collective-permute-done.4.other
  126.9 2.8 %gate.3 = (bf16[128,768]{1,0:T(8,128)(2,1)S(1)}, bf16[16,768]{1,0:T(8,128)(2,1)S(1)}, bf16[128,2048]{1,0:T(8,128)(2,1)S(1)}, f32[16,2048]{1,0:T(8,128)S(1)}) custom-call(s32[3]{0:T(128)S(1)} %pad_add_fusion.place.core, f32[128,2048]{1,0:T(8,128)S(1)} %copy-done.3, bf16[128,2048]{1,0:T(8,128)(2,1)S(1)} %collective-permute-done.4.other, ...), custom_call_target="tpu_custom_call" | custom-call | tf_op jit(solution)/shard_map/gate/pallas_call | solution.py:433
  129.7 6.1 %collective-permute-start.5 = (bf16[16,768]{1,0:T(8,128)(2,1)S(1)}, bf16[16,768]{1,0:T(8,128)(2,1)S(1)}, u32[]{:S(2)}, u32[]{:S(2)}) collective-permute-start(bf16[16,768]{1,0:T(8,128)(2,1)S(1)} %get-tuple-element.27), channel_id=1, source_target_pairs={{0,8},{8,16},{16,24},{24,32},{32,40},{40,48},{48,56},{56,64},{64,7... | collective-permute-start | bytes 73736 | tf_op jit(solution)/shard_map/ppermute | solution.py:451
  135.9 3.6 %lift.3.lifted = bf16[128,640]{1,0:T(8,128)(2,1)S(1)} custom-call(s32[3]{0:T(128)S(1)} %pad_add_fusion.place.core, bf16[128,2048]{1,0:T(8,128)(2,1)S(1)} %get-tuple-element.26.rows, bf16[8,8,352,128]{3,2,1,0:T(8,128)(2,1)} %bitcast.16), custom_call_target="tpu_custom_call" | custom-call | flops 335544320 | bytes 3145728 | tf_op jit(solution)/shard_map/lift/pallas_call | solution.py:452
  139.5 1.6 down.1
  141.1 1.9 %collective-permute-start.6 = (bf16[64,2048]{1,0:T(8,128)(2,1)S(1)}, bf16[64,2048]{1,0:T(8,128)(2,1)S(1)}, u32[]{:S(2)}, u32[]{:S(2)}) collective-permute-start(bf16[64,2048]{1,0:T(8,128)(2,1)S(1)} %get-tuple-element.29), channel_id=1, source_target_pairs={{0,1},{1,0},{2,3},{3,2},{4,5},{5,4},{6,7},{7,6},{8,9},{9,8},{10,11... | collective-permute-start | bytes 786440 | tf_op jit(solution)/shard_map/ppermute | solution.py:481
  143.0 1.5 collective-permute-done.6.other
  144.6 11.6 %all_to_all.20.parts = bf16[4,16,2048]{2,1,0:T(8,128)(2,1)S(1)} all-to-all(bf16[4,16,2048]{2,1,0:T(8,128)(2,1)S(1)} %pair.1), channel_id=1, replica_groups=mesh['z'=8,'y'=8,'x'=4,'core'=2] {'x'}, dimensions={0} | all-to-all | bytes 524288 | tf_op jit(solution)/shard_map/all_to_all | solution.py:322
  (38 shorter events, 7.4 us)
Async XLA Ops:
  8.9 40.8 %all-to-all-start = ((bf16[8,864,128]{2,1,0:T(8,128)(2,1)}), bf16[8,864,128]{2,1,0:T(8,128)(2,1)S(1)}, u32[]{:S(2)}, u32[]{:S(2)}) async-start(bf16[8,864,128]{2,1,0:T(8,128)(2,1)} %get-tuple-element.19), calls=%async_computation | async-start | bytes 3538944 | tf_op jit(solution)/shard_map/all_to_all | solution.py:322
  19.2 106.5 %all-gather.2.cloned.1.call-start = ((), (), s32[]{:S(2)}) async-start(), calls=%async_computation.4 | async-start | bytes 6488064 | tf_op jit(solution)/shard_map/all_gather | solution.py:326
  56.9 43.9 %copy-start.4 = (bf16[16,2048]{1,0:T(8,128)(2,1)S(1)}, bf16[16,2048]{1,0:T(8,128)(2,1)}, u32[]{:S(2)}) copy-start(bf16[16,2048]{1,0:T(8,128)(2,1)} %residual.1) | copy-start | bytes 196612
  56.9 43.9 %copy-start.6 = (f32[256]{0:T(256)S(1)}, f32[256]{0:T(256)}, u32[]{:S(2)}) copy-start(f32[256]{0:T(256)} %param.20) | copy-start | bytes 3076
  56.9 43.8 %all-to-all-start.1 = ((bf16[8,528,128]{2,1,0:T(8,128)(2,1)}), bf16[8,528,128]{2,1,0:T(8,128)(2,1)S(1)}, u32[]{:S(2)}, u32[]{:S(2)}) async-start(bf16[8,528,128]{2,1,0:T(8,128)(2,1)} %attend.1), calls=%async_computation.1 | async-start | bytes 2162688 | tf_op jit(solution)/shard_map/all_to_all | solution.py:322
  64.3 27.0 %collective-permute-start = (bf16[256,2048]{1,0:T(8,128)(2,1)}, bf16[256,2048]{1,0:T(8,128)(2,1)S(1)}, u32[]{:S(2)}, u32[]{:S(2)}) collective-permute-start(bf16[256,2048]{1,0:T(8,128)(2,1)} %refs_0_.1), channel_id=1, source_target_pairs={{0,2},{2,4},{4,6},{6,0},{1,3},{3,5},{5,7},{7,1},{8,10},{10,12},{12... | collective-permute-start | bytes 3145736 | tf_op jit(solution)/shard_map/ppermute | solution.py:389
  67.7 26.7 %collective-permute-start.1 = (bf16[256,2048]{1,0:T(8,128)(2,1)}, bf16[256,2048]{1,0:T(8,128)(2,1)S(1)}, u32[]{:S(2)}, u32[]{:S(2)}) collective-permute-start(bf16[256,2048]{1,0:T(8,128)(2,1)} %refs_0_.1), channel_id=1, source_target_pairs={{0,6},{2,0},{4,2},{6,4},{1,7},{3,1},{5,3},{7,5},{8,14},{10,8},{12,... | collective-permute-start | bytes 3145736 | tf_op jit(solution)/shard_map/ppermute | solution.py:390
  92.2 16.6 %collective-permute-start.2 = (bf16[128,2048]{1,0:T(8,128)(2,1)}, bf16[128,2048]{1,0:T(8,128)(2,1)}, u32[]{:S(2)}, u32[]{:S(2)}) collective-permute-start(bf16[128,2048]{1,0:T(8,128)(2,1)} %slice.21), channel_id=1, source_target_pairs={{0,2},{2,4},{4,6},{6,0},{1,3},{3,5},{5,7},{7,1},{8,10},{10,12},{12... | collective-permute-start | bytes 1572872 | tf_op jit(solution)/shard_map/ppermute | solution.py:408
  95.2 16.1 %collective-permute-start.3 = (bf16[128,2048]{1,0:T(8,128)(2,1)}, bf16[128,2048]{1,0:T(8,128)(2,1)}, u32[]{:S(2)}, u32[]{:S(2)}) collective-permute-start(bf16[128,2048]{1,0:T(8,128)(2,1)} %slice.22), channel_id=1, source_target_pairs={{0,6},{2,0},{4,2},{6,4},{1,7},{3,1},{5,3},{7,5},{8,14},{10,8},{12,... | collective-permute-start | bytes 1572872 | tf_op jit(solution)/shard_map/ppermute | solution.py:409
  101.4 0.8 copy-start.1
  102.2 13.3 %all-to-all-start.2 = ((bf16[4,256,256]{2,1,0:T(8,128)(2,1)}), bf16[4,256,256]{2,1,0:T(8,128)(2,1)S(1)}, u32[]{:S(2)}, u32[]{:S(2)}) async-start(bf16[4,256,256]{2,1,0:T(8,128)(2,1)} %copy-done.1), calls=%async_computation.2 | async-start | bytes 1048576 | tf_op jit(solution)/shard_map/all_to_all | solution.py:322
  105.8 18.4 %slice-start = ((f32[3,704]{1,0:T(4,128)}), f32[3,640]{1,0:T(4,128)S(1)}, s32[]{:S(2)}) async-start(f32[3,704]{1,0:T(4,128)} %param.26), calls=%async_computation.5 | async-start | bytes 20480 | tf_op jit(solution)/shard_map/slice | solution.py:468
  105.8 18.4 %slice-start.1 = ((f32[3,704]{1,0:T(4,128)}), f32[3,64]{1,0:T(4,128)S(1)}, s32[]{:S(2)}) async-start(f32[3,704]{1,0:T(4,128)} %param.26), calls=%async_computation.6 | async-start | bytes 4096 | tf_op jit(solution)/shard_map/slice | solution.py:468
  105.8 19.9 %copy-start.5 = (f32[2048]{0:T(1024)S(1)}, f32[2048]{0:T(1024)}, u32[]{:S(2)}) copy-start(f32[2048]{0:T(1024)} %param.23) | copy-start | bytes 24580
  118.4 1.0 copy-start.2
  119.4 6.3 %collective-permute-start.4 = (bf16[128,2048]{1,0:T(8,128)(2,1)S(1)}, bf16[128,2048]{1,0:T(8,128)(2,1)S(1)}, u32[]{:S(2)}, u32[]{:S(2)}) collective-permute-start(bf16[128,2048]{1,0:T(8,128)(2,1)S(1)} %get-tuple-element.23), channel_id=1, source_target_pairs={{0,1},{1,0},{2,3},{3,2},{4,5},{5,4},{6,7},{7,6},{8,9},{9,8},{10,11... | collective-permute-start | bytes 1572872 | tf_op jit(solution)/shard_map/ppermute | solution.py:432
  125.7 1.2 copy-start.3
  129.7 9.7 %collective-permute-start.5 = (bf16[16,768]{1,0:T(8,128)(2,1)S(1)}, bf16[16,768]{1,0:T(8,128)(2,1)S(1)}, u32[]{:S(2)}, u32[]{:S(2)}) collective-permute-start(bf16[16,768]{1,0:T(8,128)(2,1)S(1)} %get-tuple-element.27), channel_id=1, source_target_pairs={{0,8},{8,16},{16,24},{24,32},{32,40},{40,48},{48,56},{56,64},{64,7... | collective-permute-start | bytes 73736 | tf_op jit(solution)/shard_map/ppermute | solution.py:451
  135.9 3.6 %copy-start = (bf16[704,2048]{1,0:T(8,128)(2,1)S(1)}, bf16[704,2048]{1,0:T(8,128)(2,1)}, u32[]{:S(2)}) copy-start(bf16[704,2048]{1,0:T(8,128)(2,1)} %weight.1) | copy-start | bytes 8650756
  141.1 3.4 %collective-permute-start.6 = (bf16[64,2048]{1,0:T(8,128)(2,1)S(1)}, bf16[64,2048]{1,0:T(8,128)(2,1)S(1)}, u32[]{:S(2)}, u32[]{:S(2)}) collective-permute-start(bf16[64,2048]{1,0:T(8,128)(2,1)S(1)} %get-tuple-element.29), channel_id=1, source_target_pairs={{0,1},{1,0},{2,3},{3,2},{4,5},{5,4},{6,7},{7,6},{8,9},{9,8},{10,11... | collective-permute-start | bytes 786440 | tf_op jit(solution)/shard_map/ppermute | solution.py:481
Sparse Core Ops, SparseCore 0:
  50.7 57.5 all-gather.1

commit v7 on v5

--- a/solution.py
+++ b/solution.py
@@ -68,78 +68,31 @@
         copy.wait()
 
 
-def attend_kernel(plan, qpool, kpool, out, scores):
+def attend_kernel(plan, qpool, kpool, out):
     q_base, q_step, k_base, k_step = (plan[i] for i in range(4))
-    first_chunk, pairs = plan[4], plan[5]
-    row = lax.broadcasted_iota(jnp.int32, (256, 256), 0)
-    col = lax.broadcasted_iota(jnp.int32, (256, 256), 1)
     at = lax.broadcasted_iota(jnp.int32, (16, 128), 0)
-
-    def blank(c, carry):
-        for h in range(2):
-            out[2 * c + h, 0:512, :] = jnp.zeros((512, 128), bf16)
-            level = jnp.where((at == 0) | (at == 3), masked_score, 0.0)
-            out[2 * c + h, 512:528, :] = level.astype(bf16)
-        return carry
-
-    lax.fori_loop(0, first_chunk, blank, 0)
-
-    def chunk(c, carry):
-        queries = [
-            jnp.concatenate(
-                [qpool[2 * c, 128 * m : 128 * m + 128, :], qpool[2 * c + 1, 128 * m : 128 * m + 128, :]],
-                axis=0,
-            )
-            for m in range(2)
-        ]
+    row = lax.broadcasted_iota(jnp.int32, (256, 1), 0)
+    col = lax.broadcasted_iota(jnp.int32, (1, 1024), 1)
+    k_at = 2 * (k_base + k_step * (col // 128)) + (col % 128) // STRETCH
+    vals = jnp.concatenate(
+        [kpool[:, 256:384, :].reshape(1024, 128), kpool[:, 384:512, :].reshape(1024, 128)], axis=1
+    )
+    for c in range(SIDE // 2):
         q_at = 2 * (q_base + q_step * (2 * c + row // 128)) + (row % 128) // STRETCH
-
-        def scored(p, peaks):
-            k_at = 2 * (k_base + k_step * (2 * p + col // 128)) + (col % 128) // STRETCH
-            seen = k_at <= q_at
-            new = []
-            for m in range(2):
-                k = jnp.concatenate(
-                    [kpool[2 * p, 128 * m : 128 * m + 128, :], kpool[2 * p + 1, 128 * m : 128 * m + 128, :]],
-                    axis=0,
-                )
-                s = lax.dot_general(
-                    queries[m], k, (((1,), (1,)), ((), ())), preferred_element_type=f32
-                )
-                s = jnp.where(seen, s, masked_score)
-                scores[2 * p + m] = s
-                new.append(jnp.maximum(peaks[m], jnp.maximum(s[:, 0:128], s[:, 128:256])))
-            return tuple(new)
-
-        low = jnp.full((256, 128), masked_score, f32)
-        peaks = lax.fori_loop(0, pairs, scored, (low, low))
-        tops = [jnp.max(peak, axis=-1, keepdims=True) for peak in peaks]
-
-        def weighed(p, carry):
-            totals, acc = carry
-            new, ws = [], []
-            for m in range(2):
-                w = jnp.exp2((scores[2 * p + m] - tops[m]) * EXP2_SCALE)
-                new.append(totals[m] + (w[:, 0:128] + w[:, 128:256]))
-                ws.append(w.astype(bf16))
-            va = jnp.concatenate([kpool[2 * p, 256:384, :], kpool[2 * p, 384:512, :]], axis=1)
-            vb = jnp.concatenate([kpool[2 * p + 1, 256:384, :], kpool[2 * p + 1, 384:512, :]], axis=1)
-            vals = jnp.concatenate([va, vb], axis=0)
-            acc = acc + jnp.dot(
-                jnp.concatenate(ws, axis=0), vals, preferred_element_type=f32
-            )
-            return tuple(new), acc
-
-        none = jnp.zeros((256, 128), f32)
-        totals, acc = lax.fori_loop(
-            0, pairs, weighed, ((none, none), jnp.zeros((512, VD), f32))
-        )
+        seen = k_at <= q_at
         levels = []
         for m in range(2):
-            total = jnp.sum(totals[m], axis=-1, keepdims=True)
-            o = (acc[256 * m : 256 * m + 256] / total).astype(bf16)
-            seen = tops[m] > 0.5 * masked_score
-            levels.append(jnp.where(seen, tops[m] * EXP2_SCALE + jnp.log2(total), masked_score))
+            lo = slice(128 * m, 128 * m + 128)
+            q = jnp.concatenate([qpool[2 * c, lo, :], qpool[2 * c + 1, lo, :]], axis=0)
+            k = kpool[:, lo, :].reshape(1024, 128)
+            s = lax.dot_general(q, k, (((1,), (1,)), ((), ())), preferred_element_type=f32)
+            s = jnp.where(seen, s, masked_score)
+            top = jnp.max(s, axis=-1, keepdims=True)
+            w = jnp.exp2((s - top) * EXP2_SCALE)
+            total = jnp.sum(w, axis=-1, keepdims=True)
+            o = (jnp.dot(w.astype(bf16), vals, preferred_element_type=f32) / total).astype(bf16)
+            level = top * EXP2_SCALE + jnp.log2(total)
+            levels.append(jnp.where(top > 0.5 * masked_score, level, masked_score))
             for h in range(2):
                 for e in range(2):
                     out[2 * c + h, 256 * m + 128 * e : 256 * m + 128 * e + 128, :] = o[
@@ -157,9 +110,6 @@
                 for n, piece in enumerate((a, b, d)):
                     rows = jnp.where(at == 3 * m + n, piece, rows)
             out[2 * c + h, 512:528, :] = rows.astype(bf16)
-        return carry
-
-    lax.fori_loop(first_chunk, SIDE // 2, chunk, 0)
 
 
 def join_kernel(mix, parts, gain, out):
@@ -268,7 +218,15 @@
         lifted[:, 256 * n : 256 * n + part.shape[1]] = part.astype(bf16)
 
 
-def down_kernel(gated, lifted, prior, taps, weight, out):
+def own_rows(place, i):
+    return pl.ds(pl.multiple_of(32 * i + 16 * place[0], 16), 16)
+
+
+def other_rows(place, i):
+    return pl.ds(pl.multiple_of(32 * i + 16 - 16 * place[0], 16), 16)
+
+
+def down_kernel(place, gated, lifted, prior, taps, weight, keep, give, whole):
     at = lax.broadcasted_iota(jnp.int32, (128, 1), 0)
 
     def activated(lo, hi):
@@ -287,13 +245,21 @@
         acc = d if acc is None else acc + d
     g, a = activated(MAIN, MAIN + 128)
     h = (pltpu.roll(a, 64, 1) * g).astype(bf16)
-    acc = acc + jnp.dot(h[:, 0:64], weight[MAIN:, :], preferred_element_type=f32)
-    out[...] = acc.astype(bf16)
+    whole[...] = acc + jnp.dot(h[:, 0:64], weight[MAIN:, :], preferred_element_type=f32)
+    for i in range(4):
+        keep[16 * i : 16 * i + 16] = whole[own_rows(place, i)]
+        give[16 * i : 16 * i + 16] = whole[other_rows(place, i)].astype(bf16)
+
+
+def pair_kernel(keep, other, out):
+    for i in range(4):
+        rows = slice(16 * i, 16 * i + 16)
+        out[i] = (keep[rows] + other[rows].astype(f32)).astype(bf16)
 
 
 def last_kernel(parts, stream, out):
     mixer = parts[0].astype(f32)
-    for i in range(1, 8):
+    for i in range(1, 4):
         mixer = mixer + parts[i].astype(f32)
     out[...] = (stream[...] + mixer).astype(bf16)
 
@@ -311,6 +277,7 @@
 
 
 SMALL = pltpu.CompilerParams(vmem_limit_bytes=20 << 20)
+LARGE = pltpu.CompilerParams(vmem_limit_bytes=30 << 20)
 
 
 def on_device(
@@ -335,8 +302,8 @@
     z = lax.axis_index("z")
     y = lax.axis_index("y")
     core = lax.axis_index("core")
-    along_y = jnp.stack([z * SIDE, 1 + 0 * z, y, SIDE + 0 * z, 0 * z, z // 2 + 1])
-    along_z = jnp.stack([y, SIDE + 0 * z, z * SIDE, 1 + 0 * z, z // 2, SIDE // 2 + 0 * z])
+    along_y = jnp.stack([z * SIDE, 1 + 0 * z, y, SIDE + 0 * z])
+    along_z = jnp.stack([y, SIDE + 0 * z, z * SIDE, 1 + 0 * z])
     plan = jnp.where(core == 0, along_y, along_z).astype(jnp.int32)
     smem = pl.BlockSpec(memory_space=pltpu.SMEM)
     hbm = pl.BlockSpec(memory_space=pltpu.HBM)
@@ -377,8 +344,7 @@
             pl.BlockSpec((SIDE, 512, 128), lambda i: (0, 0, 0)),
         ],
         out_specs=vmem(),
-        scratch_shapes=[pltpu.VMEM((8, 256, 256), f32)],
-        compiler_params=SMALL,
+        compiler_params=LARGE,
         name="attend",
     )(plan, qpool, kpool)
     back = swapped(out, ALL, Q_GROUPS)
@@ -446,15 +412,28 @@
     )(place, rows, weights)
     gap = jnp.zeros((WIDTH, 64), f32)
     taps = jnp.concatenate([conv_taps[:, :MAIN], gap, conv_taps[:, MAIN:]], axis=1)
-    down = pl.pallas_call(
+    keep, give = pl.pallas_call(
         down_kernel,
-        out_shape=jax.ShapeDtypeStruct((tokens, width), bf16),
-        in_specs=[vmem()] * 5,
+        out_shape=[
+            jax.ShapeDtypeStruct((tokens // 2, width), f32),
+            jax.ShapeDtypeStruct((tokens // 2, width), bf16),
+        ],
+        in_specs=[smem] + [vmem()] * 5,
+        out_specs=[vmem()] * 2,
+        scratch_shapes=[pltpu.VMEM((128, 2048), f32)],
+        compiler_params=SMALL,
+        name="down",
+    )(place, gated, lifted, prior, taps, down_weight)
+    taken = lax.ppermute(give, "core", [(0, 1), (1, 0)])
+    pair = pl.pallas_call(
+        pair_kernel,
+        out_shape=jax.ShapeDtypeStruct((4, own, width), bf16),
+        in_specs=[vmem()] * 2,
         out_specs=vmem(),
         compiler_params=SMALL,
-        name="down",
-    )(gated, lifted, prior, taps, down_weight)
-    mixer = swapped(down.reshape(8, own, width), TP)
+        name="pair",
+    )(keep, taken)
+    mixer = swapped(pair, "x")
     return pl.pallas_call(
         last_kernel,
         out_shape=jax.ShapeDtypeStruct((own, width), bf16),

time: 193 us -> 186 us (0.964)
  blocking collectives: 111 us -> 101 us
  starting transfers between devices: 26.9 us -> 28.9 us
    all_gather x2, blocking collectives: 61.2 us -> 55 us  [gathered(): return lax.all_gather(a, axis, axis_index_groups=groups, axis=0, tiled=True)]
    all_to_all x2, blocking collectives: 49.9 us -> 46.4 us  [swapped(): return lax.all_to_all(a, axis, 0, 0, axis_index_groups=groups, tiled=True)]
  transfers between devices with their start and end apart: 9 -> 10, of which waited for: 5 -> 6; matrix products, arithmetic and copies ran while one was open for 1% -> 1% of each run, Pallas kernels for 7% -> 7%
where the time goes in v7:
time: 186 us
  blocking collectives  101 us (54%)
  starting transfers between devices  28.9 us (16%)
  Pallas kernels  21.4 us (12%)
  waiting for transfers between devices  14.7 us (8%)
  between operations  14.3 us (8%)
  local copies, waits for them, and re-layouts  4.84 us (3%)
    all_gather x2, blocking collectives, gathered(): return lax.all_gather(a, axis, axis_index_groups=groups, axis=0, tiled=True)  55 us
    all_to_all x2, blocking collectives, swapped(): return lax.all_to_all(a, axis, 0, 0, axis_index_groups=groups, tiled=True)  46.4 us
    all_to_all x2, starting transfers between devices, swapped(): return lax.all_to_all(a, axis, 0, 0, axis_index_groups=groups, tiled=True)  9.02 us
    pallas_call x1, Pallas kernels, on_device(): pl.pallas_call(attend_kernel, grid=(1,), out_shape=jax.ShapeDtypeStruct((...  5.25 us
    ppermute x1, waiting for transfers between devices, on_device(): lax.ppermute(above[0:128], 'x', [(i, (i + 1) % 4) for i in range(4)])  4.59 us
  transfers between devices with their start and end apart: 10, of which 6 were waited for; matrix products, arithmetic and copies ran while one was open for 1% of the time, Pallas kernels for 7%

profile of v7, /device:TPU:64, one launch (start us, length us, event | category | flops | bytes accessed | tf_op | source)
XLA Modules:
  0.0 185.8 jit_solution(3934300465815013359)
XLA Ops:
  6.5 3.4 %pack.1 = (bf16[256,128]{1,0:T(8,128)(2,1)S(1)}, bf16[8,864,128]{2,1,0:T(8,128)(2,1)S(1)}) custom-call(bf16[128,128]{1,0:T(8,128)(2,1)} %q1.1, bf16[128,128]{1,0:T(8,128)(2,1)} %q2.1, bf16[128,128]{1,0:T(8,128)(2,1)} %k1.1, bf16[128,128]{1,0:T(8,128)(2,1)} %k2.1, bf16[128,256]{1,0:T(8,128)(2,1)} %v.1, bf16[32,704]{1,0:T(8,128)(2,1)} %lift.2, ...), custom_call_target="tpu_custom_call" | custom-call | tf_op jit(solution)/shard_map/pack/pallas_call | solution.py:314
  9.9 34.9 %all_to_all.20.kpool = bf16[8,864,128]{2,1,0:T(8,128)(2,1)S(1)} all-to-all(bf16[8,864,128]{2,1,0:T(8,128)(2,1)S(1)} %get-tuple-element.19), channel_id=1, replica_groups={{0,64,128,192,256,320,384,448},{2,66,130,194,258,322,386,450},{4,68,132..., dimensions={0} | all-to-all | bytes 3538944 | tf_op jit(solution)/shard_map/all_to_all | solution.py:268
  45.9 27.6 %all_gather.9 = bf16[2048,128]{1,0:T(8,128)(2,1)S(1)} all-gather(bf16[256,128]{1,0:T(8,128)(2,1)S(1)} %get-tuple-element.18), channel_id=1, replica_groups={{0,8,16,24,32,40,48,56},{2,10,18,26,34,42,50,58},{4,12,20,28,36,44,52,6..., dimensions={0}, use_global_device_ids=true | all-gather | bytes 589824 | tf_op jit(solution)/shard_map/all_gather | solution.py:272
  73.5 5.3 %attend.1 = bf16[8,528,128]{2,1,0:T(8,128)(2,1)} custom-call(s32[4]{0:T(128)S(1)} %broadcast_select_fusion.plan, bf16[8,256,128]{2,1,0:T(8,128)(2,1)S(1)} %bitcast.10, bf16[8,864,128]{2,1,0:T(8,128)(2,1)S(1)} %all_to_all.20.kpool), custom_call_target="tpu_custom_call" | custom-call | tf_op jit(solution)/shard_map/attend/pallas_call | solution.py:337
  78.7 5.6 %all-to-all-start.1 = ((bf16[8,528,128]{2,1,0:T(8,128)(2,1)}), bf16[8,528,128]{2,1,0:T(8,128)(2,1)S(1)}, u32[]{:S(2)}, u32[]{:S(2)}) async-start(bf16[8,528,128]{2,1,0:T(8,128)(2,1)} %attend.1), calls=%async_computation.1 | async-start | bytes 2162688 | tf_op jit(solution)/shard_map/all_to_all | solution.py:268
  84.4 3.4 %collective-permute-start = (bf16[256,2048]{1,0:T(8,128)(2,1)}, bf16[256,2048]{1,0:T(8,128)(2,1)S(1)}, u32[]{:S(2)}, u32[]{:S(2)}) collective-permute-start(bf16[256,2048]{1,0:T(8,128)(2,1)} %refs_0_.1), channel_id=1, source_target_pairs={{0,2},{2,4},{4,6},{6,0},{1,3},{3,5},{5,7},{7,1},{8,10},{10,12},{12... | collective-permute-start | bytes 3145736 | tf_op jit(solution)/shard_map/ppermute | solution.py:312
  87.8 3.7 %collective-permute-start.1 = (bf16[256,2048]{1,0:T(8,128)(2,1)}, bf16[256,2048]{1,0:T(8,128)(2,1)S(1)}, u32[]{:S(2)}, u32[]{:S(2)}) collective-permute-start(bf16[256,2048]{1,0:T(8,128)(2,1)} %refs_0_.1), channel_id=1, source_target_pairs={{0,6},{2,0},{4,2},{6,4},{1,7},{3,1},{5,3},{7,5},{8,14},{10,8},{12,... | collective-permute-start | bytes 3145736 | tf_op jit(solution)/shard_map/ppermute | solution.py:313
  91.5 27.4 %all_gather.10.residual = bf16[128,2048]{1,0:T(8,128)(2,1)} all-gather(bf16[16,2048]{1,0:T(8,128)(2,1)S(1)} %copy-done.6), channel_id=1, replica_groups=mesh['z'=8,'y'=8,'x'=4,'core'=2] {'x','core'}, dimensions={0}, use_global_device_ids=true | all-gather | bytes 589824 | tf_op jit(solution)/shard_map/all_gather | solution.py:272
  119.7 3.6 %collective-permute-start.2 = (bf16[128,2048]{1,0:T(8,128)(2,1)}, bf16[128,2048]{1,0:T(8,128)(2,1)}, u32[]{:S(2)}, u32[]{:S(2)}) collective-permute-start(bf16[128,2048]{1,0:T(8,128)(2,1)} %slice.15), channel_id=1, source_target_pairs={{0,2},{2,4},{4,6},{6,0},{1,3},{3,5},{5,7},{7,1},{8,10},{10,12},{12... | collective-permute-start | bytes 1572872 | tf_op jit(solution)/shard_map/ppermute | solution.py:354
  124.1 3.4 %collective-permute-start.3 = (bf16[128,2048]{1,0:T(8,128)(2,1)}, bf16[128,2048]{1,0:T(8,128)(2,1)}, u32[]{:S(2)}, u32[]{:S(2)}) collective-permute-start(bf16[128,2048]{1,0:T(8,128)(2,1)} %slice.16), channel_id=1, source_target_pairs={{0,6},{2,0},{4,2},{6,4},{1,7},{3,1},{5,3},{7,5},{8,14},{10,8},{12,... | collective-permute-start | bytes 1572872 | tf_op jit(solution)/shard_map/ppermute | solution.py:355
  129.6 3.4 %all-to-all-start.2 = ((bf16[4,128,256]{2,1,0:T(8,128)(2,1)}), bf16[4,128,256]{2,1,0:T(8,128)(2,1)S(1)}, u32[]{:S(2)}, u32[]{:S(2)}) async-start(bf16[4,128,256]{2,1,0:T(8,128)(2,1)} %join.1), calls=%async_computation.2 | async-start | bytes 524288 | tf_op jit(solution)/shard_map/all_to_all | solution.py:268
  133.1 4.6 %collective-permute-done.2.refs_3_ = bf16[128,2048]{1,0:T(8,128)(2,1)} collective-permute-done((bf16[128,2048]{1,0:T(8,128)(2,1)}, bf16[128,2048]{1,0:T(8,128)(2,1)}, u32[]{:S(2)}, u32[]{:S(2)}) %collective-permute-start.2) | collective-permute-done | bytes 524320 | tf_op jit(solution)/shard_map/ppermute | solution.py:354
  137.7 3.5 %collective-permute-done.3.refs_4_ = bf16[128,2048]{1,0:T(8,128)(2,1)} collective-permute-done((bf16[128,2048]{1,0:T(8,128)(2,1)}, bf16[128,2048]{1,0:T(8,128)(2,1)}, u32[]{:S(2)}, u32[]{:S(2)}) %collective-permute-start.3) | collective-permute-done | bytes 524320 | tf_op jit(solution)/shard_map/ppermute | solution.py:355
  142.2 2.7 %project.1 = (f32[128,2048]{1,0:T(8,128)S(1)}, bf16[128,2048]{1,0:T(8,128)(2,1)S(1)}) custom-call(s32[3]{0:T(128)S(1)} %pad_add_fusion.place.core, bf16[4,128,256]{2,1,0:T(8,128)(2,1)S(1)} %all-to-all-done.2.heads, bf16[256,2048]{1,0:T(8,128)(2,1)} %refs_0_.1, bf16[256,2048]{1,0:T(8,128)(2,1)S(1)} %collective-permute-done.refs_1_, ...), custom_call_target="tpu_custom_call" | custom-call | tf_op jit(solution)/shard_map/project/pallas_call | solution.py:366
  146.0 1.9 %collective-permute-start.4 = (bf16[128,2048]{1,0:T(8,128)(2,1)S(1)}, bf16[128,2048]{1,0:T(8,128)(2,1)S(1)}, u32[]{:S(2)}, u32[]{:S(2)}) collective-permute-start(bf16[128,2048]{1,0:T(8,128)(2,1)S(1)} %get-tuple-element.23), channel_id=1, source_target_pairs={{0,1},{1,0},{2,3},{3,2},{4,5},{5,4},{6,7},{7,6},{8,9},{9,8},{10,11... | collective-permute-start | bytes 1572872 | tf_op jit(solution)/shard_map/ppermute | solution.py:378
  148.0 1.8 collective-permute-done.4.other
  151.0 2.9 %gate.3 = (bf16[128,768]{1,0:T(8,128)(2,1)S(1)}, bf16[16,768]{1,0:T(8,128)(2,1)S(1)}, bf16[128,2048]{1,0:T(8,128)(2,1)S(1)}, f32[16,2048]{1,0:T(8,128)S(1)}) custom-call(s32[3]{0:T(128)S(1)} %pad_add_fusion.place.core, f32[128,2048]{1,0:T(8,128)S(1)} %copy-done.3, bf16[128,2048]{1,0:T(8,128)(2,1)S(1)} %collective-permute-done.4.other, ...), custom_call_target="tpu_custom_call" | custom-call | tf_op jit(solution)/shard_map/gate/pallas_call | solution.py:379
  153.9 1.9 %collective-permute-start.5 = (bf16[16,768]{1,0:T(8,128)(2,1)S(1)}, bf16[16,768]{1,0:T(8,128)(2,1)S(1)}, u32[]{:S(2)}, u32[]{:S(2)}) collective-permute-start(bf16[16,768]{1,0:T(8,128)(2,1)S(1)} %get-tuple-element.27), channel_id=1, source_target_pairs={{0,8},{8,16},{16,24},{24,32},{32,40},{40,48},{48,56},{56,64},{64,7... | collective-permute-start | bytes 73736 | tf_op jit(solution)/shard_map/ppermute | solution.py:397
  155.8 3.6 %lift.3.lifted = bf16[128,640]{1,0:T(8,128)(2,1)S(1)} custom-call(s32[3]{0:T(128)S(1)} %pad_add_fusion.place.core, bf16[128,2048]{1,0:T(8,128)(2,1)S(1)} %get-tuple-element.26.rows, bf16[8,8,352,128]{3,2,1,0:T(8,128)(2,1)} %bitcast.14), custom_call_target="tpu_custom_call" | custom-call | flops 335544320 | bytes 3145728 | tf_op jit(solution)/shard_map/lift/pallas_call | solution.py:398
  159.4 2.3 %collective-permute-done.5.prior = bf16[16,768]{1,0:T(8,128)(2,1)S(1)} collective-permute-done((bf16[16,768]{1,0:T(8,128)(2,1)S(1)}, bf16[16,768]{1,0:T(8,128)(2,1)S(1)}, u32[]{:S(2)}, u32[]{:S(2)}) %collective-permute-start.5) | collective-permute-done | bytes 24608 | tf_op jit(solution)/shard_map/ppermute | solution.py:397
  161.7 1.6 down.1
  163.3 1.9 %collective-permute-start.6 = (bf16[64,2048]{1,0:T(8,128)(2,1)S(1)}, bf16[64,2048]{1,0:T(8,128)(2,1)S(1)}, u32[]{:S(2)}, u32[]{:S(2)}) collective-permute-start(bf16[64,2048]{1,0:T(8,128)(2,1)S(1)} %get-tuple-element.29), channel_id=1, source_target_pairs={{0,1},{1,0},{2,3},{3,2},{4,5},{5,4},{6,7},{7,6},{8,9},{9,8},{10,11... | collective-permute-start | bytes 786440 | tf_op jit(solution)/shard_map/ppermute | solution.py:427
  165.2 1.5 collective-permute-done.6.other
  166.8 11.5 %all_to_all.21.parts = bf16[4,16,2048]{2,1,0:T(8,128)(2,1)S(1)} all-to-all(bf16[4,16,2048]{2,1,0:T(8,128)(2,1)S(1)} %pair.1), channel_id=1, replica_groups=mesh['z'=8,'y'=8,'x'=4,'core'=2] {'x'}, dimensions={0} | all-to-all | bytes 524288 | tf_op jit(solution)/shard_map/all_to_all | solution.py:268
  (36 shorter events, 8.3 us)
Async XLA Ops:
  6.5 143.2 %all-gather.2.cloned.1.call-start = ((), (), s32[]{:S(2)}) async-start(), calls=%async_computation.4 | async-start | bytes 6488064 | tf_op jit(solution)/shard_map/all_gather | solution.py:272
  78.7 12.7 %copy-start.6 = (bf16[16,2048]{1,0:T(8,128)(2,1)S(1)}, bf16[16,2048]{1,0:T(8,128)(2,1)}, u32[]{:S(2)}) copy-start(bf16[16,2048]{1,0:T(8,128)(2,1)} %param.21) | copy-start | bytes 196612
  78.7 49.5 %all-to-all-start.1 = ((bf16[8,528,128]{2,1,0:T(8,128)(2,1)}), bf16[8,528,128]{2,1,0:T(8,128)(2,1)S(1)}, u32[]{:S(2)}, u32[]{:S(2)}) async-start(bf16[8,528,128]{2,1,0:T(8,128)(2,1)} %attend.1), calls=%async_computation.1 | async-start | bytes 2162688 | tf_op jit(solution)/shard_map/all_to_all | solution.py:268
  84.4 43.9 %copy-start.5 = (f32[256]{0:T(256)S(1)}, f32[256]{0:T(256)}, u32[]{:S(2)}) copy-start(f32[256]{0:T(256)} %param.20) | copy-start | bytes 3076
  84.4 34.5 %collective-permute-start = (bf16[256,2048]{1,0:T(8,128)(2,1)}, bf16[256,2048]{1,0:T(8,128)(2,1)S(1)}, u32[]{:S(2)}, u32[]{:S(2)}) collective-permute-start(bf16[256,2048]{1,0:T(8,128)(2,1)} %refs_0_.1), channel_id=1, source_target_pairs={{0,2},{2,4},{4,6},{6,0},{1,3},{3,5},{5,7},{7,1},{8,10},{10,12},{12... | collective-permute-start | bytes 3145736 | tf_op jit(solution)/shard_map/ppermute | solution.py:312
  87.8 31.1 %collective-permute-start.1 = (bf16[256,2048]{1,0:T(8,128)(2,1)}, bf16[256,2048]{1,0:T(8,128)(2,1)S(1)}, u32[]{:S(2)}, u32[]{:S(2)}) collective-permute-start(bf16[256,2048]{1,0:T(8,128)(2,1)} %refs_0_.1), channel_id=1, source_target_pairs={{0,6},{2,0},{4,2},{6,4},{1,7},{3,1},{5,3},{7,5},{8,14},{10,8},{12,... | collective-permute-start | bytes 3145736 | tf_op jit(solution)/shard_map/ppermute | solution.py:313
  119.7 18.0 %collective-permute-start.2 = (bf16[128,2048]{1,0:T(8,128)(2,1)}, bf16[128,2048]{1,0:T(8,128)(2,1)}, u32[]{:S(2)}, u32[]{:S(2)}) collective-permute-start(bf16[128,2048]{1,0:T(8,128)(2,1)} %slice.15), channel_id=1, source_target_pairs={{0,2},{2,4},{4,6},{6,0},{1,3},{3,5},{5,7},{7,1},{8,10},{10,12},{12... | collective-permute-start | bytes 1572872 | tf_op jit(solution)/shard_map/ppermute | solution.py:354
  124.1 17.0 %collective-permute-start.3 = (bf16[128,2048]{1,0:T(8,128)(2,1)}, bf16[128,2048]{1,0:T(8,128)(2,1)}, u32[]{:S(2)}, u32[]{:S(2)}) collective-permute-start(bf16[128,2048]{1,0:T(8,128)(2,1)} %slice.16), channel_id=1, source_target_pairs={{0,6},{2,0},{4,2},{6,4},{1,7},{3,1},{5,3},{7,5},{8,14},{10,8},{12,... | collective-permute-start | bytes 1572872 | tf_op jit(solution)/shard_map/ppermute | solution.py:355
  129.6 12.7 %all-to-all-start.2 = ((bf16[4,128,256]{2,1,0:T(8,128)(2,1)}), bf16[4,128,256]{2,1,0:T(8,128)(2,1)S(1)}, u32[]{:S(2)}, u32[]{:S(2)}) async-start(bf16[4,128,256]{2,1,0:T(8,128)(2,1)} %join.1), calls=%async_computation.2 | async-start | bytes 524288 | tf_op jit(solution)/shard_map/all_to_all | solution.py:268
  133.1 14.8 %slice-start = ((f32[3,704]{1,0:T(4,128)}), f32[3,640]{1,0:T(4,128)S(1)}, s32[]{:S(2)}) async-start(f32[3,704]{1,0:T(4,128)} %param.26), calls=%async_computation.5 | async-start | bytes 20480 | tf_op jit(solution)/shard_map/slice | solution.py:414
  133.1 14.8 %slice-start.1 = ((f32[3,704]{1,0:T(4,128)}), f32[3,64]{1,0:T(4,128)S(1)}, s32[]{:S(2)}) async-start(f32[3,704]{1,0:T(4,128)} %param.26), calls=%async_computation.6 | async-start | bytes 4096 | tf_op jit(solution)/shard_map/slice | solution.py:414
  133.1 16.7 %copy-start.1 = (bf16[128,2048]{1,0:T(8,128)(2,1)S(1)}, bf16[128,2048]{1,0:T(8,128)(2,1)}, u32[]{:S(2)}) copy-start(bf16[128,2048]{1,0:T(8,128)(2,1)} %all_gather.10.residual) | copy-start | bytes 1572868
  133.1 16.7 %copy-start.4 = (f32[2048]{0:T(1024)S(1)}, f32[2048]{0:T(1024)}, u32[]{:S(2)}) copy-start(f32[2048]{0:T(1024)} %param.23) | copy-start | bytes 24580
  145.0 1.0 copy-start.2
  146.0 3.8 %collective-permute-start.4 = (bf16[128,2048]{1,0:T(8,128)(2,1)S(1)}, bf16[128,2048]{1,0:T(8,128)(2,1)S(1)}, u32[]{:S(2)}, u32[]{:S(2)}) collective-permute-start(bf16[128,2048]{1,0:T(8,128)(2,1)S(1)} %get-tuple-element.23), channel_id=1, source_target_pairs={{0,1},{1,0},{2,3},{3,2},{4,5},{5,4},{6,7},{7,6},{8,9},{9,8},{10,11... | collective-permute-start | bytes 1572872 | tf_op jit(solution)/shard_map/ppermute | solution.py:378
  149.8 1.2 copy-start.3
  153.9 7.8 %collective-permute-start.5 = (bf16[16,768]{1,0:T(8,128)(2,1)S(1)}, bf16[16,768]{1,0:T(8,128)(2,1)S(1)}, u32[]{:S(2)}, u32[]{:S(2)}) collective-permute-start(bf16[16,768]{1,0:T(8,128)(2,1)S(1)} %get-tuple-element.27), channel_id=1, source_target_pairs={{0,8},{8,16},{16,24},{24,32},{32,40},{40,48},{48,56},{56,64},{64,7... | collective-permute-start | bytes 73736 | tf_op jit(solution)/shard_map/ppermute | solution.py:397
  155.8 5.9 %copy-start = (bf16[704,2048]{1,0:T(8,128)(2,1)S(1)}, bf16[704,2048]{1,0:T(8,128)(2,1)}, u32[]{:S(2)}) copy-start(bf16[704,2048]{1,0:T(8,128)(2,1)} %weight.1) | copy-start | bytes 8650756
  163.3 3.4 %collective-permute-start.6 = (bf16[64,2048]{1,0:T(8,128)(2,1)S(1)}, bf16[64,2048]{1,0:T(8,128)(2,1)S(1)}, u32[]{:S(2)}, u32[]{:S(2)}) collective-permute-start(bf16[64,2048]{1,0:T(8,128)(2,1)S(1)} %get-tuple-element.29), channel_id=1, source_target_pairs={{0,1},{1,0},{2,3},{3,2},{4,5},{5,4},{6,7},{7,6},{8,9},{9,8},{10,11... | collective-permute-start | bytes 786440 | tf_op jit(solution)/shard_map/ppermute | solution.py:427
Sparse Core Ops, SparseCore 0:
  45.9 49.0 all-gather.1

commit v8 on v7

--- a/solution.py
+++ b/solution.py
@@ -112,7 +112,7 @@
             out[2 * c + h, 512:528, :] = rows.astype(bf16)
 
 
-def join_kernel(mix, parts, gain, out):
+def join_kernel(mix, parts, gain, residual, out):
     tails = [parts[i, 512:528, :].astype(f32) for i in range(SIDE)]
 
     def joined(m):
@@ -135,31 +135,41 @@
     r = lax.rsqrt(jnp.mean(mixed * mixed, axis=-1, keepdims=True) + epsilon)
     head = (mixed * r * gain[...]).astype(bf16)
     for i in range(4):
-        out[i] = head
+        out[i, 0:128] = head
+        for j in range(8):
+            out[i, 128 + 16 * j : 144 + 16 * j, :] = residual[:, 256 * j : 256 * j + 256]
+
+
+def own_rows(place, i):
+    return pl.ds(pl.multiple_of(32 * i + 16 * place[0], 16), 16)
+
+
+def other_rows(place, i):
+    return pl.ds(pl.multiple_of(32 * i + 16 - 16 * place[0], 16), 16)
 
 
 def project_kernel(place, heads, *refs):
-    weights, (half, sent, buffer, sems) = refs[:5], refs[5:]
+    weights, (half, sent, buffer, sems) = refs[:4], refs[4:]
     x = place[1]
-    slots = [buffer.at[0], buffer.at[1], buffer.at[2], buffer.at[3, 0:128], buffer.at[3, 128:256]]
     moves = [
-        pltpu.make_async_copy(weight, slot, sems.at[i])
-        for i, (weight, slot) in enumerate(zip(weights, slots))
+        pltpu.make_async_copy(weight, buffer.at[i], sems.at[i]) for i, weight in enumerate(weights)
     ]
     for move in moves:
         move.start()
     for i, shift in enumerate(SHIFTS):
         moves[i].wait()
-        if i == 3:
-            moves[4].wait()
-        head = heads[lax.rem(x + 4 - shift, 4)]
+        head = heads[lax.rem(x + 4 - shift, 4), 0:128]
         for n in range(0, 2048, 256):
             d = jnp.dot(head, buffer[i, :, n : n + 256], preferred_element_type=f32)
             if i > 0:
                 d = d + half[:, n : n + 256]
             half[:, n : n + 256] = d
-            if i == 3:
-                sent[:, n : n + 256] = d.astype(bf16)
+    for i in range(4):
+        rows = own_rows(place, i)
+        for j in range(8):
+            r = heads[i, 128 + 16 * j : 144 + 16 * j, :].astype(f32)
+            half[rows, 256 * j : 256 * j + 256] = half[rows, 256 * j : 256 * j + 256] + r
+    sent[...] = half[...].astype(bf16)
 
 
 def fetched(core, weights, buffer, sems, first):
@@ -196,16 +206,14 @@
     return acc
 
 
-def gate_kernel(place, half, other, residual, gain, weights, gated, edge, rows, stream, buffer, sems):
+def gate_kernel(place, half, other, gain, weights, gated, edge, rows, stream, buffer, sems):
     fetched(place[0], weights, buffer, sems, 0)
     for n in range(0, 128, 32):
-        total = residual[n : n + 32].astype(f32) + (
-            half[n : n + 32] + other[n : n + 32].astype(f32)
-        )
+        total = half[n : n + 32] + other[n : n + 32].astype(f32)
         r = lax.rsqrt(jnp.mean(total * total, axis=-1, keepdims=True) + epsilon)
         rows[n : n + 32] = (total * r * gain[...]).astype(bf16)
     own = pl.ds(pl.multiple_of(place[2] * 16, 16), 16)
-    stream[...] = residual[own].astype(f32) + (half[own] + other[own].astype(f32))
+    stream[...] = half[own] + other[own].astype(f32)
     for n, part in enumerate(multiplied(rows, weights, buffer, sems, 0)):
         part = part.astype(bf16)
         gated[:, 256 * n : 256 * n + 256] = part
@@ -216,14 +224,6 @@
     fetched(core[0], weights, buffer, sems, 192)
     for n, part in enumerate(multiplied(rows, weights, buffer, sems, 192)):
         lifted[:, 256 * n : 256 * n + part.shape[1]] = part.astype(bf16)
-
-
-def own_rows(place, i):
-    return pl.ds(pl.multiple_of(32 * i + 16 * place[0], 16), 16)
-
-
-def other_rows(place, i):
-    return pl.ds(pl.multiple_of(32 * i + 16 - 16 * place[0], 16), 16)
 
 
 def down_kernel(place, gated, lifted, prior, taps, weight, keep, give, whole):
@@ -309,8 +309,6 @@
     hbm = pl.BlockSpec(memory_space=pltpu.HBM)
     x = lax.axis_index("x")
     place = jnp.stack([core, x, 2 * x + core]).astype(jnp.int32)
-    above = lax.ppermute(out_weight, "x", [(i, (i + 1) % 4) for i in range(4)])
-    below = lax.ppermute(out_weight, "x", [(i, (i + 3) % 4) for i in range(4)])
     qsend, ksend = pl.pallas_call(
         pack_kernel,
         out_shape=[
@@ -334,6 +332,8 @@
     qpool = gathered(qsend, ALL, Q_GROUPS).reshape(SIDE, 256, 128)
     part = kpool[:, 512:, :].reshape(SIDE * 352, 128)
     weights = in_hbm(gathered(part, ALL, Q_GROUPS).reshape(SIDE, SIDE, 352, 128))
+    ring = [(i, (i + 1) % 4) for i in range(4)]
+    above = lax.ppermute(out_weight, "x", ring)
     out = pl.pallas_call(
         attend_kernel,
         grid=(1,),
@@ -348,20 +348,16 @@
         name="attend",
     )(plan, qpool, kpool)
     back = swapped(out, ALL, Q_GROUPS)
-    before = gathered(residual, TP)
-    above, below, before = lax.optimization_barrier((above, below, before))
-    across = (
-        lax.ppermute(above[0:128], "x", [(i, (i + 1) % 4) for i in range(4)]),
-        lax.ppermute(below[128:256], "x", [(i, (i + 3) % 4) for i in range(4)]),
-    )
+    across = lax.ppermute(above, "x", ring)
+    below = lax.ppermute(out_weight, "x", [(j, i) for i, j in ring])
     heads = pl.pallas_call(
         join_kernel,
-        out_shape=jax.ShapeDtypeStruct((4, tokens, VD), bf16),
-        in_specs=[pl.BlockSpec(memory_space=pltpu.SMEM)] + [vmem()] * 2,
+        out_shape=jax.ShapeDtypeStruct((4, 2 * tokens, VD), bf16),
+        in_specs=[pl.BlockSpec(memory_space=pltpu.SMEM)] + [vmem()] * 3,
         out_specs=vmem(),
         compiler_params=SMALL,
         name="join",
-    )(mix_weight, back, head_gain.reshape(1, VD))
+    )(mix_weight, back, head_gain.reshape(1, VD), residual)
     heads = swapped(heads, "x")
     half, sent = pl.pallas_call(
         project_kernel,
@@ -369,12 +365,12 @@
             jax.ShapeDtypeStruct((tokens, width), f32),
             jax.ShapeDtypeStruct((tokens, width), bf16),
         ],
-        in_specs=[smem, vmem()] + [pl.BlockSpec(memory_space=pl.ANY)] * 5,
+        in_specs=[smem, vmem()] + [pl.BlockSpec(memory_space=pl.ANY)] * 4,
         out_specs=[vmem()] * 2,
-        scratch_shapes=[pltpu.VMEM((4, VD, 2048), bf16), pltpu.SemaphoreType.DMA((5,))],
+        scratch_shapes=[pltpu.VMEM((4, VD, 2048), bf16), pltpu.SemaphoreType.DMA((4,))],
         compiler_params=SMALL,
         name="project",
-    )(place, heads, in_hbm(out_weight), above, below, *across)
+    )(place, heads, *(in_hbm(a) for a in (out_weight, above, below, across)))
     other = lax.ppermute(sent, "core", [(0, 1), (1, 0)])
     gated, edge, rows, stream = pl.pallas_call(
         gate_kernel,
@@ -384,7 +380,7 @@
             jax.ShapeDtypeStruct((tokens, width), bf16),
             jax.ShapeDtypeStruct((own, width), f32),
         ],
-        in_specs=[smem] + [vmem()] * 4 + [hbm],
+        in_specs=[smem] + [vmem()] * 3 + [hbm],
         out_specs=[vmem()] * 4,
         scratch_shapes=[
             pltpu.VMEM((SIDE, SIDE, 192, 128), bf16),
@@ -392,7 +388,7 @@
         ],
         compiler_params=SMALL,
         name="gate",
-    )(place, half, other, before, norm_gain.reshape(1, width), weights)
+    )(place, half, other, norm_gain.reshape(1, width), weights)
     route = [(i, i + 1) for i in range(SIDE * SIDE - 1)]
     prior = lax.ppermute(edge, ("z", "y"), route)
     lifted = pl.pallas_call(

time: 186 us -> 178 us (0.957)
  the two profiles are of different devices: /device:TPU:64 before, /device:TPU:256 now
where the time goes in v8:
time: 178 us; the launch traced here: 177 us
  blocking collectives  65.2 us (37%)
  waiting for transfers between devices  49.6 us (28%)
  starting transfers between devices  25.1 us (14%)
  Pallas kernels  22 us (12%)
  between operations  14.2 us (8%)
    all_to_all x2, blocking collectives, swapped(): return lax.all_to_all(a, axis, 0, 0, axis_index_groups=groups, tiled=True)  37.9 us
    all_gather x1, blocking collectives, gathered(): return lax.all_gather(a, axis, axis_index_groups=groups, axis=0, tiled=True)  27.2 us
    ppermute x1, waiting for transfers between devices, on_device(): across = lax.ppermute(above, 'x', ring)  20.3 us
    ppermute x1, waiting for transfers between devices, on_device(): above = lax.ppermute(out_weight, 'x', ring)  19.8 us
    all_to_all x2, starting transfers between devices, swapped(): return lax.all_to_all(a, axis, 0, 0, axis_index_groups=groups, tiled=True)  10.1 us
    pallas_call x1, Pallas kernels, on_device(): pl.pallas_call(attend_kernel, grid=(1,), out_shape=jax.ShapeDtypeStruct((...  5.26 us
    ppermute x1, starting transfers between devices, on_device(): below = lax.ppermute(out_weight, 'x', [(j, i) for i, j in ring])  3.6 us
    pallas_call x1, Pallas kernels, on_device(): pl.pallas_call(lift_kernel, out_shape=jax.ShapeDtypeStruct((tokens, MAIN)...  3.58 us
  transfers between devices with their start and end apart: 9, of which 6 were waited for; matrix products, arithmetic and copies ran while one was open for 0% of the time, Pallas kernels for 8%

profile of v8, /device:TPU:256, one launch (start us, length us, event | category | flops | bytes accessed | tf_op | source)
XLA Modules:
  0.0 177.3 jit_solution(2472719692959984780)
XLA Ops:
  6.5 3.4 %pack.1 = (bf16[256,128]{1,0:T(8,128)(2,1)S(1)}, bf16[8,864,128]{2,1,0:T(8,128)(2,1)S(1)}) custom-call(bf16[128,128]{1,0:T(8,128)(2,1)} %q1.1, bf16[128,128]{1,0:T(8,128)(2,1)} %q2.1, bf16[128,128]{1,0:T(8,128)(2,1)} %k1.1, bf16[128,128]{1,0:T(8,128)(2,1)} %k2.1, bf16[128,256]{1,0:T(8,128)(2,1)} %v.1, bf16[32,704]{1,0:T(8,128)(2,1)} %lift.2, ...), custom_call_target="tpu_custom_call" | custom-call | tf_op jit(solution)/shard_map/pack/pallas_call | solution.py:312
  9.9 28.3 %all_to_all.20.kpool = bf16[8,864,128]{2,1,0:T(8,128)(2,1)S(1)} all-to-all(bf16[8,864,128]{2,1,0:T(8,128)(2,1)S(1)} %get-tuple-element.16), channel_id=1, replica_groups={{0,64,128,192,256,320,384,448},{2,66,130,194,258,322,386,450},{4,68,132..., dimensions={0} | all-to-all | bytes 3538944 | tf_op jit(solution)/shard_map/all_to_all | solution.py:268
  39.3 27.2 %all_gather.6 = bf16[2048,128]{1,0:T(8,128)(2,1)S(1)} all-gather(bf16[256,128]{1,0:T(8,128)(2,1)S(1)} %get-tuple-element.15), channel_id=1, replica_groups={{0,8,16,24,32,40,48,56},{2,10,18,26,34,42,50,58},{4,12,20,28,36,44,52,6..., dimensions={0}, use_global_device_ids=true | all-gather | bytes 589824 | tf_op jit(solution)/shard_map/all_gather | solution.py:272
  66.5 5.3 %attend.1 = bf16[8,528,128]{2,1,0:T(8,128)(2,1)} custom-call(s32[4]{0:T(128)S(1)} %broadcast_select_fusion.plan, bf16[8,256,128]{2,1,0:T(8,128)(2,1)S(1)} %bitcast.10, bf16[8,864,128]{2,1,0:T(8,128)(2,1)S(1)} %all_to_all.20.kpool), custom_call_target="tpu_custom_call" | custom-call | tf_op jit(solution)/shard_map/attend/pallas_call | solution.py:337
  71.8 5.9 %all-to-all-start.1 = ((bf16[8,528,128]{2,1,0:T(8,128)(2,1)}), bf16[8,528,128]{2,1,0:T(8,128)(2,1)S(1)}, u32[]{:S(2)}, u32[]{:S(2)}) async-start(bf16[8,528,128]{2,1,0:T(8,128)(2,1)} %attend.1), calls=%async_computation.1 | async-start | bytes 2162688 | tf_op jit(solution)/shard_map/all_to_all | solution.py:268
  77.7 3.5 %collective-permute-start = (bf16[256,2048]{1,0:T(8,128)(2,1)S(1)}, bf16[256,2048]{1,0:T(8,128)(2,1)}, u32[]{:S(2)}, u32[]{:S(2)}) collective-permute-start(bf16[256,2048]{1,0:T(8,128)(2,1)S(1)} %copy-done.4), channel_id=1, source_target_pairs={{0,2},{2,4},{4,6},{6,0},{1,3},{3,5},{5,7},{7,1},{8,10},{10,12},{12... | collective-permute-start | bytes 3145736 | tf_op jit(solution)/shard_map/ppermute | solution.py:336
  81.1 3.6 %collective-permute-start.1 = (bf16[256,2048]{1,0:T(8,128)(2,1)S(1)}, bf16[256,2048]{1,0:T(8,128)(2,1)}, u32[]{:S(2)}, u32[]{:S(2)}) collective-permute-start(bf16[256,2048]{1,0:T(8,128)(2,1)S(1)} %copy-done.4), channel_id=1, source_target_pairs={{2,0},{4,2},{6,4},{0,6},{3,1},{5,3},{7,5},{1,7},{10,8},{12,10},{14... | collective-permute-start | bytes 3145736 | tf_op jit(solution)/shard_map/ppermute | solution.py:352
  84.7 19.8 %collective-permute-done.refs_1_ = bf16[256,2048]{1,0:T(8,128)(2,1)} collective-permute-done((bf16[256,2048]{1,0:T(8,128)(2,1)S(1)}, bf16[256,2048]{1,0:T(8,128)(2,1)}, u32[]{:S(2)}, u32[]{:S(2)}) %collective-permute-start) | collective-permute-done | bytes 1048608 | tf_op jit(solution)/shard_map/ppermute | solution.py:336
  104.5 2.2 %collective-permute-start.2 = (bf16[256,2048]{1,0:T(8,128)(2,1)}, bf16[256,2048]{1,0:T(8,128)(2,1)}, u32[]{:S(2)}, u32[]{:S(2)}) collective-permute-start(bf16[256,2048]{1,0:T(8,128)(2,1)} %collective-permute-done.refs_1_), channel_id=1, source_target_pairs={{0,2},{2,4},{4,6},{6,0},{1,3},{3,5},{5,7},{7,1},{8,10},{10,12},{12... | collective-permute-start | bytes 3145736 | tf_op jit(solution)/shard_map/ppermute | solution.py:351
  107.3 1.5 join.1
  108.8 4.3 %all-to-all-start.2 = ((bf16[4,256,256]{2,1,0:T(8,128)(2,1)}), bf16[4,256,256]{2,1,0:T(8,128)(2,1)S(1)}, u32[]{:S(2)}, u32[]{:S(2)}) async-start(bf16[4,256,256]{2,1,0:T(8,128)(2,1)} %join.1), calls=%async_computation.2 | async-start | bytes 1048576 | tf_op jit(solution)/shard_map/all_to_all | solution.py:268
  113.1 20.3 %collective-permute-done.2.refs_3_ = bf16[256,2048]{1,0:T(8,128)(2,1)} collective-permute-done((bf16[256,2048]{1,0:T(8,128)(2,1)}, bf16[256,2048]{1,0:T(8,128)(2,1)}, u32[]{:S(2)}, u32[]{:S(2)}) %collective-permute-start.2) | collective-permute-done | bytes 1048608 | tf_op jit(solution)/shard_map/ppermute | solution.py:351
  133.5 2.7 %all-to-all-done.2.heads = bf16[4,256,256]{2,1,0:T(8,128)(2,1)S(1)} async-done(((bf16[4,256,256]{2,1,0:T(8,128)(2,1)}), bf16[4,256,256]{2,1,0:T(8,128)(2,1)S(1)}, u32[]{:S(2)}, u32[]{:S(2)}) %all-to-all-start.2) | async-done | bytes 524320 | tf_op jit(solution)/shard_map/all_to_all | solution.py:268
  136.2 3.2 %project.1 = (f32[128,2048]{1,0:T(8,128)S(1)}, bf16[128,2048]{1,0:T(8,128)(2,1)S(1)}) custom-call(s32[3]{0:T(128)S(1)} %pad_add_fusion.place.core, bf16[4,256,256]{2,1,0:T(8,128)(2,1)S(1)} %all-to-all-done.2.heads, bf16[256,2048]{1,0:T(8,128)(2,1)} %refs_0_.1, bf16[256,2048]{1,0:T(8,128)(2,1)} %collective-permute-done.refs_1_, ...), custom_call_target="tpu_custom_call" | custom-call | tf_op jit(solution)/shard_map/project/pallas_call | solution.py:362
  139.4 1.9 %collective-permute-start.3 = (bf16[128,2048]{1,0:T(8,128)(2,1)S(1)}, bf16[128,2048]{1,0:T(8,128)(2,1)S(1)}, u32[]{:S(2)}, u32[]{:S(2)}) collective-permute-start(bf16[128,2048]{1,0:T(8,128)(2,1)S(1)} %get-tuple-element.18), channel_id=1, source_target_pairs={{0,1},{1,0},{2,3},{3,2},{4,5},{5,4},{6,7},{7,6},{8,9},{9,8},{10,11... | collective-permute-start | bytes 1572872 | tf_op jit(solution)/shard_map/ppermute | solution.py:374
  141.4 1.8 collective-permute-done.3.other
  143.2 2.8 %gate.3 = (bf16[128,768]{1,0:T(8,128)(2,1)S(1)}, bf16[16,768]{1,0:T(8,128)(2,1)S(1)}, bf16[128,2048]{1,0:T(8,128)(2,1)S(1)}, f32[16,2048]{1,0:T(8,128)S(1)}) custom-call(s32[3]{0:T(128)S(1)} %pad_add_fusion.place.core, f32[128,2048]{1,0:T(8,128)S(1)} %get-tuple-element.17.half, bf16[128,2048]{1,0:T(8,128)(2,1)S(1)} %collective-permute-done.3.other, ...), custom_call_target="tpu_custom_call" | custom-call | tf_op jit(solution)/shard_map/gate/pallas_call | solution.py:375
  146.0 1.9 %collective-permute-start.4 = (bf16[16,768]{1,0:T(8,128)(2,1)S(1)}, bf16[16,768]{1,0:T(8,128)(2,1)S(1)}, u32[]{:S(2)}, u32[]{:S(2)}) collective-permute-start(bf16[16,768]{1,0:T(8,128)(2,1)S(1)} %get-tuple-element.21), channel_id=1, source_target_pairs={{0,8},{8,16},{16,24},{24,32},{32,40},{40,48},{48,56},{56,64},{64,7... | collective-permute-start | bytes 73736 | tf_op jit(solution)/shard_map/ppermute | solution.py:393
  148.0 3.6 %lift.3.lifted = bf16[128,640]{1,0:T(8,128)(2,1)S(1)} custom-call(s32[3]{0:T(128)S(1)} %pad_add_fusion.place.core, bf16[128,2048]{1,0:T(8,128)(2,1)S(1)} %get-tuple-element.20.rows, bf16[8,8,352,128]{3,2,1,0:T(8,128)(2,1)} %bitcast.14), custom_call_target="tpu_custom_call" | custom-call | flops 335544320 | bytes 3145728 | tf_op jit(solution)/shard_map/lift/pallas_call | solution.py:394
  151.5 3.5 %collective-permute-done.4.prior = bf16[16,768]{1,0:T(8,128)(2,1)S(1)} collective-permute-done((bf16[16,768]{1,0:T(8,128)(2,1)S(1)}, bf16[16,768]{1,0:T(8,128)(2,1)S(1)}, u32[]{:S(2)}, u32[]{:S(2)}) %collective-permute-start.4) | collective-permute-done | bytes 24608 | tf_op jit(solution)/shard_map/ppermute | solution.py:393
  155.1 1.6 down.1
  156.7 1.9 %collective-permute-start.5 = (bf16[64,2048]{1,0:T(8,128)(2,1)S(1)}, bf16[64,2048]{1,0:T(8,128)(2,1)S(1)}, u32[]{:S(2)}, u32[]{:S(2)}) collective-permute-start(bf16[64,2048]{1,0:T(8,128)(2,1)S(1)} %get-tuple-element.23), channel_id=1, source_target_pairs={{0,1},{1,0},{2,3},{3,2},{4,5},{5,4},{6,7},{7,6},{8,9},{9,8},{10,11... | collective-permute-start | bytes 786440 | tf_op jit(solution)/shard_map/ppermute | solution.py:423
  158.6 1.5 collective-permute-done.5.other
  160.1 9.6 %all_to_all.21.parts = bf16[4,16,2048]{2,1,0:T(8,128)(2,1)S(1)} all-to-all(bf16[4,16,2048]{2,1,0:T(8,128)(2,1)S(1)} %pair.1), channel_id=1, replica_groups=mesh['z'=8,'y'=8,'x'=4,'core'=2] {'x'}, dimensions={0} | all-to-all | bytes 524288 | tf_op jit(solution)/shard_map/all_to_all | solution.py:268
  (27 shorter events, 1.9 us)
Async XLA Ops:
  6.5 136.6 %all-gather.2.cloned.1.call-start = ((), (), s32[]{:S(2)}) async-start(), calls=%async_computation.4 | async-start | bytes 6488064 | tf_op jit(solution)/shard_map/all_gather | solution.py:272
  71.8 5.9 %copy-start.4 = (bf16[256,2048]{1,0:T(8,128)(2,1)S(1)}, bf16[256,2048]{1,0:T(8,128)(2,1)}, u32[]{:S(2)}) copy-start(bf16[256,2048]{1,0:T(8,128)(2,1)} %refs_0_.1) | copy-start | bytes 3145732
  71.8 35.5 %copy-start.1 = (bf16[16,2048]{1,0:T(8,128)(2,1)S(1)}, bf16[16,2048]{1,0:T(8,128)(2,1)}, u32[]{:S(2)}) copy-start(bf16[16,2048]{1,0:T(8,128)(2,1)} %residual.1) | copy-start | bytes 196612
  71.8 35.6 %copy-start.3 = (f32[256]{0:T(256)S(1)}, f32[256]{0:T(256)}, u32[]{:S(2)}) copy-start(f32[256]{0:T(256)} %param.20) | copy-start | bytes 3076
  71.8 35.5 %all-to-all-start.1 = ((bf16[8,528,128]{2,1,0:T(8,128)(2,1)}), bf16[8,528,128]{2,1,0:T(8,128)(2,1)S(1)}, u32[]{:S(2)}, u32[]{:S(2)}) async-start(bf16[8,528,128]{2,1,0:T(8,128)(2,1)} %attend.1), calls=%async_computation.1 | async-start | bytes 2162688 | tf_op jit(solution)/shard_map/all_to_all | solution.py:268
  77.7 26.8 %collective-permute-start = (bf16[256,2048]{1,0:T(8,128)(2,1)S(1)}, bf16[256,2048]{1,0:T(8,128)(2,1)}, u32[]{:S(2)}, u32[]{:S(2)}) collective-permute-start(bf16[256,2048]{1,0:T(8,128)(2,1)S(1)} %copy-done.4), channel_id=1, source_target_pairs={{0,2},{2,4},{4,6},{6,0},{1,3},{3,5},{5,7},{7,1},{8,10},{10,12},{12... | collective-permute-start | bytes 3145736 | tf_op jit(solution)/shard_map/ppermute | solution.py:336
  81.1 32.0 %collective-permute-start.1 = (bf16[256,2048]{1,0:T(8,128)(2,1)S(1)}, bf16[256,2048]{1,0:T(8,128)(2,1)}, u32[]{:S(2)}, u32[]{:S(2)}) collective-permute-start(bf16[256,2048]{1,0:T(8,128)(2,1)S(1)} %copy-done.4), channel_id=1, source_target_pairs={{2,0},{4,2},{6,4},{0,6},{3,1},{5,3},{7,5},{1,7},{10,8},{12,10},{14... | collective-permute-start | bytes 3145736 | tf_op jit(solution)/shard_map/ppermute | solution.py:352
  104.5 29.0 %collective-permute-start.2 = (bf16[256,2048]{1,0:T(8,128)(2,1)}, bf16[256,2048]{1,0:T(8,128)(2,1)}, u32[]{:S(2)}, u32[]{:S(2)}) collective-permute-start(bf16[256,2048]{1,0:T(8,128)(2,1)} %collective-permute-done.refs_1_), channel_id=1, source_target_pairs={{0,2},{2,4},{4,6},{6,0},{1,3},{3,5},{5,7},{7,1},{8,10},{10,12},{12... | collective-permute-start | bytes 3145736 | tf_op jit(solution)/shard_map/ppermute | solution.py:351
  108.8 27.4 %all-to-all-start.2 = ((bf16[4,256,256]{2,1,0:T(8,128)(2,1)}), bf16[4,256,256]{2,1,0:T(8,128)(2,1)S(1)}, u32[]{:S(2)}, u32[]{:S(2)}) async-start(bf16[4,256,256]{2,1,0:T(8,128)(2,1)} %join.1), calls=%async_computation.2 | async-start | bytes 1048576 | tf_op jit(solution)/shard_map/all_to_all | solution.py:268
  113.1 28.2 %slice-start = ((f32[3,704]{1,0:T(4,128)}), f32[3,640]{1,0:T(4,128)S(1)}, s32[]{:S(2)}) async-start(f32[3,704]{1,0:T(4,128)} %param.26), calls=%async_computation.5 | async-start | bytes 20480 | tf_op jit(solution)/shard_map/slice | solution.py:410
  113.1 28.2 %slice-start.1 = ((f32[3,704]{1,0:T(4,128)}), f32[3,64]{1,0:T(4,128)S(1)}, s32[]{:S(2)}) async-start(f32[3,704]{1,0:T(4,128)} %param.26), calls=%async_computation.6 | async-start | bytes 4096 | tf_op jit(solution)/shard_map/slice | solution.py:410
  113.1 30.0 %copy-start.2 = (f32[2048]{0:T(1024)S(1)}, f32[2048]{0:T(1024)}, u32[]{:S(2)}) copy-start(f32[2048]{0:T(1024)} %param.23) | copy-start | bytes 24580
  139.4 3.8 %collective-permute-start.3 = (bf16[128,2048]{1,0:T(8,128)(2,1)S(1)}, bf16[128,2048]{1,0:T(8,128)(2,1)S(1)}, u32[]{:S(2)}, u32[]{:S(2)}) collective-permute-start(bf16[128,2048]{1,0:T(8,128)(2,1)S(1)} %get-tuple-element.18), channel_id=1, source_target_pairs={{0,1},{1,0},{2,3},{3,2},{4,5},{5,4},{6,7},{7,6},{8,9},{9,8},{10,11... | collective-permute-start | bytes 1572872 | tf_op jit(solution)/shard_map/ppermute | solution.py:374
  146.0 9.0 %collective-permute-start.4 = (bf16[16,768]{1,0:T(8,128)(2,1)S(1)}, bf16[16,768]{1,0:T(8,128)(2,1)S(1)}, u32[]{:S(2)}, u32[]{:S(2)}) collective-permute-start(bf16[16,768]{1,0:T(8,128)(2,1)S(1)} %get-tuple-element.21), channel_id=1, source_target_pairs={{0,8},{8,16},{16,24},{24,32},{32,40},{40,48},{48,56},{56,64},{64,7... | collective-permute-start | bytes 73736 | tf_op jit(solution)/shard_map/ppermute | solution.py:393
  147.9 7.1 %copy-start = (bf16[704,2048]{1,0:T(8,128)(2,1)S(1)}, bf16[704,2048]{1,0:T(8,128)(2,1)}, u32[]{:S(2)}) copy-start(bf16[704,2048]{1,0:T(8,128)(2,1)} %weight.1) | copy-start | bytes 8650756
  156.7 3.4 %collective-permute-start.5 = (bf16[64,2048]{1,0:T(8,128)(2,1)S(1)}, bf16[64,2048]{1,0:T(8,128)(2,1)S(1)}, u32[]{:S(2)}, u32[]{:S(2)}) collective-permute-start(bf16[64,2048]{1,0:T(8,128)(2,1)S(1)} %get-tuple-element.23), channel_id=1, source_target_pairs={{0,1},{1,0},{2,3},{3,2},{4,5},{5,4},{6,7},{7,6},{8,9},{9,8},{10,11... | collective-permute-start | bytes 786440 | tf_op jit(solution)/shard_map/ppermute | solution.py:423
Sparse Core Ops, SparseCore 0:
  39.3 60.1 all-gather.1

commit v9 on v8

--- a/solution.py
+++ b/solution.py
@@ -68,7 +68,7 @@
         copy.wait()
 
 
-def attend_kernel(plan, qpool, kpool, out):
+def attend_kernel(plan, qpool, kpool, result, out, sems):
     q_base, q_step, k_base, k_step = (plan[i] for i in range(4))
     at = lax.broadcasted_iota(jnp.int32, (16, 128), 0)
     row = lax.broadcasted_iota(jnp.int32, (256, 1), 0)
@@ -110,6 +110,11 @@
                 for n, piece in enumerate((a, b, d)):
                     rows = jnp.where(at == 3 * m + n, piece, rows)
             out[2 * c + h, 512:528, :] = rows.astype(bf16)
+        pair = pl.ds(2 * c, 2)
+        pltpu.make_async_copy(out.at[pair], result.at[pair], sems.at[c]).start()
+    for c in range(SIDE // 2):
+        pair = pl.ds(2 * c, 2)
+        pltpu.make_async_copy(out.at[pair], result.at[pair], sems.at[c]).wait()
 
 
 def join_kernel(mix, parts, gain, residual, out):
@@ -186,14 +191,11 @@
             pltpu.make_async_copy(weights.at[g, :, rows, :], buffer.at[g], sems.at[g]).start()
 
 
-def multiplied(rows, weights, buffer, sems, first):
-    height = buffer.shape[2]
-    count = height // 32
+def multiplied(rows, buffer, ready):
+    count = buffer.shape[2] // 32
     acc = [None] * ((count + 1) // 2)
     for g in range(SIDE):
-        pltpu.make_async_copy(
-            weights.at[0, :, pl.ds(first, height), :], buffer.at[g], sems.at[g]
-        ).wait()
+        ready(g)
         lhs = rows[:, 256 * g : 256 * g + 256]
         for n in range(0, count, 2):
             tiles = [
@@ -206,23 +208,33 @@
     return acc
 
 
-def gate_kernel(place, half, other, gain, weights, gated, edge, rows, stream, buffer, sems):
+def gate_kernel(place, half, other, gain, weights, gated, edge, rows, stream, later, buffer, sems, more):
     fetched(place[0], weights, buffer, sems, 0)
+    fetched(place[0], weights, later, more, 192)
     for n in range(0, 128, 32):
         total = half[n : n + 32] + other[n : n + 32].astype(f32)
         r = lax.rsqrt(jnp.mean(total * total, axis=-1, keepdims=True) + epsilon)
         rows[n : n + 32] = (total * r * gain[...]).astype(bf16)
     own = pl.ds(pl.multiple_of(place[2] * 16, 16), 16)
     stream[...] = half[own] + other[own].astype(f32)
-    for n, part in enumerate(multiplied(rows, weights, buffer, sems, 0)):
+
+    def ready(g):
+        pltpu.make_async_copy(
+            weights.at[0, :, pl.ds(0, 192), :], buffer.at[g], sems.at[g]
+        ).wait()
+
+    for n, part in enumerate(multiplied(rows, buffer, ready)):
         part = part.astype(bf16)
         gated[:, 256 * n : 256 * n + 256] = part
         edge[:, 256 * n : 256 * n + 256] = part[112:128]
-
-
-def lift_kernel(core, rows, weights, lifted, buffer, sems):
-    fetched(core[0], weights, buffer, sems, 192)
-    for n, part in enumerate(multiplied(rows, weights, buffer, sems, 192)):
+    for g in range(SIDE):
+        pltpu.make_async_copy(
+            weights.at[0, :, pl.ds(192, 160), :], later.at[g], more.at[g]
+        ).wait()
+
+
+def lift_kernel(rows, weights, lifted):
+    for n, part in enumerate(multiplied(rows, weights, lambda g: None)):
         lifted[:, 256 * n : 256 * n + part.shape[1]] = part.astype(bf16)
 
 
@@ -336,14 +348,13 @@
     above = lax.ppermute(out_weight, "x", ring)
     out = pl.pallas_call(
         attend_kernel,
-        grid=(1,),
-        out_shape=jax.ShapeDtypeStruct((SIDE, PACK, 128), bf16),
-        in_specs=[
-            pl.BlockSpec(memory_space=pltpu.SMEM),
-            vmem(),
-            pl.BlockSpec((SIDE, 512, 128), lambda i: (0, 0, 0)),
-        ],
-        out_specs=vmem(),
+        out_shape=pltpu.HBM((SIDE, PACK, 128), bf16),
+        in_specs=[pl.BlockSpec(memory_space=pltpu.SMEM), vmem(), vmem()],
+        out_specs=hbm,
+        scratch_shapes=[
+            pltpu.VMEM((SIDE, PACK, 128), bf16),
+            pltpu.SemaphoreType.DMA((SIDE // 2,)),
+        ],
         compiler_params=LARGE,
         name="attend",
     )(plan, qpool, kpool)
@@ -372,18 +383,20 @@
         name="project",
     )(place, heads, *(in_hbm(a) for a in (out_weight, above, below, across)))
     other = lax.ppermute(sent, "core", [(0, 1), (1, 0)])
-    gated, edge, rows, stream = pl.pallas_call(
+    gated, edge, rows, stream, later = pl.pallas_call(
         gate_kernel,
         out_shape=[
             jax.ShapeDtypeStruct((tokens, MAIN + 128), bf16),
             jax.ShapeDtypeStruct((16, MAIN + 128), bf16),
             jax.ShapeDtypeStruct((tokens, width), bf16),
             jax.ShapeDtypeStruct((own, width), f32),
+            jax.ShapeDtypeStruct((SIDE, SIDE, 160, 128), bf16),
         ],
         in_specs=[smem] + [vmem()] * 3 + [hbm],
-        out_specs=[vmem()] * 4,
+        out_specs=[vmem()] * 5,
         scratch_shapes=[
             pltpu.VMEM((SIDE, SIDE, 192, 128), bf16),
+            pltpu.SemaphoreType.DMA((SIDE,)),
             pltpu.SemaphoreType.DMA((SIDE,)),
         ],
         compiler_params=SMALL,
@@ -394,18 +407,14 @@
     lifted = pl.pallas_call(
         lift_kernel,
         out_shape=jax.ShapeDtypeStruct((tokens, MAIN), bf16),
-        in_specs=[smem, vmem(), hbm],
+        in_specs=[vmem()] * 2,
         out_specs=vmem(),
-        scratch_shapes=[
-            pltpu.VMEM((SIDE, SIDE, 160, 128), bf16),
-            pltpu.SemaphoreType.DMA((SIDE,)),
-        ],
         compiler_params=SMALL,
         cost_estimate=pl.CostEstimate(
             flops=2 * 128 * 2048 * 640, bytes_accessed=3 << 20, transcendentals=0
         ),
         name="lift",
-    )(place, rows, weights)
+    )(rows, later)
     gap = jnp.zeros((WIDTH, 64), f32)
     taps = jnp.concatenate([conv_taps[:, :MAIN], gap, conv_taps[:, MAIN:]], axis=1)
     keep, give = pl.pallas_call(

time: 178 us -> 179 us (level)
  waiting for transfers between devices: 49.6 us -> 52.6 us
  Pallas kernels: 22 us -> 19.4 us
    ppermute x1, waiting for transfers between devices: 3.51 us -> 6.53 us  [on_device(): prior = lax.ppermute(edge, ('z', 'y'), route)]
    pallas_call x1, Pallas kernels: 3.58 us -> 0.58 us  [on_device(): pl.pallas_call(lift_kernel, out_shape=jax.ShapeDtypeStruct((tokens, MAIN)...]
  transfers between devices with their start and end apart: 9 -> 9, of which waited for: 6 -> 6; matrix products, arithmetic and copies ran while one was open for 0% -> 0% of each run, Pallas kernels for 8% -> 6%
where the time goes in v9:
time: 179 us; the launch traced here: 178 us
  blocking collectives  65.2 us (36%)
  waiting for transfers between devices  52.6 us (29%)
  starting transfers between devices  25.4 us (14%)
  Pallas kernels  19.4 us (11%)
  between operations  14.2 us (8%)
    all_to_all x2, blocking collectives, swapped(): return lax.all_to_all(a, axis, 0, 0, axis_index_groups=groups, tiled=True)  37.9 us
    all_gather x1, blocking collectives, gathered(): return lax.all_gather(a, axis, axis_index_groups=groups, axis=0, tiled=True)  27.2 us
    ppermute x1, waiting for transfers between devices, on_device(): across = lax.ppermute(above, 'x', ring)  20.3 us
    ppermute x1, waiting for transfers between devices, on_device(): above = lax.ppermute(out_weight, 'x', ring)  19.8 us
    all_to_all x2, starting transfers between devices, swapped(): return lax.all_to_all(a, axis, 0, 0, axis_index_groups=groups, tiled=True)  10.1 us
    ppermute x1, waiting for transfers between devices, on_device(): prior = lax.ppermute(edge, ('z', 'y'), route)  6.53 us
    pallas_call x1, Pallas kernels, on_device(): pl.pallas_call(attend_kernel, out_shape=pltpu.HBM((SIDE, PACK, 128), bf16...  5.03 us
    ppermute x1, starting transfers between devices, on_device(): below = lax.ppermute(out_weight, 'x', [(j, i) for i, j in ring])  3.61 us
  transfers between devices with their start and end apart: 9, of which 6 were waited for; matrix products, arithmetic and copies ran while one was open for 0% of the time, Pallas kernels for 6%

profile of v9, /device:TPU:256, one launch (start us, length us, event | category | flops | bytes accessed | tf_op | source)
XLA Modules:
  0.0 178.0 jit_solution(9400404483382067365)
XLA Ops:
  6.5 3.4 %pack.1 = (bf16[256,128]{1,0:T(8,128)(2,1)S(1)}, bf16[8,864,128]{2,1,0:T(8,128)(2,1)S(1)}) custom-call(bf16[128,128]{1,0:T(8,128)(2,1)} %q1.1, bf16[128,128]{1,0:T(8,128)(2,1)} %q2.1, bf16[128,128]{1,0:T(8,128)(2,1)} %k1.1, bf16[128,128]{1,0:T(8,128)(2,1)} %k2.1, bf16[128,256]{1,0:T(8,128)(2,1)} %v.1, bf16[32,704]{1,0:T(8,128)(2,1)} %lift.2, ...), custom_call_target="tpu_custom_call" | custom-call | tf_op jit(solution)/shard_map/pack/pallas_call | solution.py:324
  9.9 28.3 %all_to_all.20.kpool = bf16[8,864,128]{2,1,0:T(8,128)(2,1)S(1)} all-to-all(bf16[8,864,128]{2,1,0:T(8,128)(2,1)S(1)} %get-tuple-element.17), channel_id=1, replica_groups={{0,64,128,192,256,320,384,448},{2,66,130,194,258,322,386,450},{4,68,132..., dimensions={0} | all-to-all | bytes 3538944 | tf_op jit(solution)/shard_map/all_to_all | solution.py:280
  38.2 0.9 slice.12
  39.3 27.2 %all_gather.6 = bf16[2048,128]{1,0:T(8,128)(2,1)S(1)} all-gather(bf16[256,128]{1,0:T(8,128)(2,1)S(1)} %get-tuple-element.16), channel_id=1, replica_groups={{0,8,16,24,32,40,48,56},{2,10,18,26,34,42,50,58},{4,12,20,28,36,44,52,6..., dimensions={0}, use_global_device_ids=true | all-gather | bytes 589824 | tf_op jit(solution)/shard_map/all_gather | solution.py:284
  66.5 5.0 %attend.1 = bf16[8,528,128]{2,1,0:T(8,128)(2,1)} custom-call(s32[4]{0:T(128)S(1)} %broadcast_select_fusion.plan, bf16[8,256,128]{2,1,0:T(8,128)(2,1)S(1)} %bitcast.10, bf16[8,864,128]{2,1,0:T(8,128)(2,1)S(1)} %all_to_all.20.kpool), custom_call_target="tpu_custom_call" | custom-call | tf_op jit(solution)/shard_map/attend/pallas_call | solution.py:349
  71.6 5.9 %all-to-all-start.1 = ((bf16[8,528,128]{2,1,0:T(8,128)(2,1)}), bf16[8,528,128]{2,1,0:T(8,128)(2,1)S(1)}, u32[]{:S(2)}, u32[]{:S(2)}) async-start(bf16[8,528,128]{2,1,0:T(8,128)(2,1)} %attend.1), calls=%async_computation.1 | async-start | bytes 2162688 | tf_op jit(solution)/shard_map/all_to_all | solution.py:280
  77.5 3.5 %collective-permute-start = (bf16[256,2048]{1,0:T(8,128)(2,1)S(1)}, bf16[256,2048]{1,0:T(8,128)(2,1)}, u32[]{:S(2)}, u32[]{:S(2)}) collective-permute-start(bf16[256,2048]{1,0:T(8,128)(2,1)S(1)} %copy-done.4), channel_id=1, source_target_pairs={{0,2},{2,4},{4,6},{6,0},{1,3},{3,5},{5,7},{7,1},{8,10},{10,12},{12... | collective-permute-start | bytes 3145736 | tf_op jit(solution)/shard_map/ppermute | solution.py:348
  81.0 3.6 %collective-permute-start.1 = (bf16[256,2048]{1,0:T(8,128)(2,1)S(1)}, bf16[256,2048]{1,0:T(8,128)(2,1)}, u32[]{:S(2)}, u32[]{:S(2)}) collective-permute-start(bf16[256,2048]{1,0:T(8,128)(2,1)S(1)} %copy-done.4), channel_id=1, source_target_pairs={{2,0},{4,2},{6,4},{0,6},{3,1},{5,3},{7,5},{1,7},{10,8},{12,10},{14... | collective-permute-start | bytes 3145736 | tf_op jit(solution)/shard_map/ppermute | solution.py:363
  84.6 19.8 %collective-permute-done.refs_1_ = bf16[256,2048]{1,0:T(8,128)(2,1)} collective-permute-done((bf16[256,2048]{1,0:T(8,128)(2,1)S(1)}, bf16[256,2048]{1,0:T(8,128)(2,1)}, u32[]{:S(2)}, u32[]{:S(2)}) %collective-permute-start) | collective-permute-done | bytes 1048608 | tf_op jit(solution)/shard_map/ppermute | solution.py:348
  104.3 2.2 %collective-permute-start.2 = (bf16[256,2048]{1,0:T(8,128)(2,1)}, bf16[256,2048]{1,0:T(8,128)(2,1)}, u32[]{:S(2)}, u32[]{:S(2)}) collective-permute-start(bf16[256,2048]{1,0:T(8,128)(2,1)} %collective-permute-done.refs_1_), channel_id=1, source_target_pairs={{0,2},{2,4},{4,6},{6,0},{1,3},{3,5},{5,7},{7,1},{8,10},{10,12},{12... | collective-permute-start | bytes 3145736 | tf_op jit(solution)/shard_map/ppermute | solution.py:362
  107.2 1.5 join.1
  108.7 4.2 %all-to-all-start.2 = ((bf16[4,256,256]{2,1,0:T(8,128)(2,1)}), bf16[4,256,256]{2,1,0:T(8,128)(2,1)S(1)}, u32[]{:S(2)}, u32[]{:S(2)}) async-start(bf16[4,256,256]{2,1,0:T(8,128)(2,1)} %join.1), calls=%async_computation.2 | async-start | bytes 1048576 | tf_op jit(solution)/shard_map/all_to_all | solution.py:280
  113.0 20.3 %collective-permute-done.2.refs_3_ = bf16[256,2048]{1,0:T(8,128)(2,1)} collective-permute-done((bf16[256,2048]{1,0:T(8,128)(2,1)}, bf16[256,2048]{1,0:T(8,128)(2,1)}, u32[]{:S(2)}, u32[]{:S(2)}) %collective-permute-start.2) | collective-permute-done | bytes 1048608 | tf_op jit(solution)/shard_map/ppermute | solution.py:362
  133.3 2.7 %all-to-all-done.2.heads = bf16[4,256,256]{2,1,0:T(8,128)(2,1)S(1)} async-done(((bf16[4,256,256]{2,1,0:T(8,128)(2,1)}), bf16[4,256,256]{2,1,0:T(8,128)(2,1)S(1)}, u32[]{:S(2)}, u32[]{:S(2)}) %all-to-all-start.2) | async-done | bytes 524320 | tf_op jit(solution)/shard_map/all_to_all | solution.py:280
  136.0 3.2 %project.1 = (f32[128,2048]{1,0:T(8,128)S(1)}, bf16[128,2048]{1,0:T(8,128)(2,1)S(1)}) custom-call(s32[3]{0:T(128)S(1)} %pad_add_fusion.place, bf16[4,256,256]{2,1,0:T(8,128)(2,1)S(1)} %all-to-all-done.2.heads, bf16[256,2048]{1,0:T(8,128)(2,1)} %refs_0_.1, bf16[256,2048]{1,0:T(8,128)(2,1)} %collective-permute-done.refs_1_, ...), custom_call_target="tpu_custom_call" | custom-call | tf_op jit(solution)/shard_map/project/pallas_call | solution.py:373
  139.2 1.9 %collective-permute-start.3 = (bf16[128,2048]{1,0:T(8,128)(2,1)S(1)}, bf16[128,2048]{1,0:T(8,128)(2,1)S(1)}, u32[]{:S(2)}, u32[]{:S(2)}) collective-permute-start(bf16[128,2048]{1,0:T(8,128)(2,1)S(1)} %get-tuple-element.19), channel_id=1, source_target_pairs={{0,1},{1,0},{2,3},{3,2},{4,5},{5,4},{6,7},{7,6},{8,9},{9,8},{10,11... | collective-permute-start | bytes 1572872 | tf_op jit(solution)/shard_map/ppermute | solution.py:385
  141.2 1.8 collective-permute-done.3.other
  143.0 3.5 %gate.3 = (bf16[128,768]{1,0:T(8,128)(2,1)S(1)}, bf16[16,768]{1,0:T(8,128)(2,1)S(1)}, bf16[128,2048]{1,0:T(8,128)(2,1)S(1)}, f32[16,2048]{1,0:T(8,128)S(1)}, bf16[8,8,160,128]{3,2,1,0:T(8,128)(2,1)S(1)}) custom-call(s32[3]{0:T(128)S(1)} %pad_add_fusion.place, f32[128,2048]{1,0:T(8,128)S(1)} %get-tuple-element.18.half, ...), custom_call_target="tpu_custom_call" | custom-call | tf_op jit(solution)/shard_map/gate/pallas_call | solution.py:386
  146.5 2.2 %collective-permute-start.4 = (bf16[16,768]{1,0:T(8,128)(2,1)S(1)}, bf16[16,768]{1,0:T(8,128)(2,1)S(1)}, u32[]{:S(2)}, u32[]{:S(2)}) collective-permute-start(bf16[16,768]{1,0:T(8,128)(2,1)S(1)} %get-tuple-element.23), channel_id=1, source_target_pairs={{0,8},{8,16},{16,24},{24,32},{32,40},{40,48},{48,56},{56,64},{64,7... | collective-permute-start | bytes 73736 | tf_op jit(solution)/shard_map/ppermute | solution.py:406
  149.3 6.5 %collective-permute-done.4.prior = bf16[16,768]{1,0:T(8,128)(2,1)S(1)} collective-permute-done((bf16[16,768]{1,0:T(8,128)(2,1)S(1)}, bf16[16,768]{1,0:T(8,128)(2,1)S(1)}, u32[]{:S(2)}, u32[]{:S(2)}) %collective-permute-start.4) | collective-permute-done | bytes 24608 | tf_op jit(solution)/shard_map/ppermute | solution.py:406
  155.8 1.6 down.1
  157.4 1.9 %collective-permute-start.5 = (bf16[64,2048]{1,0:T(8,128)(2,1)S(1)}, bf16[64,2048]{1,0:T(8,128)(2,1)S(1)}, u32[]{:S(2)}, u32[]{:S(2)}) collective-permute-start(bf16[64,2048]{1,0:T(8,128)(2,1)S(1)} %get-tuple-element.25), channel_id=1, source_target_pairs={{0,1},{1,0},{2,3},{3,2},{4,5},{5,4},{6,7},{7,6},{8,9},{9,8},{10,11... | collective-permute-start | bytes 786440 | tf_op jit(solution)/shard_map/ppermute | solution.py:432
  159.3 1.5 collective-permute-done.5.other
  160.9 9.6 %all_to_all.21.parts = bf16[4,16,2048]{2,1,0:T(8,128)(2,1)S(1)} all-to-all(bf16[4,16,2048]{2,1,0:T(8,128)(2,1)S(1)} %pair.1), channel_id=1, replica_groups=mesh['z'=8,'y'=8,'x'=4,'core'=2] {'x'}, dimensions={0} | all-to-all | bytes 524288 | tf_op jit(solution)/shard_map/all_to_all | solution.py:280
  (27 shorter events, 1.6 us)
Async XLA Ops:
  6.5 136.4 %all-gather.2.cloned.1.call-start = ((), (), s32[]{:S(2)}) async-start(), calls=%async_computation.4 | async-start | bytes 6488064 | tf_op jit(solution)/shard_map/all_gather | solution.py:284
  71.6 5.9 %copy-start.4 = (bf16[256,2048]{1,0:T(8,128)(2,1)S(1)}, bf16[256,2048]{1,0:T(8,128)(2,1)}, u32[]{:S(2)}) copy-start(bf16[256,2048]{1,0:T(8,128)(2,1)} %refs_0_.1) | copy-start | bytes 3145732
  71.6 35.6 %copy-start.1 = (bf16[16,2048]{1,0:T(8,128)(2,1)S(1)}, bf16[16,2048]{1,0:T(8,128)(2,1)}, u32[]{:S(2)}) copy-start(bf16[16,2048]{1,0:T(8,128)(2,1)} %residual.1) | copy-start | bytes 196612
  71.6 35.6 %copy-start.3 = (f32[256]{0:T(256)S(1)}, f32[256]{0:T(256)}, u32[]{:S(2)}) copy-start(f32[256]{0:T(256)} %param.20) | copy-start | bytes 3076
  71.6 35.5 %all-to-all-start.1 = ((bf16[8,528,128]{2,1,0:T(8,128)(2,1)}), bf16[8,528,128]{2,1,0:T(8,128)(2,1)S(1)}, u32[]{:S(2)}, u32[]{:S(2)}) async-start(bf16[8,528,128]{2,1,0:T(8,128)(2,1)} %attend.1), calls=%async_computation.1 | async-start | bytes 2162688 | tf_op jit(solution)/shard_map/all_to_all | solution.py:280
  77.5 26.8 %collective-permute-start = (bf16[256,2048]{1,0:T(8,128)(2,1)S(1)}, bf16[256,2048]{1,0:T(8,128)(2,1)}, u32[]{:S(2)}, u32[]{:S(2)}) collective-permute-start(bf16[256,2048]{1,0:T(8,128)(2,1)S(1)} %copy-done.4), channel_id=1, source_target_pairs={{0,2},{2,4},{4,6},{6,0},{1,3},{3,5},{5,7},{7,1},{8,10},{10,12},{12... | collective-permute-start | bytes 3145736 | tf_op jit(solution)/shard_map/ppermute | solution.py:348
  81.0 32.0 %collective-permute-start.1 = (bf16[256,2048]{1,0:T(8,128)(2,1)S(1)}, bf16[256,2048]{1,0:T(8,128)(2,1)}, u32[]{:S(2)}, u32[]{:S(2)}) collective-permute-start(bf16[256,2048]{1,0:T(8,128)(2,1)S(1)} %copy-done.4), channel_id=1, source_target_pairs={{2,0},{4,2},{6,4},{0,6},{3,1},{5,3},{7,5},{1,7},{10,8},{12,10},{14... | collective-permute-start | bytes 3145736 | tf_op jit(solution)/shard_map/ppermute | solution.py:363
  104.3 29.0 %collective-permute-start.2 = (bf16[256,2048]{1,0:T(8,128)(2,1)}, bf16[256,2048]{1,0:T(8,128)(2,1)}, u32[]{:S(2)}, u32[]{:S(2)}) collective-permute-start(bf16[256,2048]{1,0:T(8,128)(2,1)} %collective-permute-done.refs_1_), channel_id=1, source_target_pairs={{0,2},{2,4},{4,6},{6,0},{1,3},{3,5},{5,7},{7,1},{8,10},{10,12},{12... | collective-permute-start | bytes 3145736 | tf_op jit(solution)/shard_map/ppermute | solution.py:362
  108.7 27.4 %all-to-all-start.2 = ((bf16[4,256,256]{2,1,0:T(8,128)(2,1)}), bf16[4,256,256]{2,1,0:T(8,128)(2,1)S(1)}, u32[]{:S(2)}, u32[]{:S(2)}) async-start(bf16[4,256,256]{2,1,0:T(8,128)(2,1)} %join.1), calls=%async_computation.2 | async-start | bytes 1048576 | tf_op jit(solution)/shard_map/all_to_all | solution.py:280
  113.0 28.2 %slice-start = ((f32[3,704]{1,0:T(4,128)}), f32[3,640]{1,0:T(4,128)S(1)}, s32[]{:S(2)}) async-start(f32[3,704]{1,0:T(4,128)} %param.26), calls=%async_computation.5 | async-start | bytes 20480 | tf_op jit(solution)/shard_map/slice | solution.py:419
  113.0 28.2 %slice-start.1 = ((f32[3,704]{1,0:T(4,128)}), f32[3,64]{1,0:T(4,128)S(1)}, s32[]{:S(2)}) async-start(f32[3,704]{1,0:T(4,128)} %param.26), calls=%async_computation.6 | async-start | bytes 4096 | tf_op jit(solution)/shard_map/slice | solution.py:419
  113.0 30.0 %copy-start.2 = (f32[2048]{0:T(1024)S(1)}, f32[2048]{0:T(1024)}, u32[]{:S(2)}) copy-start(f32[2048]{0:T(1024)} %param.23) | copy-start | bytes 24580
  139.2 3.8 %collective-permute-start.3 = (bf16[128,2048]{1,0:T(8,128)(2,1)S(1)}, bf16[128,2048]{1,0:T(8,128)(2,1)S(1)}, u32[]{:S(2)}, u32[]{:S(2)}) collective-permute-start(bf16[128,2048]{1,0:T(8,128)(2,1)S(1)} %get-tuple-element.19), channel_id=1, source_target_pairs={{0,1},{1,0},{2,3},{3,2},{4,5},{5,4},{6,7},{7,6},{8,9},{9,8},{10,11... | collective-permute-start | bytes 1572872 | tf_op jit(solution)/shard_map/ppermute | solution.py:385
  146.5 9.3 %copy-start = (bf16[704,2048]{1,0:T(8,128)(2,1)S(1)}, bf16[704,2048]{1,0:T(8,128)(2,1)}, u32[]{:S(2)}) copy-start(bf16[704,2048]{1,0:T(8,128)(2,1)} %weight.1) | copy-start | bytes 8650756
  146.5 9.3 %collective-permute-start.4 = (bf16[16,768]{1,0:T(8,128)(2,1)S(1)}, bf16[16,768]{1,0:T(8,128)(2,1)S(1)}, u32[]{:S(2)}, u32[]{:S(2)}) collective-permute-start(bf16[16,768]{1,0:T(8,128)(2,1)S(1)} %get-tuple-element.23), channel_id=1, source_target_pairs={{0,8},{8,16},{16,24},{24,32},{32,40},{40,48},{48,56},{56,64},{64,7... | collective-permute-start | bytes 73736 | tf_op jit(solution)/shard_map/ppermute | solution.py:406
  157.4 3.4 %collective-permute-start.5 = (bf16[64,2048]{1,0:T(8,128)(2,1)S(1)}, bf16[64,2048]{1,0:T(8,128)(2,1)S(1)}, u32[]{:S(2)}, u32[]{:S(2)}) collective-permute-start(bf16[64,2048]{1,0:T(8,128)(2,1)S(1)} %get-tuple-element.25), channel_id=1, source_target_pairs={{0,1},{1,0},{2,3},{3,2},{4,5},{5,4},{6,7},{7,6},{8,9},{9,8},{10,11... | collective-permute-start | bytes 786440 | tf_op jit(solution)/shard_map/ppermute | solution.py:432
Sparse Core Ops, SparseCore 0:
  39.3 60.1 all-gather.1

commit v10 on v9

--- a/solution.py
+++ b/solution.py
@@ -15,7 +15,7 @@
 PACK = 4 * BLOCK + 16
 TILES = 5
 MAIN = 128 * TILES
-SENT = 512 + 352
+SENT = 512
 SHIFTS = (0, 1, -1, 2)
 epsilon = 1e-06
 masked_score = -1e30
@@ -36,7 +36,7 @@
     return pl.BlockSpec(memory_space=pltpu.VMEM)
 
 
-def pack_kernel(q1, q2, k1, k2, v, lift, gate, qsend, ksend, vv, ll, gg, rows, sems, sent):
+def pack_kernel(q1, q2, k1, k2, v, lift, gate, qsend, ksend, wsend, vv, ll, gg, rows, sems, sent):
     moves = [
         pltpu.make_async_copy(src, dst, sems.at[i])
         for i, (src, dst) in enumerate(
@@ -58,9 +58,9 @@
     rows[256:384, :] = vv[:, 0:128]
     rows[384:512, :] = vv[:, 128:256]
     for n in range(TILES):
-        rows[512 + 32 * n : 544 + 32 * n, :] = gg[:, 128 * n : 128 * n + 128]
-        rows[704 + 32 * n : 736 + 32 * n, :] = ll[:, 128 * n : 128 * n + 128]
-    rows[672:704, :] = jnp.concatenate([ll[:, MAIN:], gg[:, MAIN:]], axis=1)
+        wsend[32 * n : 32 * n + 32, :] = gg[:, 128 * n : 128 * n + 128]
+        wsend[192 + 32 * n : 224 + 32 * n, :] = ll[:, 128 * n : 128 * n + 128]
+    wsend[160:192, :] = jnp.concatenate([ll[:, MAIN:], gg[:, MAIN:]], axis=1)
     copies = [pltpu.make_async_copy(rows, ksend.at[i], sent.at[i]) for i in range(SIDE)]
     for copy in copies:
         copy.start()
@@ -177,18 +177,10 @@
     sent[...] = half[...].astype(bf16)
 
 
-def fetched(core, weights, buffer, sems, first):
-    height = buffer.shape[2]
+def fetched(weights, buffer, sems, first):
+    rows = pl.ds(first, buffer.shape[2])
     for g in range(SIDE):
-        rows = pl.ds(first, height)
-
-        @pl.when(core == 0)
-        def _():
-            pltpu.make_async_copy(weights.at[:, g, rows, :], buffer.at[g], sems.at[g]).start()
-
-        @pl.when(core != 0)
-        def _():
-            pltpu.make_async_copy(weights.at[g, :, rows, :], buffer.at[g], sems.at[g]).start()
+        pltpu.make_async_copy(weights.at[g, :, rows, :], buffer.at[g], sems.at[g]).start()
 
 
 def multiplied(rows, buffer, ready):
@@ -209,8 +201,8 @@
 
 
 def gate_kernel(place, half, other, gain, weights, gated, edge, rows, stream, later, buffer, sems, more):
-    fetched(place[0], weights, buffer, sems, 0)
-    fetched(place[0], weights, later, more, 192)
+    fetched(weights, buffer, sems, 0)
+    fetched(weights, later, more, 192)
     for n in range(0, 128, 32):
         total = half[n : n + 32] + other[n : n + 32].astype(f32)
         r = lax.rsqrt(jnp.mean(total * total, axis=-1, keepdims=True) + epsilon)
@@ -321,14 +313,15 @@
     hbm = pl.BlockSpec(memory_space=pltpu.HBM)
     x = lax.axis_index("x")
     place = jnp.stack([core, x, 2 * x + core]).astype(jnp.int32)
-    qsend, ksend = pl.pallas_call(
+    qsend, ksend, wsend = pl.pallas_call(
         pack_kernel,
         out_shape=[
             jax.ShapeDtypeStruct((256, 128), bf16),
             jax.ShapeDtypeStruct((SIDE, SENT, 128), bf16),
+            pltpu.HBM((352, 128), bf16),
         ],
         in_specs=[hbm] * 7,
-        out_specs=[vmem(), hbm],
+        out_specs=[vmem(), hbm, vmem()],
         scratch_shapes=[
             pltpu.VMEM((128, 256), bf16),
             pltpu.VMEM((32, 704), bf16),
@@ -342,8 +335,7 @@
     )(*(in_hbm(a) for a in (query_one, query_two, key_one, key_two, values, lift_weight, gate_weight)))
     kpool = swapped(ksend, ALL, K_GROUPS)
     qpool = gathered(qsend, ALL, Q_GROUPS).reshape(SIDE, 256, 128)
-    part = kpool[:, 512:, :].reshape(SIDE * 352, 128)
-    weights = in_hbm(gathered(part, ALL, Q_GROUPS).reshape(SIDE, SIDE, 352, 128))
+    weights = in_hbm(gathered(wsend, ("z", "y")).reshape(SIDE, SIDE, 352, 128))
     ring = [(i, (i + 1) % 4) for i in range(4)]
     above = lax.ppermute(out_weight, "x", ring)
     out = pl.pallas_call(

time: 179 us -> 158 us (0.88)
  the two profiles are of different devices: /device:TPU:256 before, /device:TPU:32 now
where the time goes in v10:
time: 158 us
  waiting for transfers between devices  49.9 us (32%)
  blocking collectives  37.4 us (24%)
  starting transfers between devices  37 us (23%)
  Pallas kernels  18.6 us (12%)
  between operations  14.2 us (9%)
    all_gather x1, blocking collectives, gathered(): return lax.all_gather(a, axis, axis_index_groups=groups, axis=0, tiled=True)  27.8 us
    all_to_all x3, starting transfers between devices, swapped(): return lax.all_to_all(a, axis, 0, 0, axis_index_groups=groups, tiled=True)  21.8 us
    ppermute x1, waiting for transfers between devices, on_device(): across = lax.ppermute(above, 'x', ring)  20.1 us
    ppermute x1, waiting for transfers between devices, on_device(): above = lax.ppermute(out_weight, 'x', ring)  19.5 us
    all_to_all x1, blocking collectives, swapped(): return lax.all_to_all(a, axis, 0, 0, axis_index_groups=groups, tiled=True)  9.64 us
    pallas_call x1, Pallas kernels, on_device(): pl.pallas_call(attend_kernel, out_shape=pltpu.HBM((SIDE, PACK, 128), bf16...  5.04 us
    ppermute x1, waiting for transfers between devices, on_device(): prior = lax.ppermute(edge, ('z', 'y'), route)  4.42 us
    ppermute x1, starting transfers between devices, on_device(): below = lax.ppermute(out_weight, 'x', [(j, i) for i, j in ring])  3.66 us
  transfers between devices with their start and end apart: 10, of which 6 were waited for; matrix products, arithmetic and copies ran while one was open for 0% of the time, Pallas kernels for 6%

profile of v10, /device:TPU:32, one launch (start us, length us, event | category | flops | bytes accessed | tf_op | source)
XLA Modules:
  0.0 157.6 jit_solution(13820469028313216073)
XLA Ops:
  6.5 2.7 %pack.1 = (bf16[256,128]{1,0:T(8,128)(2,1)S(1)}, bf16[8,512,128]{2,1,0:T(8,128)(2,1)}, bf16[352,128]{1,0:T(8,128)(2,1)}) custom-call(bf16[128,128]{1,0:T(8,128)(2,1)} %q1.1, bf16[128,128]{1,0:T(8,128)(2,1)} %q2.1, bf16[128,128]{1,0:T(8,128)(2,1)} %k1.1, bf16[128,128]{1,0:T(8,128)(2,1)} %k2.1, bf16[128,256]{1,0:T(8,128)(2,1)} %v.1, bf16[32,704]{1,0:T(8,128)(2,1)} %lift.2, ...), custom_call_target="tpu_custom_call" | custom-call | tf_op jit(solution)/shard_map/pack/pallas_call | solution.py:316
  9.2 10.3 %all-to-all-start = ((bf16[8,512,128]{2,1,0:T(8,128)(2,1)}), bf16[8,512,128]{2,1,0:T(8,128)(2,1)S(1)}, u32[]{:S(2)}, u32[]{:S(2)}) async-start(bf16[8,512,128]{2,1,0:T(8,128)(2,1)} %get-tuple-element.18), calls=%async_computation | async-start | bytes 2097152 | tf_op jit(solution)/shard_map/all_to_all | solution.py:272
  19.7 27.8 %all_gather.6 = bf16[2048,128]{1,0:T(8,128)(2,1)S(1)} all-gather(bf16[256,128]{1,0:T(8,128)(2,1)S(1)} %get-tuple-element.17), channel_id=1, replica_groups={{0,8,16,24,32,40,48,56},{2,10,18,26,34,42,50,58},{4,12,20,28,36,44,52,6..., dimensions={0}, use_global_device_ids=true | all-gather | bytes 589824 | tf_op jit(solution)/shard_map/all_gather | solution.py:276
  47.5 5.0 %attend.1 = bf16[8,528,128]{2,1,0:T(8,128)(2,1)} custom-call(s32[4]{0:T(128)S(1)} %broadcast_select_fusion.plan, bf16[8,256,128]{2,1,0:T(8,128)(2,1)S(1)} %bitcast.9, bf16[8,512,128]{2,1,0:T(8,128)(2,1)S(1)} %all-to-all-done.kpool), custom_call_target="tpu_custom_call" | custom-call | tf_op jit(solution)/shard_map/attend/pallas_call | solution.py:341
  52.5 7.2 %all-to-all-start.1 = ((bf16[8,528,128]{2,1,0:T(8,128)(2,1)}), bf16[8,528,128]{2,1,0:T(8,128)(2,1)S(1)}, u32[]{:S(2)}, u32[]{:S(2)}) async-start(bf16[8,528,128]{2,1,0:T(8,128)(2,1)} %attend.1), calls=%async_computation.1 | async-start | bytes 2162688 | tf_op jit(solution)/shard_map/all_to_all | solution.py:272
  59.7 3.4 %collective-permute-start = (bf16[256,2048]{1,0:T(8,128)(2,1)S(1)}, bf16[256,2048]{1,0:T(8,128)(2,1)}, u32[]{:S(2)}, u32[]{:S(2)}) collective-permute-start(bf16[256,2048]{1,0:T(8,128)(2,1)S(1)} %copy-done.4), channel_id=1, source_target_pairs={{0,2},{2,4},{4,6},{6,0},{1,3},{3,5},{5,7},{7,1},{8,10},{10,12},{12... | collective-permute-start | bytes 3145736 | tf_op jit(solution)/shard_map/ppermute | solution.py:340
  63.1 3.7 %collective-permute-start.1 = (bf16[256,2048]{1,0:T(8,128)(2,1)S(1)}, bf16[256,2048]{1,0:T(8,128)(2,1)}, u32[]{:S(2)}, u32[]{:S(2)}) collective-permute-start(bf16[256,2048]{1,0:T(8,128)(2,1)S(1)} %copy-done.4), channel_id=1, source_target_pairs={{2,0},{4,2},{6,4},{0,6},{3,1},{5,3},{7,5},{1,7},{10,8},{12,10},{14... | collective-permute-start | bytes 3145736 | tf_op jit(solution)/shard_map/ppermute | solution.py:355
  66.8 19.5 %collective-permute-done.refs_1_ = bf16[256,2048]{1,0:T(8,128)(2,1)} collective-permute-done((bf16[256,2048]{1,0:T(8,128)(2,1)S(1)}, bf16[256,2048]{1,0:T(8,128)(2,1)}, u32[]{:S(2)}, u32[]{:S(2)}) %collective-permute-start) | collective-permute-done | bytes 1048608 | tf_op jit(solution)/shard_map/ppermute | solution.py:340
  86.3 2.1 %collective-permute-start.2 = (bf16[256,2048]{1,0:T(8,128)(2,1)}, bf16[256,2048]{1,0:T(8,128)(2,1)}, u32[]{:S(2)}, u32[]{:S(2)}) collective-permute-start(bf16[256,2048]{1,0:T(8,128)(2,1)} %collective-permute-done.refs_1_), channel_id=1, source_target_pairs={{0,2},{2,4},{4,6},{6,0},{1,3},{3,5},{5,7},{7,1},{8,10},{10,12},{12... | collective-permute-start | bytes 3145736 | tf_op jit(solution)/shard_map/ppermute | solution.py:354
  89.1 1.4 join.1
  90.6 4.3 %all-to-all-start.2 = ((bf16[4,256,256]{2,1,0:T(8,128)(2,1)}), bf16[4,256,256]{2,1,0:T(8,128)(2,1)S(1)}, u32[]{:S(2)}, u32[]{:S(2)}) async-start(bf16[4,256,256]{2,1,0:T(8,128)(2,1)} %join.1), calls=%async_computation.2 | async-start | bytes 1048576 | tf_op jit(solution)/shard_map/all_to_all | solution.py:272
  94.9 20.1 %collective-permute-done.2.refs_3_ = bf16[256,2048]{1,0:T(8,128)(2,1)} collective-permute-done((bf16[256,2048]{1,0:T(8,128)(2,1)}, bf16[256,2048]{1,0:T(8,128)(2,1)}, u32[]{:S(2)}, u32[]{:S(2)}) %collective-permute-start.2) | collective-permute-done | bytes 1048608 | tf_op jit(solution)/shard_map/ppermute | solution.py:354
  115.0 2.7 %all-to-all-done.2.heads = bf16[4,256,256]{2,1,0:T(8,128)(2,1)S(1)} async-done(((bf16[4,256,256]{2,1,0:T(8,128)(2,1)}), bf16[4,256,256]{2,1,0:T(8,128)(2,1)S(1)}, u32[]{:S(2)}, u32[]{:S(2)}) %all-to-all-start.2) | async-done | bytes 524320 | tf_op jit(solution)/shard_map/all_to_all | solution.py:272
  117.7 3.2 %project.1 = (f32[128,2048]{1,0:T(8,128)S(1)}, bf16[128,2048]{1,0:T(8,128)(2,1)S(1)}) custom-call(s32[3]{0:T(128)S(1)} %pad_add_fusion.place, bf16[4,256,256]{2,1,0:T(8,128)(2,1)S(1)} %all-to-all-done.2.heads, bf16[256,2048]{1,0:T(8,128)(2,1)} %refs_0_.1, bf16[256,2048]{1,0:T(8,128)(2,1)} %collective-permute-done.refs_1_, ...), custom_call_target="tpu_custom_call" | custom-call | tf_op jit(solution)/shard_map/project/pallas_call | solution.py:365
  120.9 1.9 %collective-permute-start.3 = (bf16[128,2048]{1,0:T(8,128)(2,1)S(1)}, bf16[128,2048]{1,0:T(8,128)(2,1)S(1)}, u32[]{:S(2)}, u32[]{:S(2)}) collective-permute-start(bf16[128,2048]{1,0:T(8,128)(2,1)S(1)} %get-tuple-element.20), channel_id=1, source_target_pairs={{0,1},{1,0},{2,3},{3,2},{4,5},{5,4},{6,7},{7,6},{8,9},{9,8},{10,11... | collective-permute-start | bytes 1572872 | tf_op jit(solution)/shard_map/ppermute | solution.py:377
  122.9 1.8 %collective-permute-done.3.other = bf16[128,2048]{1,0:T(8,128)(2,1)S(1)} collective-permute-done((bf16[128,2048]{1,0:T(8,128)(2,1)S(1)}, bf16[128,2048]{1,0:T(8,128)(2,1)S(1)}, u32[]{:S(2)}, u32[]{:S(2)}) %collective-permute-start.3) | collective-permute-done | bytes 524320 | tf_op jit(solution)/shard_map/ppermute | solution.py:377
  124.7 3.5 %gate.3 = (bf16[128,768]{1,0:T(8,128)(2,1)S(1)}, bf16[16,768]{1,0:T(8,128)(2,1)S(1)}, bf16[128,2048]{1,0:T(8,128)(2,1)S(1)}, f32[16,2048]{1,0:T(8,128)S(1)}, bf16[8,8,160,128]{3,2,1,0:T(8,128)(2,1)S(1)}) custom-call(s32[3]{0:T(128)S(1)} %pad_add_fusion.place, f32[128,2048]{1,0:T(8,128)S(1)} %get-tuple-element.19.half, ...), custom_call_target="tpu_custom_call" | custom-call | tf_op jit(solution)/shard_map/gate/pallas_call | solution.py:378
  128.1 2.2 %collective-permute-start.4 = (bf16[16,768]{1,0:T(8,128)(2,1)S(1)}, bf16[16,768]{1,0:T(8,128)(2,1)S(1)}, u32[]{:S(2)}, u32[]{:S(2)}) collective-permute-start(bf16[16,768]{1,0:T(8,128)(2,1)S(1)} %get-tuple-element.25), channel_id=1, source_target_pairs={{0,8},{8,16},{16,24},{24,32},{32,40},{40,48},{48,56},{56,64},{64,7... | collective-permute-start | bytes 73736 | tf_op jit(solution)/shard_map/ppermute | solution.py:398
  130.9 4.4 %collective-permute-done.4.prior = bf16[16,768]{1,0:T(8,128)(2,1)S(1)} collective-permute-done((bf16[16,768]{1,0:T(8,128)(2,1)S(1)}, bf16[16,768]{1,0:T(8,128)(2,1)S(1)}, u32[]{:S(2)}, u32[]{:S(2)}) %collective-permute-start.4) | collective-permute-done | bytes 24608 | tf_op jit(solution)/shard_map/ppermute | solution.py:398
  135.3 1.6 down.1
  136.9 1.9 %collective-permute-start.5 = (bf16[64,2048]{1,0:T(8,128)(2,1)S(1)}, bf16[64,2048]{1,0:T(8,128)(2,1)S(1)}, u32[]{:S(2)}, u32[]{:S(2)}) collective-permute-start(bf16[64,2048]{1,0:T(8,128)(2,1)S(1)} %get-tuple-element.27), channel_id=1, source_target_pairs={{0,1},{1,0},{2,3},{3,2},{4,5},{5,4},{6,7},{7,6},{8,9},{9,8},{10,11... | collective-permute-start | bytes 786440 | tf_op jit(solution)/shard_map/ppermute | solution.py:424
  138.8 1.5 collective-permute-done.5.other
  140.4 9.6 %all_to_all.20.parts = bf16[4,16,2048]{2,1,0:T(8,128)(2,1)S(1)} all-to-all(bf16[4,16,2048]{2,1,0:T(8,128)(2,1)S(1)} %pair.1), channel_id=1, replica_groups=mesh['z'=8,'y'=8,'x'=4,'core'=2] {'x'}, dimensions={0} | all-to-all | bytes 524288 | tf_op jit(solution)/shard_map/all_to_all | solution.py:272
  150.0 0.7 last.1
  (27 shorter events, 0.9 us)
Async XLA Ops:
  6.5 118.1 %all-gather.2.cloned.1.call-start = ((), (), s32[]{:S(2)}) async-start(), calls=%async_computation.4 | async-start | bytes 5857280 | tf_op jit(solution)/shard_map/all_gather | solution.py:276
  9.2 38.2 %all-to-all-start = ((bf16[8,512,128]{2,1,0:T(8,128)(2,1)}), bf16[8,512,128]{2,1,0:T(8,128)(2,1)S(1)}, u32[]{:S(2)}, u32[]{:S(2)}) async-start(bf16[8,512,128]{2,1,0:T(8,128)(2,1)} %get-tuple-element.18), calls=%async_computation | async-start | bytes 2097152 | tf_op jit(solution)/shard_map/all_to_all | solution.py:272
  19.6 40.1 %copy-start.4 = (bf16[256,2048]{1,0:T(8,128)(2,1)S(1)}, bf16[256,2048]{1,0:T(8,128)(2,1)}, u32[]{:S(2)}) copy-start(bf16[256,2048]{1,0:T(8,128)(2,1)} %refs_0_.1) | copy-start | bytes 3145732
  19.6 69.5 %copy-start.1 = (bf16[16,2048]{1,0:T(8,128)(2,1)S(1)}, bf16[16,2048]{1,0:T(8,128)(2,1)}, u32[]{:S(2)}) copy-start(bf16[16,2048]{1,0:T(8,128)(2,1)} %residual.1) | copy-start | bytes 196612
  19.6 69.5 %copy-start.3 = (f32[256]{0:T(256)S(1)}, f32[256]{0:T(256)}, u32[]{:S(2)}) copy-start(f32[256]{0:T(256)} %param.20) | copy-start | bytes 3076
  52.5 36.6 %all-to-all-start.1 = ((bf16[8,528,128]{2,1,0:T(8,128)(2,1)}), bf16[8,528,128]{2,1,0:T(8,128)(2,1)S(1)}, u32[]{:S(2)}, u32[]{:S(2)}) async-start(bf16[8,528,128]{2,1,0:T(8,128)(2,1)} %attend.1), calls=%async_computation.1 | async-start | bytes 2162688 | tf_op jit(solution)/shard_map/all_to_all | solution.py:272
  59.7 26.5 %collective-permute-start = (bf16[256,2048]{1,0:T(8,128)(2,1)S(1)}, bf16[256,2048]{1,0:T(8,128)(2,1)}, u32[]{:S(2)}, u32[]{:S(2)}) collective-permute-start(bf16[256,2048]{1,0:T(8,128)(2,1)S(1)} %copy-done.4), channel_id=1, source_target_pairs={{0,2},{2,4},{4,6},{6,0},{1,3},{3,5},{5,7},{7,1},{8,10},{10,12},{12... | collective-permute-start | bytes 3145736 | tf_op jit(solution)/shard_map/ppermute | solution.py:340
  63.1 31.8 %collective-permute-start.1 = (bf16[256,2048]{1,0:T(8,128)(2,1)S(1)}, bf16[256,2048]{1,0:T(8,128)(2,1)}, u32[]{:S(2)}, u32[]{:S(2)}) collective-permute-start(bf16[256,2048]{1,0:T(8,128)(2,1)S(1)} %copy-done.4), channel_id=1, source_target_pairs={{2,0},{4,2},{6,4},{0,6},{3,1},{5,3},{7,5},{1,7},{10,8},{12,10},{14... | collective-permute-start | bytes 3145736 | tf_op jit(solution)/shard_map/ppermute | solution.py:355
  86.3 28.7 %collective-permute-start.2 = (bf16[256,2048]{1,0:T(8,128)(2,1)}, bf16[256,2048]{1,0:T(8,128)(2,1)}, u32[]{:S(2)}, u32[]{:S(2)}) collective-permute-start(bf16[256,2048]{1,0:T(8,128)(2,1)} %collective-permute-done.refs_1_), channel_id=1, source_target_pairs={{0,2},{2,4},{4,6},{6,0},{1,3},{3,5},{5,7},{7,1},{8,10},{10,12},{12... | collective-permute-start | bytes 3145736 | tf_op jit(solution)/shard_map/ppermute | solution.py:354
  90.6 27.1 %all-to-all-start.2 = ((bf16[4,256,256]{2,1,0:T(8,128)(2,1)}), bf16[4,256,256]{2,1,0:T(8,128)(2,1)S(1)}, u32[]{:S(2)}, u32[]{:S(2)}) async-start(bf16[4,256,256]{2,1,0:T(8,128)(2,1)} %join.1), calls=%async_computation.2 | async-start | bytes 1048576 | tf_op jit(solution)/shard_map/all_to_all | solution.py:272
  94.8 28.0 %slice-start = ((f32[3,704]{1,0:T(4,128)}), f32[3,640]{1,0:T(4,128)S(1)}, s32[]{:S(2)}) async-start(f32[3,704]{1,0:T(4,128)} %param.26), calls=%async_computation.5 | async-start | bytes 20480 | tf_op jit(solution)/shard_map/slice | solution.py:411
  94.8 28.0 %slice-start.1 = ((f32[3,704]{1,0:T(4,128)}), f32[3,64]{1,0:T(4,128)S(1)}, s32[]{:S(2)}) async-start(f32[3,704]{1,0:T(4,128)} %param.26), calls=%async_computation.6 | async-start | bytes 4096 | tf_op jit(solution)/shard_map/slice | solution.py:411
  94.8 29.8 %copy-start.2 = (f32[2048]{0:T(1024)S(1)}, f32[2048]{0:T(1024)}, u32[]{:S(2)}) copy-start(f32[2048]{0:T(1024)} %param.23) | copy-start | bytes 24580
  120.9 3.8 %collective-permute-start.3 = (bf16[128,2048]{1,0:T(8,128)(2,1)S(1)}, bf16[128,2048]{1,0:T(8,128)(2,1)S(1)}, u32[]{:S(2)}, u32[]{:S(2)}) collective-permute-start(bf16[128,2048]{1,0:T(8,128)(2,1)S(1)} %get-tuple-element.20), channel_id=1, source_target_pairs={{0,1},{1,0},{2,3},{3,2},{4,5},{5,4},{6,7},{7,6},{8,9},{9,8},{10,11... | collective-permute-start | bytes 1572872 | tf_op jit(solution)/shard_map/ppermute | solution.py:377
  128.1 7.2 %copy-start = (bf16[704,2048]{1,0:T(8,128)(2,1)S(1)}, bf16[704,2048]{1,0:T(8,128)(2,1)}, u32[]{:S(2)}) copy-start(bf16[704,2048]{1,0:T(8,128)(2,1)} %weight.1) | copy-start | bytes 8650756
  128.1 7.2 %collective-permute-start.4 = (bf16[16,768]{1,0:T(8,128)(2,1)S(1)}, bf16[16,768]{1,0:T(8,128)(2,1)S(1)}, u32[]{:S(2)}, u32[]{:S(2)}) collective-permute-start(bf16[16,768]{1,0:T(8,128)(2,1)S(1)} %get-tuple-element.25), channel_id=1, source_target_pairs={{0,8},{8,16},{16,24},{24,32},{32,40},{40,48},{48,56},{56,64},{64,7... | collective-permute-start | bytes 73736 | tf_op jit(solution)/shard_map/ppermute | solution.py:398
  136.9 3.4 %collective-permute-start.5 = (bf16[64,2048]{1,0:T(8,128)(2,1)S(1)}, bf16[64,2048]{1,0:T(8,128)(2,1)S(1)}, u32[]{:S(2)}, u32[]{:S(2)}) collective-permute-start(bf16[64,2048]{1,0:T(8,128)(2,1)S(1)} %get-tuple-element.27), channel_id=1, source_target_pairs={{0,1},{1,0},{2,3},{3,2},{4,5},{5,4},{6,7},{7,6},{8,9},{9,8},{10,11... | collective-permute-start | bytes 786440 | tf_op jit(solution)/shard_map/ppermute | solution.py:424
Sparse Core Ops, SparseCore 0:
  10.3 95.7 all-gather.1

commit v11 on v10

--- a/solution.py
+++ b/solution.py
@@ -36,20 +36,27 @@
     return pl.BlockSpec(memory_space=pltpu.VMEM)
 
 
-def pack_kernel(q1, q2, k1, k2, v, lift, gate, qsend, ksend, wsend, vv, ll, gg, rows, sems, sent):
+def rows_kernel(lift, gate, wsend, ll, gg, sems):
+    moves = [
+        pltpu.make_async_copy(gate, gg, sems.at[0]),
+        pltpu.make_async_copy(lift, ll, sems.at[1]),
+    ]
+    for move in moves:
+        move.start()
+    for move in moves:
+        move.wait()
+    for n in range(TILES):
+        wsend[32 * n : 32 * n + 32, :] = gg[:, 128 * n : 128 * n + 128]
+        wsend[192 + 32 * n : 224 + 32 * n, :] = ll[:, 128 * n : 128 * n + 128]
+    wsend[160:192, :] = jnp.concatenate([ll[:, MAIN:], gg[:, MAIN:]], axis=1)
+
+
+def pack_kernel(q1, q2, k1, k2, v, qsend, ksend, vv, rows, sems, sent):
+    sources = (k1, k2, v, q1, q2)
+    targets = (rows.at[0:128], rows.at[128:256], vv, qsend.at[0:128], qsend.at[128:256])
     moves = [
         pltpu.make_async_copy(src, dst, sems.at[i])
-        for i, (src, dst) in enumerate(
-            (
-                (k1, rows.at[0:128]),
-                (k2, rows.at[128:256]),
-                (v, vv),
-                (lift, ll),
-                (gate, gg),
-                (q1, qsend.at[0:128]),
-                (q2, qsend.at[128:256]),
-            )
-        )
+        for i, (src, dst) in enumerate(zip(sources, targets))
     ]
     for move in moves:
         move.start()
@@ -57,10 +64,6 @@
         move.wait()
     rows[256:384, :] = vv[:, 0:128]
     rows[384:512, :] = vv[:, 128:256]
-    for n in range(TILES):
-        wsend[32 * n : 32 * n + 32, :] = gg[:, 128 * n : 128 * n + 128]
-        wsend[192 + 32 * n : 224 + 32 * n, :] = ll[:, 128 * n : 128 * n + 128]
-    wsend[160:192, :] = jnp.concatenate([ll[:, MAIN:], gg[:, MAIN:]], axis=1)
     copies = [pltpu.make_async_copy(rows, ksend.at[i], sent.at[i]) for i in range(SIDE)]
     for copy in copies:
         copy.start()
@@ -313,26 +316,39 @@
     hbm = pl.BlockSpec(memory_space=pltpu.HBM)
     x = lax.axis_index("x")
     place = jnp.stack([core, x, 2 * x + core]).astype(jnp.int32)
-    qsend, ksend, wsend = pl.pallas_call(
+    wsend = pl.pallas_call(
+        rows_kernel,
+        out_shape=pltpu.HBM((352, 128), bf16),
+        in_specs=[hbm] * 2,
+        out_specs=vmem(),
+        scratch_shapes=[
+            pltpu.VMEM((32, 704), bf16),
+            pltpu.VMEM((32, 704), bf16),
+            pltpu.SemaphoreType.DMA((2,)),
+        ],
+        compiler_params=SMALL,
+        name="rows",
+    )(in_hbm(lift_weight), in_hbm(gate_weight))
+    wsend, *sources = lax.optimization_barrier(
+        (wsend, query_one, query_two, key_one, key_two, values)
+    )
+    qsend, ksend = pl.pallas_call(
         pack_kernel,
         out_shape=[
             jax.ShapeDtypeStruct((256, 128), bf16),
             jax.ShapeDtypeStruct((SIDE, SENT, 128), bf16),
-            pltpu.HBM((352, 128), bf16),
-        ],
-        in_specs=[hbm] * 7,
-        out_specs=[vmem(), hbm, vmem()],
+        ],
+        in_specs=[hbm] * 5,
+        out_specs=[vmem(), hbm],
         scratch_shapes=[
             pltpu.VMEM((128, 256), bf16),
-            pltpu.VMEM((32, 704), bf16),
-            pltpu.VMEM((32, 704), bf16),
             pltpu.VMEM((SENT, 128), bf16),
-            pltpu.SemaphoreType.DMA((7,)),
+            pltpu.SemaphoreType.DMA((5,)),
             pltpu.SemaphoreType.DMA((SIDE,)),
         ],
         compiler_params=SMALL,
         name="pack",
-    )(*(in_hbm(a) for a in (query_one, query_two, key_one, key_two, values, lift_weight, gate_weight)))
+    )(*(in_hbm(a) for a in sources))
     kpool = swapped(ksend, ALL, K_GROUPS)
     qpool = gathered(qsend, ALL, Q_GROUPS).reshape(SIDE, 256, 128)
     weights = in_hbm(gathered(wsend, ("z", "y")).reshape(SIDE, SIDE, 352, 128))

time: 158 us -> 158 us (level)
  transfers between devices with their start and end apart: 10 -> 10, of which waited for: 6 -> 6; matrix products, arithmetic and copies ran while one was open for 0% -> 0% of each run, Pallas kernels for 6% -> 8%
where the time goes in v11:
time: 158 us
  waiting for transfers between devices  49.2 us (31%)
  blocking collectives  37.5 us (24%)
  starting transfers between devices  37.1 us (23%)
  Pallas kernels  19.5 us (12%)
  between operations  14.2 us (9%)
    all_gather x1, blocking collectives, gathered(): return lax.all_gather(a, axis, axis_index_groups=groups, axis=0, tiled=True)  27.8 us
    all_to_all x3, starting transfers between devices, swapped(): return lax.all_to_all(a, axis, 0, 0, axis_index_groups=groups, tiled=True)  21.7 us
    ppermute x1, waiting for transfers between devices, on_device(): across = lax.ppermute(above, 'x', ring)  19.7 us
    ppermute x1, waiting for transfers between devices, on_device(): above = lax.ppermute(out_weight, 'x', ring)  19.1 us
    all_to_all x1, blocking collectives, swapped(): return lax.all_to_all(a, axis, 0, 0, axis_index_groups=groups, tiled=True)  9.64 us
    pallas_call x1, Pallas kernels, on_device(): pl.pallas_call(attend_kernel, out_shape=pltpu.HBM((SIDE, PACK, 128), bf16...  5.04 us
    ppermute x1, waiting for transfers between devices, on_device(): prior = lax.ppermute(edge, ('z', 'y'), route)  4.39 us
    ppermute x1, starting transfers between devices, on_device(): below = lax.ppermute(out_weight, 'x', [(j, i) for i, j in ring])  3.67 us
  transfers between devices with their start and end apart: 10, of which 6 were waited for; matrix products, arithmetic and copies ran while one was open for 0% of the time, Pallas kernels for 8%

profile of v11, /device:TPU:32, one launch (start us, length us, event | category | flops | bytes accessed | tf_op | source)
XLA Modules:
  0.0 157.7 jit_solution(3319447302334879206)
XLA Ops:
  6.5 1.5 rows.1
  8.1 2.0 %pack.1 = (bf16[256,128]{1,0:T(8,128)(2,1)S(1)}, bf16[8,512,128]{2,1,0:T(8,128)(2,1)}) custom-call(bf16[128,128]{1,0:T(8,128)(2,1)} %q1, bf16[128,128]{1,0:T(8,128)(2,1)} %q2, bf16[128,128]{1,0:T(8,128)(2,1)} %k1, bf16[128,128]{1,0:T(8,128)(2,1)} %k2, bf16[128,256]{1,0:T(8,128)(2,1)} %v), custom_call_target="tpu_custom_call" | custom-call | tf_op jit(solution)/shard_map/pack/pallas_call | solution.py:335
  10.1 10.3 %all-to-all-start = ((bf16[8,512,128]{2,1,0:T(8,128)(2,1)}), bf16[8,512,128]{2,1,0:T(8,128)(2,1)S(1)}, u32[]{:S(2)}, u32[]{:S(2)}) async-start(bf16[8,512,128]{2,1,0:T(8,128)(2,1)} %get-tuple-element.28), calls=%async_computation | async-start | bytes 2097152 | tf_op jit(solution)/shard_map/all_to_all | solution.py:275
  20.5 27.8 %all_gather.6 = bf16[2048,128]{1,0:T(8,128)(2,1)S(1)} all-gather(bf16[256,128]{1,0:T(8,128)(2,1)S(1)} %get-tuple-element.27), channel_id=1, replica_groups={{0,8,16,24,32,40,48,56},{2,10,18,26,34,42,50,58},{4,12,20,28,36,44,52,6..., dimensions={0}, use_global_device_ids=true | all-gather | bytes 589824 | tf_op jit(solution)/shard_map/all_gather | solution.py:279
  48.4 5.0 %attend.1 = bf16[8,528,128]{2,1,0:T(8,128)(2,1)} custom-call(s32[4]{0:T(128)S(1)} %broadcast_select_fusion.plan, bf16[8,256,128]{2,1,0:T(8,128)(2,1)S(1)} %bitcast.9, bf16[8,512,128]{2,1,0:T(8,128)(2,1)S(1)} %all-to-all-done.kpool), custom_call_target="tpu_custom_call" | custom-call | tf_op jit(solution)/shard_map/attend/pallas_call | solution.py:357
  53.4 7.2 %all-to-all-start.1 = ((bf16[8,528,128]{2,1,0:T(8,128)(2,1)}), bf16[8,528,128]{2,1,0:T(8,128)(2,1)S(1)}, u32[]{:S(2)}, u32[]{:S(2)}) async-start(bf16[8,528,128]{2,1,0:T(8,128)(2,1)} %attend.1), calls=%async_computation.1 | async-start | bytes 2162688 | tf_op jit(solution)/shard_map/all_to_all | solution.py:275
  60.6 3.4 %collective-permute-start = (bf16[256,2048]{1,0:T(8,128)(2,1)S(1)}, bf16[256,2048]{1,0:T(8,128)(2,1)}, u32[]{:S(2)}, u32[]{:S(2)}) collective-permute-start(bf16[256,2048]{1,0:T(8,128)(2,1)S(1)} %copy-done.4), channel_id=1, source_target_pairs={{0,2},{2,4},{4,6},{6,0},{1,3},{3,5},{5,7},{7,1},{8,10},{10,12},{12... | collective-permute-start | bytes 3145736 | tf_op jit(solution)/shard_map/ppermute | solution.py:356
  64.0 3.7 %collective-permute-start.1 = (bf16[256,2048]{1,0:T(8,128)(2,1)S(1)}, bf16[256,2048]{1,0:T(8,128)(2,1)}, u32[]{:S(2)}, u32[]{:S(2)}) collective-permute-start(bf16[256,2048]{1,0:T(8,128)(2,1)S(1)} %copy-done.4), channel_id=1, source_target_pairs={{2,0},{4,2},{6,4},{0,6},{3,1},{5,3},{7,5},{1,7},{10,8},{12,10},{14... | collective-permute-start | bytes 3145736 | tf_op jit(solution)/shard_map/ppermute | solution.py:371
  67.7 19.1 %collective-permute-done.refs_1_ = bf16[256,2048]{1,0:T(8,128)(2,1)} collective-permute-done((bf16[256,2048]{1,0:T(8,128)(2,1)S(1)}, bf16[256,2048]{1,0:T(8,128)(2,1)}, u32[]{:S(2)}, u32[]{:S(2)}) %collective-permute-start) | collective-permute-done | bytes 1048608 | tf_op jit(solution)/shard_map/ppermute | solution.py:356
  86.8 2.2 %collective-permute-start.2 = (bf16[256,2048]{1,0:T(8,128)(2,1)}, bf16[256,2048]{1,0:T(8,128)(2,1)}, u32[]{:S(2)}, u32[]{:S(2)}) collective-permute-start(bf16[256,2048]{1,0:T(8,128)(2,1)} %collective-permute-done.refs_1_), channel_id=1, source_target_pairs={{0,2},{2,4},{4,6},{6,0},{1,3},{3,5},{5,7},{7,1},{8,10},{10,12},{12... | collective-permute-start | bytes 3145736 | tf_op jit(solution)/shard_map/ppermute | solution.py:370
  89.7 1.4 join.1
  91.1 4.2 %all-to-all-start.2 = ((bf16[4,256,256]{2,1,0:T(8,128)(2,1)}), bf16[4,256,256]{2,1,0:T(8,128)(2,1)S(1)}, u32[]{:S(2)}, u32[]{:S(2)}) async-start(bf16[4,256,256]{2,1,0:T(8,128)(2,1)} %join.1), calls=%async_computation.2 | async-start | bytes 1048576 | tf_op jit(solution)/shard_map/all_to_all | solution.py:275
  95.4 19.7 %collective-permute-done.2.refs_3_ = bf16[256,2048]{1,0:T(8,128)(2,1)} collective-permute-done((bf16[256,2048]{1,0:T(8,128)(2,1)}, bf16[256,2048]{1,0:T(8,128)(2,1)}, u32[]{:S(2)}, u32[]{:S(2)}) %collective-permute-start.2) | collective-permute-done | bytes 1048608 | tf_op jit(solution)/shard_map/ppermute | solution.py:370
  115.1 2.7 %all-to-all-done.2.heads = bf16[4,256,256]{2,1,0:T(8,128)(2,1)S(1)} async-done(((bf16[4,256,256]{2,1,0:T(8,128)(2,1)}), bf16[4,256,256]{2,1,0:T(8,128)(2,1)S(1)}, u32[]{:S(2)}, u32[]{:S(2)}) %all-to-all-start.2) | async-done | bytes 524320 | tf_op jit(solution)/shard_map/all_to_all | solution.py:275
  117.8 3.2 %project.1 = (f32[128,2048]{1,0:T(8,128)S(1)}, bf16[128,2048]{1,0:T(8,128)(2,1)S(1)}) custom-call(s32[3]{0:T(128)S(1)} %pad_add_fusion.place, bf16[4,256,256]{2,1,0:T(8,128)(2,1)S(1)} %all-to-all-done.2.heads, bf16[256,2048]{1,0:T(8,128)(2,1)} %refs_0_.1, bf16[256,2048]{1,0:T(8,128)(2,1)} %collective-permute-done.refs_1_, ...), custom_call_target="tpu_custom_call" | custom-call | tf_op jit(solution)/shard_map/project/pallas_call | solution.py:381
  121.0 1.9 %collective-permute-start.3 = (bf16[128,2048]{1,0:T(8,128)(2,1)S(1)}, bf16[128,2048]{1,0:T(8,128)(2,1)S(1)}, u32[]{:S(2)}, u32[]{:S(2)}) collective-permute-start(bf16[128,2048]{1,0:T(8,128)(2,1)S(1)} %get-tuple-element.30), channel_id=1, source_target_pairs={{0,1},{1,0},{2,3},{3,2},{4,5},{5,4},{6,7},{7,6},{8,9},{9,8},{10,11... | collective-permute-start | bytes 1572872 | tf_op jit(solution)/shard_map/ppermute | solution.py:393
  123.1 1.8 %collective-permute-done.3.other = bf16[128,2048]{1,0:T(8,128)(2,1)S(1)} collective-permute-done((bf16[128,2048]{1,0:T(8,128)(2,1)S(1)}, bf16[128,2048]{1,0:T(8,128)(2,1)S(1)}, u32[]{:S(2)}, u32[]{:S(2)}) %collective-permute-start.3) | collective-permute-done | bytes 524320 | tf_op jit(solution)/shard_map/ppermute | solution.py:393
  124.8 3.5 %gate.3 = (bf16[128,768]{1,0:T(8,128)(2,1)S(1)}, bf16[16,768]{1,0:T(8,128)(2,1)S(1)}, bf16[128,2048]{1,0:T(8,128)(2,1)S(1)}, f32[16,2048]{1,0:T(8,128)S(1)}, bf16[8,8,160,128]{3,2,1,0:T(8,128)(2,1)S(1)}) custom-call(s32[3]{0:T(128)S(1)} %pad_add_fusion.place, f32[128,2048]{1,0:T(8,128)S(1)} %get-tuple-element.29.half, ...), custom_call_target="tpu_custom_call" | custom-call | tf_op jit(solution)/shard_map/gate/pallas_call | solution.py:394
  128.3 2.2 %collective-permute-start.4 = (bf16[16,768]{1,0:T(8,128)(2,1)S(1)}, bf16[16,768]{1,0:T(8,128)(2,1)S(1)}, u32[]{:S(2)}, u32[]{:S(2)}) collective-permute-start(bf16[16,768]{1,0:T(8,128)(2,1)S(1)} %get-tuple-element.35), channel_id=1, source_target_pairs={{0,8},{8,16},{16,24},{24,32},{32,40},{40,48},{48,56},{56,64},{64,7... | collective-permute-start | bytes 73736 | tf_op jit(solution)/shard_map/ppermute | solution.py:414
  131.1 4.4 %collective-permute-done.4.prior = bf16[16,768]{1,0:T(8,128)(2,1)S(1)} collective-permute-done((bf16[16,768]{1,0:T(8,128)(2,1)S(1)}, bf16[16,768]{1,0:T(8,128)(2,1)S(1)}, u32[]{:S(2)}, u32[]{:S(2)}) %collective-permute-start.4) | collective-permute-done | bytes 24608 | tf_op jit(solution)/shard_map/ppermute | solution.py:414
  135.5 1.6 down.1
  137.1 1.9 %collective-permute-start.5 = (bf16[64,2048]{1,0:T(8,128)(2,1)S(1)}, bf16[64,2048]{1,0:T(8,128)(2,1)S(1)}, u32[]{:S(2)}, u32[]{:S(2)}) collective-permute-start(bf16[64,2048]{1,0:T(8,128)(2,1)S(1)} %get-tuple-element.37), channel_id=1, source_target_pairs={{0,1},{1,0},{2,3},{3,2},{4,5},{5,4},{6,7},{7,6},{8,9},{9,8},{10,11... | collective-permute-start | bytes 786440 | tf_op jit(solution)/shard_map/ppermute | solution.py:440
  139.0 1.5 collective-permute-done.5.other
  140.6 9.6 %all_to_all.20.parts = bf16[4,16,2048]{2,1,0:T(8,128)(2,1)S(1)} all-to-all(bf16[4,16,2048]{2,1,0:T(8,128)(2,1)S(1)} %pair.1), channel_id=1, replica_groups=mesh['z'=8,'y'=8,'x'=4,'core'=2] {'x'}, dimensions={0} | all-to-all | bytes 524288 | tf_op jit(solution)/shard_map/all_to_all | solution.py:275
  (28 shorter events, 1.6 us)
Async XLA Ops:
  6.5 118.3 %all-gather.2.cloned.1.call-start = ((), (), s32[]{:S(2)}) async-start(), calls=%async_computation.4 | async-start | bytes 5857280 | tf_op jit(solution)/shard_map/all_gather | solution.py:279
  10.1 38.2 %all-to-all-start = ((bf16[8,512,128]{2,1,0:T(8,128)(2,1)}), bf16[8,512,128]{2,1,0:T(8,128)(2,1)S(1)}, u32[]{:S(2)}, u32[]{:S(2)}) async-start(bf16[8,512,128]{2,1,0:T(8,128)(2,1)} %get-tuple-element.28), calls=%async_computation | async-start | bytes 2097152 | tf_op jit(solution)/shard_map/all_to_all | solution.py:275
  20.5 40.1 %copy-start.4 = (bf16[256,2048]{1,0:T(8,128)(2,1)S(1)}, bf16[256,2048]{1,0:T(8,128)(2,1)}, u32[]{:S(2)}) copy-start(bf16[256,2048]{1,0:T(8,128)(2,1)} %refs_0_.1) | copy-start | bytes 3145732
  20.5 69.2 %copy-start.1 = (bf16[16,2048]{1,0:T(8,128)(2,1)S(1)}, bf16[16,2048]{1,0:T(8,128)(2,1)}, u32[]{:S(2)}) copy-start(bf16[16,2048]{1,0:T(8,128)(2,1)} %residual.1) | copy-start | bytes 196612
  20.5 69.2 %copy-start.3 = (f32[256]{0:T(256)S(1)}, f32[256]{0:T(256)}, u32[]{:S(2)}) copy-start(f32[256]{0:T(256)} %param.20) | copy-start | bytes 3076
  53.4 36.3 %all-to-all-start.1 = ((bf16[8,528,128]{2,1,0:T(8,128)(2,1)}), bf16[8,528,128]{2,1,0:T(8,128)(2,1)S(1)}, u32[]{:S(2)}, u32[]{:S(2)}) async-start(bf16[8,528,128]{2,1,0:T(8,128)(2,1)} %attend.1), calls=%async_computation.1 | async-start | bytes 2162688 | tf_op jit(solution)/shard_map/all_to_all | solution.py:275
  60.6 26.2 %collective-permute-start = (bf16[256,2048]{1,0:T(8,128)(2,1)S(1)}, bf16[256,2048]{1,0:T(8,128)(2,1)}, u32[]{:S(2)}, u32[]{:S(2)}) collective-permute-start(bf16[256,2048]{1,0:T(8,128)(2,1)S(1)} %copy-done.4), channel_id=1, source_target_pairs={{0,2},{2,4},{4,6},{6,0},{1,3},{3,5},{5,7},{7,1},{8,10},{10,12},{12... | collective-permute-start | bytes 3145736 | tf_op jit(solution)/shard_map/ppermute | solution.py:356
  64.0 31.4 %collective-permute-start.1 = (bf16[256,2048]{1,0:T(8,128)(2,1)S(1)}, bf16[256,2048]{1,0:T(8,128)(2,1)}, u32[]{:S(2)}, u32[]{:S(2)}) collective-permute-start(bf16[256,2048]{1,0:T(8,128)(2,1)S(1)} %copy-done.4), channel_id=1, source_target_pairs={{2,0},{4,2},{6,4},{0,6},{3,1},{5,3},{7,5},{1,7},{10,8},{12,10},{14... | collective-permute-start | bytes 3145736 | tf_op jit(solution)/shard_map/ppermute | solution.py:371
  86.8 28.3 %collective-permute-start.2 = (bf16[256,2048]{1,0:T(8,128)(2,1)}, bf16[256,2048]{1,0:T(8,128)(2,1)}, u32[]{:S(2)}, u32[]{:S(2)}) collective-permute-start(bf16[256,2048]{1,0:T(8,128)(2,1)} %collective-permute-done.refs_1_), channel_id=1, source_target_pairs={{0,2},{2,4},{4,6},{6,0},{1,3},{3,5},{5,7},{7,1},{8,10},{10,12},{12... | collective-permute-start | bytes 3145736 | tf_op jit(solution)/shard_map/ppermute | solution.py:370
  91.1 26.7 %all-to-all-start.2 = ((bf16[4,256,256]{2,1,0:T(8,128)(2,1)}), bf16[4,256,256]{2,1,0:T(8,128)(2,1)S(1)}, u32[]{:S(2)}, u32[]{:S(2)}) async-start(bf16[4,256,256]{2,1,0:T(8,128)(2,1)} %join.1), calls=%async_computation.2 | async-start | bytes 1048576 | tf_op jit(solution)/shard_map/all_to_all | solution.py:275
  95.3 27.6 %slice-start = ((f32[3,704]{1,0:T(4,128)}), f32[3,640]{1,0:T(4,128)S(1)}, s32[]{:S(2)}) async-start(f32[3,704]{1,0:T(4,128)} %param.26), calls=%async_computation.5 | async-start | bytes 20480 | tf_op jit(solution)/shard_map/slice | solution.py:427
  95.3 27.6 %slice-start.1 = ((f32[3,704]{1,0:T(4,128)}), f32[3,64]{1,0:T(4,128)S(1)}, s32[]{:S(2)}) async-start(f32[3,704]{1,0:T(4,128)} %param.26), calls=%async_computation.6 | async-start | bytes 4096 | tf_op jit(solution)/shard_map/slice | solution.py:427
  95.3 29.5 %copy-start.2 = (f32[2048]{0:T(1024)S(1)}, f32[2048]{0:T(1024)}, u32[]{:S(2)}) copy-start(f32[2048]{0:T(1024)} %param.23) | copy-start | bytes 24580
  121.0 3.8 %collective-permute-start.3 = (bf16[128,2048]{1,0:T(8,128)(2,1)S(1)}, bf16[128,2048]{1,0:T(8,128)(2,1)S(1)}, u32[]{:S(2)}, u32[]{:S(2)}) collective-permute-start(bf16[128,2048]{1,0:T(8,128)(2,1)S(1)} %get-tuple-element.30), channel_id=1, source_target_pairs={{0,1},{1,0},{2,3},{3,2},{4,5},{5,4},{6,7},{7,6},{8,9},{9,8},{10,11... | collective-permute-start | bytes 1572872 | tf_op jit(solution)/shard_map/ppermute | solution.py:393
  128.3 7.2 %copy-start = (bf16[704,2048]{1,0:T(8,128)(2,1)S(1)}, bf16[704,2048]{1,0:T(8,128)(2,1)}, u32[]{:S(2)}) copy-start(bf16[704,2048]{1,0:T(8,128)(2,1)} %weight.1) | copy-start | bytes 8650756
  128.3 7.2 %collective-permute-start.4 = (bf16[16,768]{1,0:T(8,128)(2,1)S(1)}, bf16[16,768]{1,0:T(8,128)(2,1)S(1)}, u32[]{:S(2)}, u32[]{:S(2)}) collective-permute-start(bf16[16,768]{1,0:T(8,128)(2,1)S(1)} %get-tuple-element.35), channel_id=1, source_target_pairs={{0,8},{8,16},{16,24},{24,32},{32,40},{40,48},{48,56},{56,64},{64,7... | collective-permute-start | bytes 73736 | tf_op jit(solution)/shard_map/ppermute | solution.py:414
  137.1 3.4 %collective-permute-start.5 = (bf16[64,2048]{1,0:T(8,128)(2,1)S(1)}, bf16[64,2048]{1,0:T(8,128)(2,1)S(1)}, u32[]{:S(2)}, u32[]{:S(2)}) collective-permute-start(bf16[64,2048]{1,0:T(8,128)(2,1)S(1)} %get-tuple-element.37), channel_id=1, source_target_pairs={{0,1},{1,0},{2,3},{3,2},{4,5},{5,4},{6,7},{7,6},{8,9},{9,8},{10,11... | collective-permute-start | bytes 786440 | tf_op jit(solution)/shard_map/ppermute | solution.py:440
Sparse Core Ops, SparseCore 0:
  10.3 96.3 all-gather.1
